TPU v7x, 32 devices: a whole 2x2x4 slice. The times are simulated.
32 devices in a mesh: grp: 2 (over x), tp: 4 (over z), dp: 4 (over y, core).
Axes of the slice: x: 2, y: 2, z: 4, core: 2. Of those that a mesh axis runs over, the one named last changes fastest.
Arguments:
- hidden: bfloat16 [16, 2048], P('grp', 'dp'), parts along dimension 0, may hold values from -20 to 20
- lengths: int32 [16], P(('grp', 'dp')), parts along dimension 0, may hold values from 1 to 256, 512 in all
- input_norm_gain: float32 [2, 2048], P(None, 'dp'), may hold values from 0.1 to 1.9
- gate_matrix: bfloat16 [2, 2048, 4096], P(None, 'dp', 'tp'), may hold values from -0.125 to 0.125
- input_matrix: bfloat16 [2, 2048, 4096], P(None, 'dp', 'tp'), may hold values from -0.125 to 0.125
- write_matrix: bfloat16 [2, 2048, 2048], P(None, 'dp', 'tp'), may hold values from -0.125 to 0.125
- read_matrix: bfloat16 [2, 2048, 2048], P(None, 'dp', 'tp'), may hold values from -0.125 to 0.125
- step_matrix: bfloat16 [2, 2048, 64], P(None, 'dp'), may hold values from -0.125 to 0.125
- step_size_bias: float32 [2, 64], P(None, 'tp'), may hold values from -2 to 1
- log_decay_rate: float32 [2, 64], P(None, 'tp'), may hold values from -1 to 2
- direct_path_gain: float32 [2, 64], P(None, 'tp'), may hold values from 0.5 to 1.5
- input_filter_taps: bfloat16 [2, 4, 4096], P(None, None, 'tp'), may hold values from -3 to 3
- write_filter_taps: bfloat16 [2, 4, 2048], P(None, None, 'tp'), may hold values from -3 to 3
- read_filter_taps: bfloat16 [2, 4, 2048], P(None, None, 'tp'), may hold values from -3 to 3
- position_log_decay: float32 [2, 256, 64], P(None, None, 'tp'), may hold values from -0.7 to 0
- grouped_norm_gain: float32 [2, 4096], P(None, 'tp'), may hold values from 0.1 to 1.9
- output_matrix: bfloat16 [2, 4096, 2048], P(None, 'tp', 'dp'), may hold values from -0.09375 to 0.09375
- recurrent_head_state: float32 [2, 16, 64, 64, 128], P(None, ('grp', 'dp'), 'tp'), parts along dimension 1, may hold values from -3 to 3
- history_input_rows: bfloat16 [2, 16, 3, 4096], P(None, ('grp', 'dp'), None, 'tp'), parts along dimension 1, may hold values from -5 to 5
- history_write_rows: bfloat16 [2, 16, 3, 2048], P(None, ('grp', 'dp'), None, 'tp'), parts along dimension 1, may hold values from -5 to 5
- history_read_rows: bfloat16 [2, 16, 3, 2048], P(None, ('grp', 'dp'), None, 'tp'), parts along dimension 1, may hold values from -5 to 5
Outputs:
- stream_out: bfloat16 [16, 2048], P('grp', 'dp'), parts along dimension 0
- state_out: float32 [2, 16, 64, 64, 128], P(None, ('grp', 'dp'), 'tp'), parts along dimension 1
- buffer_value_out: bfloat16 [2, 16, 3, 4096], P(None, ('grp', 'dp'), None, 'tp'), parts along dimension 1
- buffer_write_out: bfloat16 [2, 16, 3, 2048], P(None, ('grp', 'dp'), None, 'tp'), parts along dimension 1
- buffer_read_out: bfloat16 [2, 16, 3, 2048], P(None, ('grp', 'dp'), None, 'tp'), parts along dimension 1
There are 2 independent parts, one for each index of `grp`. A program takes and returns all parts, laid end to end along the dimension named above; an argument that names none is the same for every part. Nothing has to cross between parts.
Inputs may be any that keep to these rules, and one draw needn't show every extreme that they name: `lengths`: a sequence's current token stands at position length - 1; some sequence has length 256.
All inputs are finite; a program needn't handle non-finite values. No bound on the sum of `lengths` on one device may be relied on, other than what follows from the above.
Results may differ from a plain program's by a relative error of at most 0.0065.
Values may be sent and summed in bfloat16 or wider, within the bound.
No kernel may reach another device: no remote copies, remote signals or barrier semaphores. Data moves between devices by JAX's collectives and lax.ppermute only.
A program may use at most 64 MiB of HBM per device.

v0:
```python
import jax
import jax.numpy as jnp
from jax import lax
from jax.sharding import PartitionSpec as P

D = 2048


epsilon = 1e-06


def convolve(buffer, new_row, weights, tap_valid):
    tap_rows = weights.astype(jnp.float32)
    depth = weights.shape[0] - 1
    summed = new_row.astype(jnp.float32) * tap_rows[depth]
    for k in range(depth):
        summed = summed + buffer[:, k].astype(jnp.float32) * tap_rows[k] * tap_valid[:, k : k + 1]
    shifted = jnp.concatenate([buffer[:, 1:], new_row[:, None]], axis=1)
    return (jax.nn.silu(summed), shifted)


def spread_groups(rows, seq_local, groups_local, per_group, state_dim):
    grouped = rows.reshape(seq_local, groups_local, 1, state_dim)
    return jnp.broadcast_to(grouped, (seq_local, groups_local, per_group, state_dim)).reshape(
        seq_local, groups_local * per_group, state_dim
    )


def on_device(
    hidden,
    lengths,
    input_norm_gain,
    gate_matrix,
    input_matrix,
    write_matrix,
    read_matrix,
    step_matrix,
    step_size_bias,
    log_decay_rate,
    direct_path_gain,
    input_filter_taps,
    write_filter_taps,
    read_filter_taps,
    position_log_decay,
    grouped_norm_gain,
    output_matrix,
    recurrent_head_state,
    history_input_rows,
    history_write_rows,
    history_read_rows,
):
    seq_local = lengths.shape[0]
    heads_local = step_size_bias.shape[1]
    head_dim = recurrent_head_state.shape[3]
    state_dim = recurrent_head_state.shape[4]
    groups_local = write_filter_taps.shape[2] // state_dim
    per_group = heads_local // groups_local
    inner_local = heads_local * head_dim
    shared_local = groups_local * state_dim
    depth = input_filter_taps.shape[1] - 1
    token_position = lengths - 1
    tap_valid = (jnp.arange(depth)[None, :] >= depth - token_position[:, None]).astype(jnp.float32)
    state_is_valid = (token_position > 0).astype(jnp.float32)[:, None]
    position_indicator = (
        token_position[:, None] == jnp.arange(position_log_decay.shape[1])[None, :]
    ).astype(jnp.float32)
    head_first = lax.axis_index("tp") * heads_local
    seq_first = lax.axis_index("dp") * seq_local
    share_rows = hidden.shape[0] // lax.axis_size("tp")
    share_first = lax.axis_index("tp") * share_rows
    stream = hidden
    states, values, writes, reads = ([], [], [], [])
    for layer_index in range(input_norm_gain.shape[0]):
        stream_float = stream.astype(jnp.float32)
        squares = jnp.sum(stream_float * stream_float, axis=1)
        normed = (stream_float * input_norm_gain[layer_index]).astype(jnp.bfloat16)
        pieces = [
            jnp.dot(normed, weight[layer_index], preferred_element_type=jnp.float32)
            for weight in (gate_matrix, input_matrix, write_matrix, read_matrix)
        ]
        joined = jnp.concatenate(pieces, axis=1)
        step_weight = step_matrix[layer_index]
        step_term = jnp.dot(normed, step_weight, preferred_element_type=jnp.float32)
        squares_all = lax.psum(squares, "dp")
        joined_mine, step_mine = (
            lax.psum_scatter(joined, "dp", scatter_dimension=0, tiled=True),
            lax.psum_scatter(step_term, "dp", scatter_dimension=0, tiled=True),
        )
        mean_square = lax.dynamic_slice_in_dim(squares_all, seq_first, seq_local, 0) / D
        row_scale = lax.rsqrt(mean_square + epsilon)[:, None]
        step_raw = lax.dynamic_slice_in_dim(step_mine, head_first, heads_local, 1) * row_scale
        scaled = joined_mine * row_scale
        proj_gate = scaled[:, :inner_local]
        value_row = scaled[:, inner_local : 2 * inner_local].astype(jnp.bfloat16)
        write_row = scaled[:, 2 * inner_local : 2 * inner_local + shared_local].astype(jnp.bfloat16)
        read_row = scaled[:, 2 * inner_local + shared_local :].astype(jnp.bfloat16)
        value_act, value_buf = convolve(
            history_input_rows[layer_index], value_row, input_filter_taps[layer_index], tap_valid
        )
        write_act, write_buf = convolve(
            history_write_rows[layer_index], write_row, write_filter_taps[layer_index], tap_valid
        )
        read_act, read_buf = convolve(
            history_read_rows[layer_index], read_row, read_filter_taps[layer_index], tap_valid
        )
        head_step_size = jax.nn.softplus(step_raw + step_size_bias[layer_index])
        current_log_decay = jnp.dot(
            position_indicator, position_log_decay[layer_index], precision=lax.Precision.HIGHEST
        )
        current_decay = (
            jnp.exp(-jnp.exp(log_decay_rate[layer_index]) * head_step_size + current_log_decay)
            * state_is_valid
        )
        value_heads = value_act.reshape(seq_local, heads_local, head_dim)
        write_heads = spread_groups(write_act, seq_local, groups_local, per_group, state_dim)
        read_heads = spread_groups(read_act, seq_local, groups_local, per_group, state_dim)
        updated = (
            current_decay[:, :, None, None] * recurrent_head_state[layer_index]
            + (head_step_size[:, :, None] * value_heads)[:, :, :, None] * write_heads[:, :, None, :]
        )
        readout = jnp.einsum("shpn,shn->shp", updated, read_heads, precision=lax.Precision.HIGHEST)
        mixed_heads = (
            readout + direct_path_gain[layer_index][None, :, None] * value_heads
        ) * jax.nn.silu(proj_gate.reshape(seq_local, heads_local, head_dim))
        grouped = mixed_heads.reshape(seq_local, groups_local, per_group * head_dim)
        grouped = grouped * lax.rsqrt(jnp.mean(grouped * grouped, axis=2, keepdims=True) + epsilon)
        gated_rows = (
            grouped.reshape(seq_local, inner_local) * grouped_norm_gain[layer_index]
        ).astype(jnp.bfloat16)
        out_weight = output_matrix[layer_index]

        def project(rows_in, first_row, out_weight=out_weight):
            return jnp.dot(rows_in, out_weight, preferred_element_type=jnp.float32)

        partial_out = project(lax.all_gather(gated_rows, "dp", axis=0, tiled=True), jnp.int32(0))
        branch_share = lax.psum_scatter(partial_out, "tp", scatter_dimension=0, tiled=True)
        stream_share = lax.dynamic_slice_in_dim(stream_float, share_first, share_rows, 0)
        new_share = (stream_share + branch_share).astype(jnp.bfloat16)
        stream = lax.all_gather(new_share, "tp", axis=0, tiled=True)
        states.append(updated)
        values.append(value_buf)
        writes.append(write_buf)
        reads.append(read_buf)
    return (stream, jnp.stack(states), jnp.stack(values), jnp.stack(writes), jnp.stack(reads))


def solution(mesh):
    placed = (
        P("grp", "dp"),
        P(("grp", "dp")),
        P(None, "dp"),
        P(None, "dp", "tp"),
        P(None, "dp", "tp"),
        P(None, "dp", "tp"),
        P(None, "dp", "tp"),
        P(None, "dp", None),
        P(None, "tp"),
        P(None, "tp"),
        P(None, "tp"),
        P(None, None, "tp"),
        P(None, None, "tp"),
        P(None, None, "tp"),
        P(None, None, "tp"),
        P(None, "tp"),
        P(None, "tp", "dp"),
        P(None, ("grp", "dp"), "tp", None, None),
        P(None, ("grp", "dp"), None, "tp"),
        P(None, ("grp", "dp"), None, "tp"),
        P(None, ("grp", "dp"), None, "tp"),
    )
    return jax.shard_map(
        on_device,
        mesh=mesh,
        in_specs=placed,
        out_specs=(
            P("grp", "dp"),
            P(None, ("grp", "dp"), "tp", None, None),
            P(None, ("grp", "dp"), None, "tp"),
            P(None, ("grp", "dp"), None, "tp"),
            P(None, ("grp", "dp"), None, "tp"),
        ),
        check_vma=False,
    )
```

profile of v0, /device:TPU:0, one launch (start us, length us, event | category | flops | bytes accessed | tf_op | source)
XLA Modules:
  0.0 185.2 jit_solution(15273092470525130623)
XLA Ops:
  7.4 0.8 fusion.114
  8.2 1.3 fusion.38
  9.5 1.2 fusion.36
  10.8 1.5 fusion.17
  12.3 0.2 fusion.15
  12.5 0.7 pad_maximum_fusion.1
  13.3 0.1 multiply_reduce_fusion.3
  13.4 0.6 dynamic-slice
  14.7 0.5 slice_bitcast_fusion.31
  15.2 0.6 negate_bitcast_fusion
  15.8 0.1 fusion.52
  16.1 8.5 %all-reduce.7 = (f32[8]{0:T(128)S(1)}, f32[8,64]{1,0:T(8,128)S(1)}) all-reduce(f32[8]{0:T(128)S(1)} %multiply_reduce_fusion.3, f32[8,64]{1,0:T(8,128)S(1)} %fusion.52), channel_id=1, replica_groups=mesh['grp'=2,'tp'=4,'dp'=4] {'dp'}, use_global_device_ids=true, to_apply=%region_2.0 | all-reduce | flops 520 | bytes 4160 | tf_op jit(solution)/shard_map/psum | solution.py:84
  24.6 0.1 add_rsqrt_fusion.3
  24.7 0.6 fusion.111
  25.4 0.1 compare_select_fusion.1
  25.5 1.5 fusion.2
  27.0 0.6 slice_bitcast_fusion.30
  27.6 0.6 dynamic-slice.4
  28.8 19.0 %all-reduce.11.cloned.1.call-done = f32[8,3072]{1,0:T(8,128)} async-done(((f32[8,3072]{1,0:T(8,128)}), f32[8,3072]{1,0:T(8,128)}) %all-reduce.11.cloned.1.call-update) | async-done | bytes 98320
  47.8 1.0 fusion.106
  48.8 0.8 divide_multiply_fusion.5
  49.7 0.1 divide_multiply_fusion.1
  49.8 0.1 reshape.186
  49.9 0.8 broadcast_multiply_fusion.1
  50.7 3.1 %fusion.20 = f32[2,16,1,64]{3,2,1,0:T(1,128)S(1)} fusion(f32[2,16,128,1]{2,3,1,0:T(1,128)S(1)} %bitcast.277, f32[2,2,16,64,128]{4,3,2,1,0:T(8,128)} %param.38, f32[2,16,128]{2,1,0:T(8,128)S(1)} %bitcast.270, f32[2,16,64]{2,1,0:T(8,128)S(1)} %broadcast_multiply_fusion.1, f32[2,16]{1,0:T(2,128)} %fusion.2), kind=kOutput, calls=%fused_computation.24 | convolution fusion | flops 3932160 | bytes 1098752 | tf_op jit(solution)/shard_map/shpn,shn->shp/dot_general | solution.py:121
  53.8 0.8 multiply_reduce_fusion.2
  54.6 0.1 reduce_sum.52
  54.7 0.1 reduce_sum.53
  54.9 0.1 reshape.189
  55.0 5.2 %all-gather = bf16[4,2,1024]{2,1,0:T(2,128)(2,1)S(1)} all-gather(bf16[1,2,1024]{2,1,0:T(2,128)(2,1)S(1)} %fusion.72), channel_id=1, replica_groups=mesh['grp'=2,'tp'=4,'dp'=4] {'dp'}, dimensions={0}, use_global_device_ids=true | all-gather | bytes 20480 | tf_op jit(solution)/shard_map/all_gather | solution.py:135
  60.2 1.5 fusion.13
  61.7 18.7 %all-reduce.2 = f32[8,512]{1,0:T(8,128)S(1)} all-reduce(f32[8,512]{1,0:T(8,128)S(1)} %fusion.13), channel_id=4, replica_groups=mesh['grp'=2,'tp'=4,'dp'=4] {'tp'}, use_global_device_ids=true, to_apply=%region_6.7.clone | all-reduce | flops 4096 | bytes 32768
  80.4 11.9 %all-gather.1 = bf16[4,2,512]{2,1,0:T(2,128)(2,1)S(1)} all-gather(bf16[1,2,512]{2,1,0:T(2,128)(2,1)S(1)} %fusion.100), channel_id=1, replica_groups=mesh['grp'=2,'tp'=4,'dp'=4] {'tp'}, dimensions={0}, use_global_device_ids=true | all-gather | bytes 10240 | tf_op jit(solution)/shard_map/all_gather | solution.py:139
  92.4 0.1 multiply_convert_fusion
  92.5 0.1 fusion.50
  92.6 0.2 fusion.32
  92.8 1.4 fusion.34
  94.2 0.3 fusion.6
  94.5 0.3 fusion.8
  94.7 5.9 %all-reduce.6 = (f32[8]{0:T(128)S(1)}, f32[8,64]{1,0:T(8,128)S(1)}) all-reduce(f32[8]{0:T(128)S(1)} %get-tuple-element.28, f32[8,64]{1,0:T(8,128)S(1)} %fusion.50), channel_id=1, replica_groups=mesh['grp'=2,'tp'=4,'dp'=4] {'dp'}, use_global_device_ids=true, to_apply=%region_9.10 | all-reduce | flops 520 | bytes 4160 | tf_op jit(solution)/shard_map/psum | solution.py:84
  100.7 0.1 add_rsqrt_fusion.2
  100.8 0.7 pad_maximum_fusion.2
  101.5 0.1 compare_select_fusion
  101.6 0.9 fusion.3
  102.5 28.3 %all-reduce.13.cloned.1.call-done = f32[8,3072]{1,0:T(8,128)} async-done(((f32[8,3072]{1,0:T(8,128)}), f32[8,3072]{1,0:T(8,128)}) %all-reduce.13.cloned.1.call-update) | async-done | bytes 98320
  130.9 1.0 fusion.105
  131.9 0.1 divide_multiply_fusion.3
  132.0 0.1 divide_multiply_fusion
  132.1 0.1 reshape.190
  132.4 2.2 %multiply_add_fusion.1 = (f32[1,2,16,64,128]{4,3,2,1,0:T(8,128)S(1)}, f32[1,2,16,64,128]{4,3,2,1,0:T(8,128)S(1)}) fusion(f32[2,2,16,64,128]{4,3,2,1,0:T(8,128)} %param.38, f32[2,16,128]{2,1,0:T(8,128)S(1)} %bitcast.271, f32[2,16,64]{2,1,0:T(8,128)S(1)} %broadcast_multiply_fusion.1, f32[2,16]{1,0:T(2,128)S(1)} %copy-done.19, f32[2,16,128]{2,1,0:T(8,128)S(1)} %bitcast.272, ...), kind=kLoop, calls=%fused_computation.26 | loop fusion | flops 1572864 | bytes 4243712 | tf_op jit(solution)/shard_map/add | solution.py:118
  134.6 1.9 %fusion.11 = f32[2,16,1,64]{3,2,1,0:T(1,128)S(1)} fusion(f32[2,16,128,1]{2,3,1,0:T(1,128)S(1)} %bitcast.276, f32[2,2,16,64,128]{4,3,2,1,0:T(8,128)S(1)} %copy-done.2, f32[2,16,128]{2,1,0:T(8,128)S(1)} %bitcast.273, f32[2,16,64]{2,1,0:T(8,128)S(1)} %broadcast_multiply_fusion, f32[2,16]{1,0:T(2,128)S(1)} %fusion.3), kind=kOutput, calls=%fused_computation.15 | convolution fusion | flops 3932160 | bytes 1106944 | tf_op jit(solution)/shard_map/shpn,shn->shp/dot_general | solution.py:121
  136.5 0.2 multiply_reduce_fusion
  136.6 0.1 reduce_sum.56
  136.7 0.1 reduce_sum.57
  136.9 0.1 reshape.193
  137.0 5.2 %all-gather.2 = bf16[4,2,1024]{2,1,0:T(2,128)(2,1)S(1)} all-gather(bf16[1,2,1024]{2,1,0:T(2,128)(2,1)S(1)} %fusion.73), channel_id=1, replica_groups=mesh['grp'=2,'tp'=4,'dp'=4] {'dp'}, dimensions={0}, use_global_device_ids=true | all-gather | bytes 20480 | tf_op jit(solution)/shard_map/all_gather | solution.py:135
  142.2 1.5 fusion.4
  143.7 18.7 %all-reduce.5 = f32[8,512]{1,0:T(8,128)S(1)} all-reduce(f32[8,512]{1,0:T(8,128)S(1)} %fusion.4), channel_id=7, replica_groups=mesh['grp'=2,'tp'=4,'dp'=4] {'tp'}, use_global_device_ids=true, to_apply=%region_13.14.clone | all-reduce | flops 4096 | bytes 32768
  162.4 11.9 %all-gather.3 = bf16[4,2,512]{2,1,0:T(2,128)(2,1)S(1)} all-gather(bf16[1,2,512]{2,1,0:T(2,128)(2,1)S(1)} %fusion.101), channel_id=1, replica_groups=mesh['grp'=2,'tp'=4,'dp'=4] {'tp'}, dimensions={0}, use_global_device_ids=true | all-gather | bytes 10240 | tf_op jit(solution)/shard_map/all_gather | solution.py:139
  174.4 0.6 reshape.219
  175.0 0.6 pad_maximum_fusion.5
  175.6 0.6 pad_maximum_fusion.3
  176.3 0.6 pad_maximum_fusion.4
  176.9 1.5 pad_maximum_fusion
  (115 shorter events, 1.1 us)
Async XLA Ops:
  7.2 6.3 %copy-start.25 = (u32[32]{0:T(128)S(1)}, u32[32]{0:T(128)}, u32[]{:S(2)}) copy-start(u32[32]{0:T(128)} %constant.58) | copy-start | bytes 388
  7.2 5.1 %copy-start.4 = (bf16[8,512]{1,0:T(8,128)(2,1)S(1)}, bf16[8,512]{1,0:T(8,128)(2,1)}, u32[]{:S(2)}) copy-start(bf16[8,512]{1,0:T(8,128)(2,1)} %param.21) | copy-start | bytes 24580
  7.2 5.1 %copy-start = (bf16[2,512,1024]{2,1,0:T(8,128)(2,1)S(1)}, bf16[2,512,1024]{2,1,0:T(8,128)(2,1)}, u32[]{:S(2)}) copy-start(bf16[2,512,1024]{2,1,0:T(8,128)(2,1)} %param.25) | copy-start | bytes 6291460
  7.2 6.2 %copy-start.21 = (s32[2]{0:T(128)S(1)}, s32[2]{0:T(128)}, u32[]{:S(2)}) copy-start(s32[2]{0:T(128)} %param.22) | copy-start | bytes 28
  7.2 7.5 %copy-start.16 = (f32[2,16]{1,0:T(2,128)S(1)}, f32[2,16]{1,0:T(2,128)}, u32[]{:S(2)}) copy-start(f32[2,16]{1,0:T(2,128)} %param.29) | copy-start | bytes 388
  7.2 8.0 %copy-start.17 = (f32[2,16]{1,0:T(2,128)S(1)}, f32[2,16]{1,0:T(2,128)}, u32[]{:S(2)}) copy-start(f32[2,16]{1,0:T(2,128)} %param.30) | copy-start | bytes 388
  7.2 8.6 %copy-start.5 = (bf16[2,512,64]{1,2,0:T(8,128)(2,1)S(1)}, bf16[2,512,64]{1,2,0:T(8,128)(2,1)}, u32[]{:S(2)}) copy-start(bf16[2,512,64]{1,2,0:T(8,128)(2,1)} %param.28) | copy-start | bytes 393220
  7.2 8.7 %copy-start.12 = (f32[2,1024]{1,0:T(2,128)S(1)}, f32[2,1024]{1,0:T(2,128)}, u32[]{:S(2)}) copy-start(f32[2,1024]{1,0:T(2,128)} %param.36) | copy-start | bytes 24580
  7.3 8.7 %copy-start.10 = (bf16[2,4,512]{2,1,0:T(4,128)(2,1)S(1)}, bf16[2,4,512]{2,1,0:T(4,128)(2,1)}, u32[]{:S(2)}) copy-start(bf16[2,4,512]{2,1,0:T(4,128)(2,1)} %param.33) | copy-start | bytes 24580
  7.3 8.7 %copy-start.11 = (bf16[2,4,512]{2,1,0:T(4,128)(2,1)S(1)}, bf16[2,4,512]{2,1,0:T(4,128)(2,1)}, u32[]{:S(2)}) copy-start(bf16[2,4,512]{2,1,0:T(4,128)(2,1)} %param.34) | copy-start | bytes 24580
  7.3 8.7 %copy-start.6 = (bf16[2,2,3,1024]{3,1,2,0:T(2,128)(2,1)S(1)}, bf16[2,2,3,1024]{3,1,2,0:T(2,128)(2,1)}, u32[]{:S(2)}) copy-start(bf16[2,2,3,1024]{3,1,2,0:T(2,128)(2,1)} %param.39) | copy-start | bytes 73732
  7.3 8.7 %copy-start.7 = (bf16[2,4,1024]{2,1,0:T(4,128)(2,1)S(1)}, bf16[2,4,1024]{2,1,0:T(4,128)(2,1)}, u32[]{:S(2)}) copy-start(bf16[2,4,1024]{2,1,0:T(4,128)(2,1)} %param.32) | copy-start | bytes 49156
  7.3 18.0 %copy-start.8 = (bf16[2,2,3,512]{3,1,2,0:T(2,128)(2,1)S(1)}, bf16[2,2,3,512]{3,1,2,0:T(2,128)(2,1)}, u32[]{:S(2)}) copy-start(bf16[2,2,3,512]{3,1,2,0:T(2,128)(2,1)} %param.41) | copy-start | bytes 36868
  7.3 18.0 %copy-start.9 = (bf16[2,2,3,512]{3,1,2,0:T(2,128)(2,1)S(1)}, bf16[2,2,3,512]{3,1,2,0:T(2,128)(2,1)}, u32[]{:S(2)}) copy-start(bf16[2,2,3,512]{3,1,2,0:T(2,128)(2,1)} %param.40) | copy-start | bytes 36868
  7.3 40.5 %all-reduce.11.cloned.1.call-start = ((), (), s32[]{:S(2)}) async-start(), calls=%async_computation | async-start | bytes 196608
  8.2 18.8 %copy-start.18 = (f32[2,16]{1,0:T(2,128)S(1)}, f32[2,16]{1,0:T(2,128)}, u32[]{:S(2)}) copy-start(f32[2,16]{1,0:T(2,128)} %param.31) | copy-start | bytes 388
  8.2 19.4 %copy-start.24 = (u32[32]{0:T(128)S(1)}, u32[32]{0:T(128)}, u32[]{:S(2)}) copy-start(u32[32]{0:T(128)} %constant.66) | copy-start | bytes 388
  12.5 80.1 %copy-start.3 = (bf16[2,512,512]{2,1,0:T(8,128)(2,1)S(1)}, bf16[2,512,512]{2,1,0:T(8,128)(2,1)}, u32[]{:S(2)}) copy-start(bf16[2,512,512]{2,1,0:T(8,128)(2,1)} %param.27) | copy-start | bytes 3145732
  13.2 117.7 %all-reduce.13.cloned.1.call-start = ((), (), s32[]{:S(2)}) async-start(), calls=%async_computation.1 | async-start | bytes 196608
  13.4 14.2 %copy-start.26 = (f32[2]{0:T(128)}, f32[2]{0:T(128)S(1)}, u32[]{:S(2)}) copy-start(f32[2]{0:T(128)S(1)} %compare_convert_fusion) | copy-start | bytes 28
  13.4 14.2 %copy-start.22 = (s32[2]{0:T(128)}, s32[2]{0:T(128)S(1)}, u32[]{:S(2)}) copy-start(s32[2]{0:T(128)S(1)} %get-tuple-element.78) | copy-start | bytes 28
  25.5 3.4 %copy-start.13 = (f32[2,16]{1,0:T(2,128)}, f32[2,16]{1,0:T(2,128)S(1)}, u32[]{:S(2)}) copy-start(f32[2,16]{1,0:T(2,128)S(1)} %compare_select_fusion.1) | copy-start | bytes 388
  61.7 39.8 %copy-start.15 = (f32[16]{0:T(128)S(1)}, f32[16]{0:T(128)}, u32[]{:S(2)}) copy-start(f32[16]{0:T(128)} %get-tuple-element.76) | copy-start | bytes 196
  61.7 39.9 %copy-start.20 = (f32[16]{0:T(128)S(1)}, f32[16]{0:T(128)}, u32[]{:S(2)}) copy-start(f32[16]{0:T(128)} %get-tuple-element.74) | copy-start | bytes 196
  61.7 39.9 %copy-start.23 = (s32[2]{0:T(128)S(1)}, s32[2]{0:T(128)}, u32[]{:S(2)}) copy-start(s32[2]{0:T(128)} %copy-done.22) | copy-start | bytes 28
  61.7 39.9 %copy-start.27 = (f32[2]{0:T(128)S(1)}, f32[2]{0:T(128)}, u32[]{:S(2)}) copy-start(f32[2]{0:T(128)} %copy-done.26) | copy-start | bytes 28
  92.4 2.1 %copy-start.1 = (bf16[2,512,1024]{2,1,0:T(8,128)(2,1)S(1)}, bf16[2,512,1024]{2,1,0:T(8,128)(2,1)}, u32[]{:S(2)}) copy-start(bf16[2,512,1024]{2,1,0:T(8,128)(2,1)} %param.24) | copy-start | bytes 6291460
  92.5 39.9 %copy-start.19 = (f32[2,16]{1,0:T(2,128)S(1)}, f32[2,16]{1,0:T(2,128)}, u32[]{:S(2)}) copy-start(f32[2,16]{1,0:T(2,128)} %fusion.2) | copy-start | bytes 388
  132.4 2.2 %copy-start.2 = (f32[2,2,16,64,128]{4,3,2,1,0:T(8,128)S(1)}, f32[2,2,16,64,128]{4,3,2,1,0:T(8,128)}, u32[]{:S(2)}) copy-start(f32[2,2,16,64,128]{4,3,2,1,0:T(8,128)} %param.38) | copy-start | bytes 6291460
  132.4 4.1 %copy-start.14 = (f32[16]{0:T(128)S(1)}, f32[16]{0:T(128)}, u32[]{:S(2)}) copy-start(f32[16]{0:T(128)} %get-tuple-element.72) | copy-start | bytes 196
Sparse Core Ops, SparseCore 0:
  13.3 34.4 all-reduce.10
  101.6 29.2 all-reduce.12
where the time goes:
time: 186 us; the launch traced here: 185 us
  blocking collectives  86.2 us (46%)
  waiting for transfers between devices  47.3 us (25%)
  matrix products  16.9 us (9%)
  between operations  15.9 us (9%)
  other arithmetic  13.2 us (7%)
  local copies, waits for them, and re-layouts  5.54 us (3%)
    unnamed x4, waiting for transfers between devices  47.3 us
    unnamed x2, blocking collectives  37.4 us
    all_gather x2, blocking collectives, on_device(): stream = lax.all_gather(new_share, 'tp', axis=0, tiled=True)  23.9 us
    psum x2, blocking collectives, on_device(): squares_all = lax.psum(squares, 'dp')  14.5 us
    all_gather x2, blocking collectives, on_device(): lax.all_gather(gated_rows, 'dp', axis=0, tiled=True)  10.4 us
    dot_general x8, matrix products, on_device(): jnp.dot(normed, weight[layer_index], preferred_element_type=jnp.float32)  6.41 us
    dot_general x2, matrix products, on_device(): jnp.einsum('shpn,shn->shp', updated, read_heads, precision=lax.Precision....  4.94 us
  transfers between devices with their start and end apart: 2, of which 2 were waited for; matrix products, arithmetic and copies ran while one was open for 4% of the time, Pallas kernels for 0%

commit v1 on v0

--- a/solution.py
+++ b/solution.py
@@ -24,6 +24,49 @@
     return jnp.broadcast_to(grouped, (seq_local, groups_local, per_group, state_dim)).reshape(
         seq_local, groups_local * per_group, state_dim
     )
+
+
+def direct(axis):
+    size = lax.axis_size(axis)
+    return size <= 8 and size & (size - 1) == 0
+
+
+def swap(array, axis, mask):
+    return lax.ppermute(array, axis, [(i, i ^ mask) for i in range(lax.axis_size(axis))])
+
+
+def tree_sum(parts):
+    while len(parts) > 1:
+        parts = [parts[i] + parts[i + 1] for i in range(0, len(parts), 2)]
+    return parts[0]
+
+
+def exchange_rows(rows, axis, count):
+    if not direct(axis):
+        return lax.psum_scatter(rows, axis, scatter_dimension=0, tiled=True)
+    me = lax.axis_index(axis)
+    parts = [
+        lax.dynamic_slice_in_dim(rows, (me ^ mask) * count, count, 0)
+        for mask in range(lax.axis_size(axis))
+    ]
+    return tree_sum([parts[0]] + [swap(parts[mask], axis, mask) for mask in range(1, len(parts))])
+
+
+def gather_rows(rows, axis):
+    if not direct(axis):
+        return lax.all_gather(rows, axis, axis=0, tiled=True)
+    me, size = lax.axis_index(axis), lax.axis_size(axis)
+    parts = [rows] + [swap(rows, axis, mask) for mask in range(1, size)]
+    whole = jnp.zeros((size,) + rows.shape, rows.dtype)
+    for mask in range(size):
+        whole = lax.dynamic_update_index_in_dim(whole, parts[mask], me ^ mask, 0)
+    return whole.reshape((size * rows.shape[0],) + rows.shape[1:])
+
+
+def sum_copies(rows, axis):
+    if not direct(axis):
+        return lax.psum(rows, axis)
+    return tree_sum([rows] + [swap(rows, axis, mask) for mask in range(1, lax.axis_size(axis))])
 
 
 def on_device(
@@ -65,9 +108,6 @@
         token_position[:, None] == jnp.arange(position_log_decay.shape[1])[None, :]
     ).astype(jnp.float32)
     head_first = lax.axis_index("tp") * heads_local
-    seq_first = lax.axis_index("dp") * seq_local
-    share_rows = hidden.shape[0] // lax.axis_size("tp")
-    share_first = lax.axis_index("tp") * share_rows
     stream = hidden
     states, values, writes, reads = ([], [], [], [])
     for layer_index in range(input_norm_gain.shape[0]):
@@ -78,18 +118,16 @@
             jnp.dot(normed, weight[layer_index], preferred_element_type=jnp.float32)
             for weight in (gate_matrix, input_matrix, write_matrix, read_matrix)
         ]
-        joined = jnp.concatenate(pieces, axis=1)
-        step_weight = step_matrix[layer_index]
-        step_term = jnp.dot(normed, step_weight, preferred_element_type=jnp.float32)
-        squares_all = lax.psum(squares, "dp")
-        joined_mine, step_mine = (
-            lax.psum_scatter(joined, "dp", scatter_dimension=0, tiled=True),
-            lax.psum_scatter(step_term, "dp", scatter_dimension=0, tiled=True),
-        )
-        mean_square = lax.dynamic_slice_in_dim(squares_all, seq_first, seq_local, 0) / D
-        row_scale = lax.rsqrt(mean_square + epsilon)[:, None]
+        step_term = jnp.dot(normed, step_matrix[layer_index], preferred_element_type=jnp.float32)
+        heads_all = step_term.shape[1]
+        width = sum(piece.shape[1] for piece in pieces)
+        joined = jnp.concatenate(pieces + [step_term, squares[:, None]], axis=1)
+        joined_mine = exchange_rows(joined, "dp", seq_local)
+        mean_square = joined_mine[:, width + heads_all :] / D
+        row_scale = lax.rsqrt(mean_square + epsilon)
+        step_mine = joined_mine[:, width : width + heads_all]
         step_raw = lax.dynamic_slice_in_dim(step_mine, head_first, heads_local, 1) * row_scale
-        scaled = joined_mine * row_scale
+        scaled = joined_mine[:, :width] * row_scale
         proj_gate = scaled[:, :inner_local]
         value_row = scaled[:, inner_local : 2 * inner_local].astype(jnp.bfloat16)
         write_row = scaled[:, 2 * inner_local : 2 * inner_local + shared_local].astype(jnp.bfloat16)
@@ -129,14 +167,10 @@
         ).astype(jnp.bfloat16)
         out_weight = output_matrix[layer_index]
 
-        def project(rows_in, first_row, out_weight=out_weight):
-            return jnp.dot(rows_in, out_weight, preferred_element_type=jnp.float32)
-
-        partial_out = project(lax.all_gather(gated_rows, "dp", axis=0, tiled=True), jnp.int32(0))
-        branch_share = lax.psum_scatter(partial_out, "tp", scatter_dimension=0, tiled=True)
-        stream_share = lax.dynamic_slice_in_dim(stream_float, share_first, share_rows, 0)
-        new_share = (stream_share + branch_share).astype(jnp.bfloat16)
-        stream = lax.all_gather(new_share, "tp", axis=0, tiled=True)
+        gathered = gather_rows(gated_rows, "dp")
+        partial_out = jnp.dot(gathered, out_weight, preferred_element_type=jnp.float32)
+        branch = sum_copies(partial_out, "tp")
+        stream = (stream_float + branch).astype(jnp.bfloat16)
         states.append(updated)
         values.append(value_buf)
         writes.append(write_buf)

time: 186 us -> 62.2 us (0.33)
  blocking collectives: 86.2 us -> 0 us
  waiting for transfers between devices: 47.3 us -> 12.3 us
  starting transfers between devices: 0.08 us -> 18.1 us
  between operations: 15.9 us -> 1.4 us
  other arithmetic: 13.2 us -> 9.12 us
  local copies, waits for them, and re-layouts: 5.54 us -> 2.86 us
    unnamed x4 -> x0, waiting for transfers between devices: 47.3 us -> none
    unnamed x2 -> x0, blocking collectives: 37.4 us -> none
    all_gather x4 -> x0, blocking collectives: 34.3 us -> none  [the longest x2 23.9 us: on_device(): stream = lax.all_gather(new_share, 'tp', axis=0, tiled=True)]
    ppermute x0 -> x18, starting transfers between devices: none -> 18.1 us  [swap(): lax.ppermute(array, axis, [(i, i ^ mask) for i in range(lax.axis_size(axi...]
    psum x2 -> x0, blocking collectives: 14.5 us -> none  [on_device(): squares_all = lax.psum(squares, 'dp')]
    ppermute x0 -> x18, waiting for transfers between devices: none -> 12.3 us  [swap(): lax.ppermute(array, axis, [(i, i ^ mask) for i in range(lax.axis_size(axi...]
  transfers between devices with their start and end apart: 2 -> 18, of which waited for: 2 -> 11; matrix products, arithmetic and copies ran while one was open for 4% -> 10% of each run, Pallas kernels for 0% -> 0%
where the time goes in v1:
time: 62.2 us; the launch traced here: 61.5 us
  starting transfers between devices  18.1 us (29%)
  matrix products  17.7 us (28%)
  waiting for transfers between devices  12.3 us (20%)
  other arithmetic  9.12 us (15%)
  local copies, waits for them, and re-layouts  2.86 us (5%)
  between operations  1.4 us (2%)
    ppermute x18, starting transfers between devices, swap(): lax.ppermute(array, axis, [(i, i ^ mask) for i in range(lax.axis_size(axi...  18.1 us
    ppermute x18, waiting for transfers between devices, swap(): lax.ppermute(array, axis, [(i, i ^ mask) for i in range(lax.axis_size(axi...  12.3 us
    dot_general x2, matrix products, on_device(): jnp.einsum('shpn,shn->shp', updated, read_heads, precision=lax.Precision....  6.15 us
    dot_general x8, matrix products, on_device(): jnp.dot(normed, weight[layer_index], preferred_element_type=jnp.float32)  6.14 us
    dot_general x2, matrix products, on_device(): jnp.dot(gathered, out_weight, preferred_element_type=jnp.float32)  3.07 us
    add x1, other arithmetic, on_device(): current_decay[:, :, None, None] * recurrent_head_state[layer_index]  2.02 us
    another operation x1, other arithmetic, on_device(): jnp.stack(states)  1.52 us
    dot_general x2, matrix products, on_device(): jnp.dot(position_indicator, position_log_decay[layer_index], precision=la...  1.26 us
  transfers between devices with their start and end apart: 18, of which 11 were waited for; matrix products, arithmetic and copies ran while one was open for 10% of the time, Pallas kernels for 0%

profile of v1, /device:TPU:0, one launch (start us, length us, event | category | flops | bytes accessed | tf_op | source)
XLA Modules:
  0.0 61.5 jit_solution(9689486493895060499)
XLA Ops:
  0.8 0.9 %fusion.57 = f32[8]{0:T(128)S(1)} fusion(bf16[8,512]{1,0:T(8,128)(2,1)} %param.21), kind=kLoop, calls=%fused_computation.73 | loop fusion | flops 12280 | bytes 8224 | tf_op jit(solution)/shard_map/reduce_sum | solution.py:115
  1.8 0.8 %fusion.135 = (f32[1,512]{1,0:T(1,128)S(1)}, f32[1,512]{1,0:T(1,128)S(1)}) fusion(f32[2,512]{1,0:T(2,128)} %param.23), kind=kLoop, calls=%fused_computation.256 | loop fusion | bytes 8192 | tf_op jit(solution)/shard_map/slice | solution.py:116
  2.6 1.0 %fusion.52 = f32[8,64]{1,0:T(8,128)S(1)} fusion(bf16[2,512,64]{1,2,0:T(8,128)(2,1)} %param.28, bf16[8,512]{1,0:T(8,128)(2,1)} %param.21, f32[512]{0:T(512)S(1)} %bitcast.269), kind=kOutput, calls=%fused_computation.57 | convolution fusion | flops 536576 | bytes 77824 | tf_op jit(solution)/shard_map/dot_general | solution.py:121
  3.6 1.2 %fusion.38 = f32[8,512]{1,0:T(8,128)S(1)} fusion(bf16[2,512,512]{2,1,0:T(8,128)(2,1)} %param.26, bf16[8,512]{1,0:T(8,128)(2,1)} %param.21, f32[512]{0:T(512)S(1)} %bitcast.270), kind=kOutput, calls=%fused_computation.43 | convolution fusion | flops 4206592 | bytes 550912 | tf_op jit(solution)/shard_map/dot_general | solution.py:118
  4.8 1.2 %fusion.36 = f32[8,512]{1,0:T(8,128)S(1)} fusion(bf16[2,512,512]{2,1,0:T(8,128)(2,1)} %param.27, bf16[8,512]{1,0:T(8,128)(2,1)} %param.21, f32[512]{0:T(512)S(1)} %bitcast.271), kind=kOutput, calls=%fused_computation.41 | convolution fusion | flops 4206592 | bytes 550912 | tf_op jit(solution)/shard_map/dot_general | solution.py:118
  6.0 1.5 %fusion.18 = f32[8,1024]{1,0:T(8,128)S(1)} fusion(bf16[2,512,1024]{2,1,0:T(8,128)(2,1)} %param.25, bf16[8,512]{1,0:T(8,128)(2,1)} %param.21, f32[512]{0:T(512)S(1)} %bitcast.272), kind=kOutput, calls=%fused_computation.21 | convolution fusion | flops 8400896 | bytes 1091584 | tf_op jit(solution)/shard_map/dot_general | solution.py:118
  7.5 0.2 fusion.20
  7.9 0.6 collective-permute-start
  8.5 2.6 %collective-permute-start.2 = (f32[2,3137]{1,0:T(2,128)S(1)}, f32[2,3137]{1,0:T(2,128)S(1)}, u32[]{:S(2)}, u32[]{:S(2)}) collective-permute-start(f32[2,3137]{1,0:T(2,128)S(1)} %get-tuple-element.21), channel_id=1, source_target_pairs={{0,3},{1,2},{2,1},{3,0},{4,7},{5,6},{6,5},{7,4},{8,11},{9,10},{10,... | collective-permute-start | bytes 75296 | tf_op jit(solution)/shard_map/ppermute | solution.py:35
  11.7 1.0 %collective-permute-done.2 = f32[2,3137]{1,0:T(2,128)S(1)} collective-permute-done((f32[2,3137]{1,0:T(2,128)S(1)}, f32[2,3137]{1,0:T(2,128)S(1)}, u32[]{:S(2)}, u32[]{:S(2)}) %collective-permute-start.2) | collective-permute-done | bytes 25128 | tf_op jit(solution)/shard_map/ppermute | solution.py:35
  12.6 2.3 %collective-permute-done.1 = f32[2,3137]{1,0:T(2,128)S(1)} collective-permute-done((f32[2,3137]{1,0:T(2,128)S(1)}, f32[2,3137]{1,0:T(2,128)S(1)}, u32[]{:S(2)}, u32[]{:S(2)}) %collective-permute-start.1) | collective-permute-done | bytes 25128 | tf_op jit(solution)/shard_map/ppermute | solution.py:35
  15.0 0.2 fusion.113
  15.3 0.1 divide_multiply_fusion.5
  15.4 0.1 divide_multiply_fusion.1
  15.9 1.1 %fusion.2 = f32[2,16]{1,0:T(2,128)S(1)} fusion(f32[2,256,16]{1,2,0:T(8,128)} %param.35, s32[2]{0:T(128)S(1)} %get-tuple-element.80, f32[2,16]{1,0:T(2,128)S(1)} %compare_select_fusion.1, f32[2]{0:T(128)S(1)} %compare_convert_fusion, f32[16]{0:T(128)S(1)} %get-tuple-element.77), kind=kOutput, calls=%fused_computation.5 | convolution fusion | flops 98912 | bytes 16720 | tf_op jit(solution)/shard_map/dot_general | solution.py:145
  16.9 3.1 %fusion.16 = f32[2,16,1,64]{3,2,1,0:T(1,128)S(1)} fusion(f32[2,16,128,1]{2,3,1,0:T(1,128)S(1)} %bitcast.284, f32[2,2,16,64,128]{4,3,2,1,0:T(8,128)} %param.38, f32[2,16,128]{2,1,0:T(8,128)S(1)} %bitcast.274, f32[2,16,64]{2,1,0:T(8,128)S(1)} %broadcast_multiply_fusion.1, f32[2,16]{1,0:T(2,128)S(1)} %fusion.2), kind=kOutput, calls=%fused_computation.20 | convolution fusion | flops 3932160 | bytes 1097856 | tf_op jit(solution)/shard_map/shpn,shn->shp/dot_general | solution.py:159
  20.0 0.2 multiply_reduce_fusion.1
  20.2 0.1 reshape.292
  20.3 0.1 reshape.291
  20.4 0.1 reduce_sum.53
  20.7 0.5 collective-permute-start.4
  21.3 1.3 %collective-permute-start.3 = (bf16[2,1024]{1,0:T(2,128)(2,1)S(1)}, bf16[2,1024]{1,0:T(2,128)(2,1)S(1)}, u32[]{:S(2)}, u32[]{:S(2)}) collective-permute-start(bf16[2,1024]{1,0:T(2,128)(2,1)S(1)} %multiply_convert_fusion.2), channel_id=1, source_target_pairs={{0,1},{1,0},{2,3},{3,2},{4,5},{5,4},{6,7},{7,6},{8,9},{9,8},{10,11... | collective-permute-start | bytes 12296 | tf_op jit(solution)/shard_map/ppermute | solution.py:35
  22.7 0.7 %collective-permute-done.3 = bf16[2,1024]{1,0:T(2,128)(2,1)S(1)} collective-permute-done((bf16[2,1024]{1,0:T(2,128)(2,1)S(1)}, bf16[2,1024]{1,0:T(2,128)(2,1)S(1)}, u32[]{:S(2)}, u32[]{:S(2)}) %collective-permute-start.3) | collective-permute-done | bytes 4128 | tf_op jit(solution)/shard_map/ppermute | solution.py:35
  23.4 1.0 %collective-permute-done.4 = bf16[2,1024]{1,0:T(2,128)(2,1)S(1)} collective-permute-done((bf16[2,1024]{1,0:T(2,128)(2,1)S(1)}, bf16[2,1024]{1,0:T(2,128)(2,1)S(1)}, u32[]{:S(2)}, u32[]{:S(2)}) %collective-permute-start.4) | collective-permute-done | bytes 4128 | tf_op jit(solution)/shard_map/ppermute | solution.py:35
  24.5 1.6 %fusion.13 = f32[8,512]{1,0:T(8,128)S(1)} fusion(bf16[8,1024]{1,0:T(8,128)(2,1)S(1)} %reshape.293, bf16[2,1024,512]{2,1,0:T(8,128)(2,1)} %param.37), kind=kOutput, calls=%fused_computation.16 | convolution fusion | flops 8388608 | bytes 1081344 | tf_op jit(solution)/shard_map/dot_general | solution.py:171
  26.1 3.6 %collective-permute-start.8 = (f32[8,512]{1,0:T(8,128)S(1)}, f32[8,512]{1,0:T(8,128)S(1)}, u32[]{:S(2)}, u32[]{:S(2)}) collective-permute-start(f32[8,512]{1,0:T(8,128)S(1)} %fusion.13), channel_id=1, source_target_pairs={{0,12},{4,8},{8,4},{12,0},{1,13},{5,9},{9,5},{13,1},{2,14},{6,10},... | collective-permute-start | bytes 49160 | tf_op jit(solution)/shard_map/ppermute | solution.py:35
  29.7 0.8 %collective-permute-start.6 = (f32[8,512]{1,0:T(8,128)S(1)}, f32[8,512]{1,0:T(8,128)S(1)}, u32[]{:S(2)}, u32[]{:S(2)}) collective-permute-start(f32[8,512]{1,0:T(8,128)S(1)} %fusion.13), channel_id=1, source_target_pairs={{0,4},{4,0},{8,12},{12,8},{1,5},{5,1},{9,13},{13,9},{2,6},{6,2},{1... | collective-permute-start | bytes 49160 | tf_op jit(solution)/shard_map/ppermute | solution.py:35
  30.5 1.3 %collective-permute-done.8 = f32[8,512]{1,0:T(8,128)S(1)} collective-permute-done((f32[8,512]{1,0:T(8,128)S(1)}, f32[8,512]{1,0:T(8,128)S(1)}, u32[]{:S(2)}, u32[]{:S(2)}) %collective-permute-start.8) | collective-permute-done | bytes 16416 | tf_op jit(solution)/shard_map/ppermute | solution.py:35
  31.8 2.5 %collective-permute-done.7 = f32[8,512]{1,0:T(8,128)S(1)} collective-permute-done((f32[8,512]{1,0:T(8,128)S(1)}, f32[8,512]{1,0:T(8,128)S(1)}, u32[]{:S(2)}, u32[]{:S(2)}) %collective-permute-start.7) | collective-permute-done | bytes 16416 | tf_op jit(solution)/shard_map/ppermute | solution.py:35
  34.3 0.1 fusion.60
  34.5 0.1 fusion.50
  34.6 0.2 fusion.34
  34.8 1.2 %fusion.32 = f32[8,512]{1,0:T(8,128)S(1)} fusion(bf16[2,512,512]{2,1,0:T(8,128)(2,1)} %param.27, bf16[8,512]{1,0:T(8,128)(2,1)S(1)} %get-tuple-element.10, f32[512]{0:T(512)S(1)} %bitcast.266), kind=kOutput, calls=%fused_computation.37 | convolution fusion | flops 4206592 | bytes 550912 | tf_op jit(solution)/shard_map/dot_general | solution.py:118
  36.0 0.3 fusion.9
  36.3 0.3 fusion.11
  36.8 0.6 collective-permute-start.11
  37.4 1.5 %collective-permute-start.10 = (f32[2,3137]{1,0:T(2,128)S(1)}, f32[2,3137]{1,0:T(2,128)S(1)}, u32[]{:S(2)}, u32[]{:S(2)}) collective-permute-start(f32[2,3137]{1,0:T(2,128)S(1)} %get-tuple-element.19), channel_id=1, source_target_pairs={{0,2},{1,3},{2,0},{3,1},{4,6},{5,7},{6,4},{7,5},{8,10},{9,11},{10,... | collective-permute-start | bytes 75296 | tf_op jit(solution)/shard_map/ppermute | solution.py:35
  39.0 1.2 %collective-permute-done.11 = f32[2,3137]{1,0:T(2,128)S(1)} collective-permute-done((f32[2,3137]{1,0:T(2,128)S(1)}, f32[2,3137]{1,0:T(2,128)S(1)}, u32[]{:S(2)}, u32[]{:S(2)}) %collective-permute-start.11) | collective-permute-done | bytes 25128 | tf_op jit(solution)/shard_map/ppermute | solution.py:35
  40.1 1.1 %collective-permute-done.10 = f32[2,3137]{1,0:T(2,128)S(1)} collective-permute-done((f32[2,3137]{1,0:T(2,128)S(1)}, f32[2,3137]{1,0:T(2,128)S(1)}, u32[]{:S(2)}, u32[]{:S(2)}) %collective-permute-start.10) | collective-permute-done | bytes 25128 | tf_op jit(solution)/shard_map/ppermute | solution.py:35
  41.3 0.2 fusion.114
  41.6 0.1 divide_multiply_fusion.3
  41.8 0.1 divide_multiply_fusion
  42.1 0.2 fusion.3
  42.4 3.1 %fusion.7 = f32[2,16,1,64]{3,2,1,0:T(1,128)S(1)} fusion(f32[2,16,128,1]{2,3,1,0:T(1,128)S(1)} %bitcast.285, f32[2,2,16,64,128]{4,3,2,1,0:T(8,128)} %param.38, f32[2,16,128]{2,1,0:T(8,128)S(1)} %bitcast.276, f32[2,16,64]{2,1,0:T(8,128)S(1)} %broadcast_multiply_fusion, f32[2,16]{1,0:T(2,128)S(1)} %fusion.3), kind=kOutput, calls=%fused_computation.11 | convolution fusion | flops 3932160 | bytes 1097856 | tf_op jit(solution)/shard_map/shpn,shn->shp/dot_general | solution.py:159
  45.5 0.2 multiply_reduce_fusion
  45.6 0.1 reshape.298
  45.7 0.1 reshape.297
  45.9 0.1 reduce_sum.57
  46.1 0.1 collective-permute-start.14
  46.2 1.5 %collective-permute-start.13 = (bf16[2,1024]{1,0:T(2,128)(2,1)S(1)}, bf16[2,1024]{1,0:T(2,128)(2,1)S(1)}, u32[]{:S(2)}, u32[]{:S(2)}) collective-permute-start(bf16[2,1024]{1,0:T(2,128)(2,1)S(1)} %multiply_convert_fusion), channel_id=1, source_target_pairs={{0,2},{1,3},{2,0},{3,1},{4,6},{5,7},{6,4},{7,5},{8,10},{9,11},{10,... | collective-permute-start | bytes 12296 | tf_op jit(solution)/shard_map/ppermute | solution.py:35
  47.8 0.3 collective-permute-start.12
  48.0 2.0 %multiply_add_fusion.1 = (f32[1,2,16,64,128]{4,3,2,1,0:T(8,128)S(1)}, f32[1,2,16,64,128]{4,3,2,1,0:T(8,128)S(1)}) fusion(f32[2,2,16,64,128]{4,3,2,1,0:T(8,128)} %param.38, f32[2,16,128]{2,1,0:T(8,128)S(1)} %bitcast.275, f32[2,16,64]{2,1,0:T(8,128)S(1)} %broadcast_multiply_fusion.1, f32[2,16]{1,0:T(2,128)S(1)} %fusion.2, f32[2,16,128]{2,1,0:T(8,128)S(1)} %bitcast.277, ...), kind=kLoop, calls=%fused_computation.26 | loop fusion | flops 1572864 | bytes 4243712 | tf_op jit(solution)/shard_map/add | solution.py:156
  50.2 0.6 %pad_maximum_fusion.3 = bf16[2,2,3,512]{3,1,2,0:T(2,128)(2,1)} fusion(bf16[1,2,3,512]{3,1,2,0:T(2,128)(2,1)S(1)} %maximum_bitcast_fusion.5, bf16[1,2,3,512]{3,1,2,0:T(2,128)(2,1)S(1)} %maximum_bitcast_fusion.4), kind=kLoop, calls=%fused_computation.89 | loop fusion | flops 6144 | bytes 24576 | tf_op jit(solution)/shard_map/stack | solution.py:178
  50.8 0.6 %pad_maximum_fusion.1 = bf16[2,2,3,1024]{3,1,2,0:T(2,128)(2,1)} fusion(bf16[1,2,3,1024]{3,1,2,0:T(2,128)(2,1)S(1)} %maximum_bitcast_fusion.1, bf16[1,2,3,1024]{3,1,2,0:T(2,128)(2,1)S(1)} %maximum_bitcast_fusion), kind=kLoop, calls=%fused_computation.65 | loop fusion | flops 12288 | bytes 49152 | tf_op jit(solution)/shard_map/stack | solution.py:178
  51.5 1.5 %pad_maximum_fusion = f32[2,2,16,64,128]{4,3,2,1,0:T(8,128)} fusion(f32[1,2,16,64,128]{4,3,2,1,0:T(8,128)S(1)} %get-tuple-element.16, f32[1,2,16,64,128]{4,3,2,1,0:T(8,128)S(1)} %get-tuple-element.15), kind=kLoop, calls=%fused_computation | loop fusion | flops 524288 | bytes 4194304 | tf_op jit(solution)/shard_map/stack | solution.py:178
  53.1 1.5 %fusion.4 = f32[8,512]{1,0:T(8,128)S(1)} fusion(bf16[8,1024]{1,0:T(8,128)(2,1)S(1)} %reshape.299, bf16[2,1024,512]{2,1,0:T(8,128)(2,1)} %param.37), kind=kOutput, calls=%fused_computation.7 | convolution fusion | flops 8388608 | bytes 1081344 | tf_op jit(solution)/shard_map/dot_general | solution.py:171
  54.6 1.5 %collective-permute-start.17 = (f32[8,512]{1,0:T(8,128)S(1)}, f32[8,512]{1,0:T(8,128)S(1)}, u32[]{:S(2)}, u32[]{:S(2)}) collective-permute-start(f32[8,512]{1,0:T(8,128)S(1)} %fusion.4), channel_id=1, source_target_pairs={{0,12},{4,8},{8,4},{12,0},{1,13},{5,9},{9,5},{13,1},{2,14},{6,10},... | collective-permute-start | bytes 49160 | tf_op jit(solution)/shard_map/ppermute | solution.py:35
  56.1 0.6 collective-permute-start.16
  56.7 2.3 %collective-permute-start.15 = (f32[8,512]{1,0:T(8,128)S(1)}, f32[8,512]{1,0:T(8,128)S(1)}, u32[]{:S(2)}, u32[]{:S(2)}) collective-permute-start(f32[8,512]{1,0:T(8,128)S(1)} %fusion.4), channel_id=1, source_target_pairs={{0,4},{4,0},{8,12},{12,8},{1,5},{5,1},{9,13},{13,9},{2,6},{6,2},{1... | collective-permute-start | bytes 49160 | tf_op jit(solution)/shard_map/ppermute | solution.py:35
  59.0 0.6 %pad_maximum_fusion.2 = bf16[2,2,3,512]{3,1,2,0:T(2,128)(2,1)} fusion(bf16[1,2,3,512]{3,1,2,0:T(2,128)(2,1)S(1)} %maximum_bitcast_fusion.3, bf16[1,2,3,512]{3,1,2,0:T(2,128)(2,1)S(1)} %maximum_bitcast_fusion.2), kind=kLoop, calls=%fused_computation.88 | loop fusion | flops 6144 | bytes 24576 | tf_op jit(solution)/shard_map/stack | solution.py:178
  59.6 0.6 collective-permute-done.17
  60.2 0.5 collective-permute-done.16
  60.7 0.2 collective-permute-done.15
  60.9 0.6 fusion.61
  (139 shorter events, 2.7 us)
Async XLA Ops:
  0.6 6.9 %copy-start.4 = (bf16[8,512]{1,0:T(8,128)(2,1)S(1)}, bf16[8,512]{1,0:T(8,128)(2,1)}, u32[]{:S(2)}) copy-start(bf16[8,512]{1,0:T(8,128)(2,1)} %param.21) | copy-start | bytes 24580
  0.6 6.9 %copy-start.1 = (bf16[2,512,1024]{2,1,0:T(8,128)(2,1)S(1)}, bf16[2,512,1024]{2,1,0:T(8,128)(2,1)}, u32[]{:S(2)}) copy-start(bf16[2,512,1024]{2,1,0:T(8,128)(2,1)} %param.24) | copy-start | bytes 6291460
  0.7 10.5 %copy-start.13 = (f32[2,16]{1,0:T(2,128)S(1)}, f32[2,16]{1,0:T(2,128)}, u32[]{:S(2)}) copy-start(f32[2,16]{1,0:T(2,128)} %param.29) | copy-start | bytes 388
  0.7 10.5 %copy-start.14 = (f32[2,16]{1,0:T(2,128)S(1)}, f32[2,16]{1,0:T(2,128)}, u32[]{:S(2)}) copy-start(f32[2,16]{1,0:T(2,128)} %param.30) | copy-start | bytes 388
  0.7 10.5 %copy-start.15 = (f32[2,16]{1,0:T(2,128)S(1)}, f32[2,16]{1,0:T(2,128)}, u32[]{:S(2)}) copy-start(f32[2,16]{1,0:T(2,128)} %param.31) | copy-start | bytes 388
  0.7 10.5 %copy-start.17 = (s32[2]{0:T(128)S(1)}, s32[2]{0:T(128)}, u32[]{:S(2)}) copy-start(s32[2]{0:T(128)} %param.22) | copy-start | bytes 28
  0.7 10.5 %copy-start.12 = (f32[2,1024]{1,0:T(2,128)S(1)}, f32[2,1024]{1,0:T(2,128)}, u32[]{:S(2)}) copy-start(f32[2,1024]{1,0:T(2,128)} %param.36) | copy-start | bytes 24580
  0.7 10.6 %copy-start.10 = (bf16[2,4,512]{2,1,0:T(4,128)(2,1)S(1)}, bf16[2,4,512]{2,1,0:T(4,128)(2,1)}, u32[]{:S(2)}) copy-start(bf16[2,4,512]{2,1,0:T(4,128)(2,1)} %param.33) | copy-start | bytes 24580
  0.7 10.6 %copy-start.11 = (bf16[2,4,512]{2,1,0:T(4,128)(2,1)S(1)}, bf16[2,4,512]{2,1,0:T(4,128)(2,1)}, u32[]{:S(2)}) copy-start(bf16[2,4,512]{2,1,0:T(4,128)(2,1)} %param.34) | copy-start | bytes 24580
  0.7 10.6 %copy-start.6 = (bf16[2,2,3,1024]{3,1,2,0:T(2,128)(2,1)S(1)}, bf16[2,2,3,1024]{3,1,2,0:T(2,128)(2,1)}, u32[]{:S(2)}) copy-start(bf16[2,2,3,1024]{3,1,2,0:T(2,128)(2,1)} %param.39) | copy-start | bytes 73732
  0.7 10.6 %copy-start.7 = (bf16[2,4,1024]{2,1,0:T(4,128)(2,1)S(1)}, bf16[2,4,1024]{2,1,0:T(4,128)(2,1)}, u32[]{:S(2)}) copy-start(bf16[2,4,1024]{2,1,0:T(4,128)(2,1)} %param.32) | copy-start | bytes 49156
  0.8 10.7 %copy-start.8 = (bf16[2,2,3,512]{3,1,2,0:T(2,128)(2,1)S(1)}, bf16[2,2,3,512]{3,1,2,0:T(2,128)(2,1)}, u32[]{:S(2)}) copy-start(bf16[2,2,3,512]{3,1,2,0:T(2,128)(2,1)} %param.41) | copy-start | bytes 36868
  0.8 10.7 %copy-start.9 = (bf16[2,2,3,512]{3,1,2,0:T(2,128)(2,1)S(1)}, bf16[2,2,3,512]{3,1,2,0:T(2,128)(2,1)}, u32[]{:S(2)}) copy-start(bf16[2,2,3,512]{3,1,2,0:T(2,128)(2,1)} %param.40) | copy-start | bytes 36868
  7.9 26.6 %copy-start.5 = (bf16[2,512,64]{1,2,0:T(8,128)(2,1)S(1)}, bf16[2,512,64]{1,2,0:T(8,128)(2,1)}, u32[]{:S(2)}) copy-start(bf16[2,512,64]{1,2,0:T(8,128)(2,1)} %param.28) | copy-start | bytes 393220
  7.9 26.7 %copy-start.3 = (bf16[2,512,512]{2,1,0:T(8,128)(2,1)S(1)}, bf16[2,512,512]{2,1,0:T(8,128)(2,1)}, u32[]{:S(2)}) copy-start(bf16[2,512,512]{2,1,0:T(8,128)(2,1)} %param.26) | copy-start | bytes 3145732
  7.9 3.7 %collective-permute-start = (f32[2,3137]{1,0:T(2,128)S(1)}, f32[2,3137]{1,0:T(2,128)S(1)}, u32[]{:S(2)}, u32[]{:S(2)}) collective-permute-start(f32[2,3137]{1,0:T(2,128)S(1)} %get-tuple-element.20), channel_id=1, source_target_pairs={{0,1},{1,0},{2,3},{3,2},{4,5},{5,4},{6,7},{7,6},{8,9},{9,8},{10,11... | collective-permute-start | bytes 75296 | tf_op jit(solution)/shard_map/ppermute | solution.py:35
  8.5 4.1 %collective-permute-start.2 = (f32[2,3137]{1,0:T(2,128)S(1)}, f32[2,3137]{1,0:T(2,128)S(1)}, u32[]{:S(2)}, u32[]{:S(2)}) collective-permute-start(f32[2,3137]{1,0:T(2,128)S(1)} %get-tuple-element.21), channel_id=1, source_target_pairs={{0,3},{1,2},{2,1},{3,0},{4,7},{5,6},{6,5},{7,4},{8,11},{9,10},{10,... | collective-permute-start | bytes 75296 | tf_op jit(solution)/shard_map/ppermute | solution.py:35
  11.1 3.8 %collective-permute-start.1 = (f32[2,3137]{1,0:T(2,128)S(1)}, f32[2,3137]{1,0:T(2,128)S(1)}, u32[]{:S(2)}, u32[]{:S(2)}) collective-permute-start(f32[2,3137]{1,0:T(2,128)S(1)} %get-tuple-element.22), channel_id=1, source_target_pairs={{0,2},{1,3},{2,0},{3,1},{4,6},{5,7},{6,4},{7,5},{8,10},{9,11},{10,... | collective-permute-start | bytes 75296 | tf_op jit(solution)/shard_map/ppermute | solution.py:35
  11.5 8.5 %copy-start.18 = (f32[2]{0:T(128)}, f32[2]{0:T(128)S(1)}, u32[]{:S(2)}) copy-start(f32[2]{0:T(128)S(1)} %compare_convert_fusion) | copy-start | bytes 28
  15.8 20.2 %copy-start = (bf16[2,512,1024]{2,1,0:T(8,128)(2,1)S(1)}, bf16[2,512,1024]{2,1,0:T(8,128)(2,1)}, u32[]{:S(2)}) copy-start(bf16[2,512,1024]{2,1,0:T(8,128)(2,1)} %param.25) | copy-start | bytes 6291460
  20.7 3.8 %collective-permute-start.5 = (bf16[2,1024]{1,0:T(2,128)(2,1)S(1)}, bf16[2,1024]{1,0:T(2,128)(2,1)S(1)}, u32[]{:S(2)}, u32[]{:S(2)}) collective-permute-start(bf16[2,1024]{1,0:T(2,128)(2,1)S(1)} %multiply_convert_fusion.2), channel_id=1, source_target_pairs={{0,3},{1,2},{2,1},{3,0},{4,7},{5,6},{6,5},{7,4},{8,11},{9,10},{10,... | collective-permute-start | bytes 12296 | tf_op jit(solution)/shard_map/ppermute | solution.py:35
  20.7 3.7 %collective-permute-start.4 = (bf16[2,1024]{1,0:T(2,128)(2,1)S(1)}, bf16[2,1024]{1,0:T(2,128)(2,1)S(1)}, u32[]{:S(2)}, u32[]{:S(2)}) collective-permute-start(bf16[2,1024]{1,0:T(2,128)(2,1)S(1)} %multiply_convert_fusion.2), channel_id=1, source_target_pairs={{0,2},{1,3},{2,0},{3,1},{4,6},{5,7},{6,4},{7,5},{8,10},{9,11},{10,... | collective-permute-start | bytes 12296 | tf_op jit(solution)/shard_map/ppermute | solution.py:35
  21.3 2.1 %collective-permute-start.3 = (bf16[2,1024]{1,0:T(2,128)(2,1)S(1)}, bf16[2,1024]{1,0:T(2,128)(2,1)S(1)}, u32[]{:S(2)}, u32[]{:S(2)}) collective-permute-start(bf16[2,1024]{1,0:T(2,128)(2,1)S(1)} %multiply_convert_fusion.2), channel_id=1, source_target_pairs={{0,1},{1,0},{2,3},{3,2},{4,5},{5,4},{6,7},{7,6},{8,9},{9,8},{10,11... | collective-permute-start | bytes 12296 | tf_op jit(solution)/shard_map/ppermute | solution.py:35
  24.5 11.8 %copy-start.2 = (bf16[2,512,1024]{2,1,0:T(8,128)(2,1)S(1)}, bf16[2,512,1024]{2,1,0:T(8,128)(2,1)}, u32[]{:S(2)}) copy-start(bf16[2,512,1024]{2,1,0:T(8,128)(2,1)} %param.24) | copy-start | bytes 6291460
  26.1 5.7 %collective-permute-start.8 = (f32[8,512]{1,0:T(8,128)S(1)}, f32[8,512]{1,0:T(8,128)S(1)}, u32[]{:S(2)}, u32[]{:S(2)}) collective-permute-start(f32[8,512]{1,0:T(8,128)S(1)} %fusion.13), channel_id=1, source_target_pairs={{0,12},{4,8},{8,4},{12,0},{1,13},{5,9},{9,5},{13,1},{2,14},{6,10},... | collective-permute-start | bytes 49160 | tf_op jit(solution)/shard_map/ppermute | solution.py:35
  29.7 4.6 %collective-permute-start.7 = (f32[8,512]{1,0:T(8,128)S(1)}, f32[8,512]{1,0:T(8,128)S(1)}, u32[]{:S(2)}, u32[]{:S(2)}) collective-permute-start(f32[8,512]{1,0:T(8,128)S(1)} %fusion.13), channel_id=1, source_target_pairs={{0,8},{4,12},{8,0},{12,4},{1,9},{5,13},{9,1},{13,5},{2,10},{6,14},... | collective-permute-start | bytes 49160 | tf_op jit(solution)/shard_map/ppermute | solution.py:35
  29.7 4.6 %collective-permute-start.6 = (f32[8,512]{1,0:T(8,128)S(1)}, f32[8,512]{1,0:T(8,128)S(1)}, u32[]{:S(2)}, u32[]{:S(2)}) collective-permute-start(f32[8,512]{1,0:T(8,128)S(1)} %fusion.13), channel_id=1, source_target_pairs={{0,4},{4,0},{8,12},{12,8},{1,5},{5,1},{9,13},{13,9},{2,6},{6,2},{1... | collective-permute-start | bytes 49160 | tf_op jit(solution)/shard_map/ppermute | solution.py:35
  34.5 7.6 %copy-start.16 = (f32[2,256,16]{1,2,0:T(8,128)S(1)}, f32[2,256,16]{1,2,0:T(8,128)}, u32[]{:S(2)}) copy-start(f32[2,256,16]{1,2,0:T(8,128)} %param.35) | copy-start | bytes 98308
  34.5 7.6 %copy-start.19 = (f32[2]{0:T(128)S(1)}, f32[2]{0:T(128)}, u32[]{:S(2)}) copy-start(f32[2]{0:T(128)} %copy-done.18) | copy-start | bytes 28
  36.7 2.2 %collective-permute-start.9 = (f32[2,3137]{1,0:T(2,128)S(1)}, f32[2,3137]{1,0:T(2,128)S(1)}, u32[]{:S(2)}, u32[]{:S(2)}) collective-permute-start(f32[2,3137]{1,0:T(2,128)S(1)} %get-tuple-element.17), channel_id=1, source_target_pairs={{0,1},{1,0},{2,3},{3,2},{4,5},{5,4},{6,7},{7,6},{8,9},{9,8},{10,11... | collective-permute-start | bytes 75296 | tf_op jit(solution)/shard_map/ppermute | solution.py:35
  36.8 3.3 %collective-permute-start.11 = (f32[2,3137]{1,0:T(2,128)S(1)}, f32[2,3137]{1,0:T(2,128)S(1)}, u32[]{:S(2)}, u32[]{:S(2)}) collective-permute-start(f32[2,3137]{1,0:T(2,128)S(1)} %get-tuple-element.18), channel_id=1, source_target_pairs={{0,3},{1,2},{2,1},{3,0},{4,7},{5,6},{6,5},{7,4},{8,11},{9,10},{10,... | collective-permute-start | bytes 75296 | tf_op jit(solution)/shard_map/ppermute | solution.py:35
  37.4 3.8 %collective-permute-start.10 = (f32[2,3137]{1,0:T(2,128)S(1)}, f32[2,3137]{1,0:T(2,128)S(1)}, u32[]{:S(2)}, u32[]{:S(2)}) collective-permute-start(f32[2,3137]{1,0:T(2,128)S(1)} %get-tuple-element.19), channel_id=1, source_target_pairs={{0,2},{1,3},{2,0},{3,1},{4,6},{5,7},{6,4},{7,5},{8,10},{9,11},{10,... | collective-permute-start | bytes 75296 | tf_op jit(solution)/shard_map/ppermute | solution.py:35
  46.1 7.0 %collective-permute-start.14 = (bf16[2,1024]{1,0:T(2,128)(2,1)S(1)}, bf16[2,1024]{1,0:T(2,128)(2,1)S(1)}, u32[]{:S(2)}, u32[]{:S(2)}) collective-permute-start(bf16[2,1024]{1,0:T(2,128)(2,1)S(1)} %multiply_convert_fusion), channel_id=1, source_target_pairs={{0,3},{1,2},{2,1},{3,0},{4,7},{5,6},{6,5},{7,4},{8,11},{9,10},{10,... | collective-permute-start | bytes 12296 | tf_op jit(solution)/shard_map/ppermute | solution.py:35
  46.2 6.9 %collective-permute-start.13 = (bf16[2,1024]{1,0:T(2,128)(2,1)S(1)}, bf16[2,1024]{1,0:T(2,128)(2,1)S(1)}, u32[]{:S(2)}, u32[]{:S(2)}) collective-permute-start(bf16[2,1024]{1,0:T(2,128)(2,1)S(1)} %multiply_convert_fusion), channel_id=1, source_target_pairs={{0,2},{1,3},{2,0},{3,1},{4,6},{5,7},{6,4},{7,5},{8,10},{9,11},{10,... | collective-permute-start | bytes 12296 | tf_op jit(solution)/shard_map/ppermute | solution.py:35
  47.8 5.3 %collective-permute-start.12 = (bf16[2,1024]{1,0:T(2,128)(2,1)S(1)}, bf16[2,1024]{1,0:T(2,128)(2,1)S(1)}, u32[]{:S(2)}, u32[]{:S(2)}) collective-permute-start(bf16[2,1024]{1,0:T(2,128)(2,1)S(1)} %multiply_convert_fusion), channel_id=1, source_target_pairs={{0,1},{1,0},{2,3},{3,2},{4,5},{5,4},{6,7},{7,6},{8,9},{9,8},{10,11... | collective-permute-start | bytes 12296 | tf_op jit(solution)/shard_map/ppermute | solution.py:35
  54.6 5.6 %collective-permute-start.17 = (f32[8,512]{1,0:T(8,128)S(1)}, f32[8,512]{1,0:T(8,128)S(1)}, u32[]{:S(2)}, u32[]{:S(2)}) collective-permute-start(f32[8,512]{1,0:T(8,128)S(1)} %fusion.4), channel_id=1, source_target_pairs={{0,12},{4,8},{8,4},{12,0},{1,13},{5,9},{9,5},{13,1},{2,14},{6,10},... | collective-permute-start | bytes 49160 | tf_op jit(solution)/shard_map/ppermute | solution.py:35
  56.1 4.6 %collective-permute-start.16 = (f32[8,512]{1,0:T(8,128)S(1)}, f32[8,512]{1,0:T(8,128)S(1)}, u32[]{:S(2)}, u32[]{:S(2)}) collective-permute-start(f32[8,512]{1,0:T(8,128)S(1)} %fusion.4), channel_id=1, source_target_pairs={{0,8},{4,12},{8,0},{12,4},{1,9},{5,13},{9,1},{13,5},{2,10},{6,14},... | collective-permute-start | bytes 49160 | tf_op jit(solution)/shard_map/ppermute | solution.py:35
  56.7 4.2 %collective-permute-start.15 = (f32[8,512]{1,0:T(8,128)S(1)}, f32[8,512]{1,0:T(8,128)S(1)}, u32[]{:S(2)}, u32[]{:S(2)}) collective-permute-start(f32[8,512]{1,0:T(8,128)S(1)} %fusion.4), channel_id=1, source_target_pairs={{0,4},{4,0},{8,12},{12,8},{1,5},{5,1},{9,13},{13,9},{2,6},{6,2},{1... | collective-permute-start | bytes 49160 | tf_op jit(solution)/shard_map/ppermute | solution.py:35

commit v2 on v1

--- a/solution.py
+++ b/solution.py
@@ -1,12 +1,665 @@
+import functools
+
 import jax
 import jax.numpy as jnp
 from jax import lax
+from jax.experimental import pallas as pl
+from jax.experimental.pallas import tpu as pltpu
 from jax.sharding import PartitionSpec as P
 
 D = 2048
 
 
 epsilon = 1e-06
+LANES = 128
+TABLE = 64
+f32 = jnp.float32
+bf16 = jnp.bfloat16
+VMEM = pltpu.VMEM
+
+
+def lane_iota(shape):
+    return lax.broadcasted_iota(jnp.int32, shape, 1)
+
+
+def pack(row):
+    return jnp.concatenate(
+        [row[:, i : i + LANES] for i in range(0, row.shape[1], LANES)], axis=0
+    )
+
+
+def unpack(rows):
+    return jnp.concatenate([rows[i : i + 1] for i in range(rows.shape[0])], axis=1)
+
+
+def column(row, count):
+    wide = jnp.broadcast_to(row[:, :count], (count, count))
+    eye = lane_iota((count, count)) == lax.broadcasted_iota(jnp.int32, (count, count), 0)
+    return jnp.broadcast_to(
+        jnp.sum(jnp.where(eye, wide, 0.0), axis=1, keepdims=True), (count, LANES)
+    )
+
+
+def interleave(scratch, rows):
+    half = rows.shape[0] // 2
+    scratch[...] = rows
+    even = scratch[pl.ds(0, half, stride=2), :]
+    odd = scratch[pl.ds(1, half, stride=2), :]
+    return jnp.where(lane_iota((half, LANES)) < LANES // 2, even, odd)
+
+
+def tree_sum(parts):
+    while len(parts) > 1:
+        parts = [parts[i] + parts[i + 1] for i in range(0, len(parts), 2)]
+    return parts[0]
+
+
+def start_all(pairs, sems):
+    copies = [pltpu.make_async_copy(source, target, sems.at[i]) for i, (source, target) in enumerate(pairs)]
+    for copy in copies:
+        copy.start()
+    return copies
+
+
+def halves(source, target, count=2):
+    size = target.shape[0] // count
+    return [
+        (source.at[pl.ds(i * size, size)], target.at[pl.ds(i * size, size)]) for i in range(count)
+    ]
+
+
+def project_rows(dims, x, gain, held, waits, outs, scratch):
+    seqs, chunks, shared, heads, rows, fan = dims
+    squares = jnp.sum(x * x, axis=1, keepdims=True)
+    normed = (x * gain).astype(bf16)
+    count = x.shape[0]
+    base = 0
+    for i in range(4):
+        for copy in waits[i]:
+            copy.wait()
+        piece = jnp.dot(normed, held[i][...], preferred_element_type=f32)
+        for c in range(piece.shape[1] // LANES):
+            scratch[pl.ds((base + c) * count, count), :] = piece[:, c * LANES : (c + 1) * LANES]
+        base += piece.shape[1] // LANES
+    for copy in waits[4]:
+        copy.wait()
+    step = lax.dot_general(
+        normed, held[4][...], (((1,), (1,)), ((), ())), preferred_element_type=f32
+    )
+    width = step.shape[1]
+    if width < LANES:
+        step = jnp.concatenate([step, jnp.zeros((count, LANES - width), f32)], axis=1)
+    shift = lax.rem(LANES - lax.axis_index("tp") * heads, LANES)
+    step = pltpu.roll(step, shift, 1)
+    last = jnp.where(lane_iota((count, LANES)) < heads, step, jnp.broadcast_to(squares, (count, LANES)))
+    scratch[pl.ds(base * count, count), :] = last
+    for i in range(base + 1, rows):
+        scratch[pl.ds(i * count, count), :] = jnp.zeros((count, LANES), f32)
+    me = lax.axis_index("dp")
+    for mask in range(fan):
+        first = lax.bitwise_xor(me, jnp.int32(mask)) * seqs
+        for s in range(seqs):
+            outs[mask][pl.ds(s * rows, rows), :] = scratch[pl.ds(first + s, rows, stride=count), :]
+
+
+def first_project_kernel(dims, layer, *refs):
+    fan = dims[5]
+    refs = list(refs)
+    x_hbm, gain_hbm = refs[:2]
+    weights = refs[2:7]
+    outs = refs[7 : 7 + fan]
+    x_ref, gain_ref = refs[7 + fan : 9 + fan]
+    held = refs[9 + fan : 14 + fan]
+    scratch, sems = refs[14 + fan :]
+    pairs = [(x_hbm, x_ref), (gain_hbm, gain_ref)]
+    spans = []
+    for source, target in zip(weights, held):
+        more = halves(source.at[layer], target)
+        spans.append((len(pairs), len(pairs) + len(more)))
+        pairs += more
+    copies = start_all(pairs, sems)
+    copies[0].wait()
+    copies[1].wait()
+    waits = [copies[low:high] for low, high in spans]
+    project_rows(
+        dims, x_ref[...].astype(f32), gain_ref[layer : layer + 1, :], held, waits, outs, scratch
+    )
+
+
+def next_project_kernel(dims, layer, *refs):
+    fan, tp = dims[5], lax.axis_size("tp")
+    refs = list(refs)
+    x_ref, parts, gain_ref = refs[0], refs[1 : 1 + tp], refs[1 + tp]
+    held = refs[2 + tp : 7 + tp]
+    new_ref = refs[7 + tp]
+    outs = refs[8 + tp : 8 + tp + fan]
+    scratch = refs[-1]
+    new = (x_ref[...].astype(f32) + tree_sum([part[...] for part in parts])).astype(bf16)
+    new_ref[...] = new
+    project_rows(
+        dims, new.astype(f32), gain_ref[layer : layer + 1, :], held, [[]] * 5, outs, scratch
+    )
+
+
+def table_kernel(dims, *refs):
+    seqs, chunks, shared, heads, rows, fan = dims
+    lengths_ref = refs[0]
+    sources = refs[2:13]
+    state, weight, gain, hidden = refs[13:17]
+    out, state_out, weight_out, gain_out, hidden_out, split_out = refs[17:23]
+    hv, hw, hr, tv, tw, tr, bias, rate, direct, pos, norm = held = refs[23:34]
+    scratch, sems = refs[34:]
+    copies = start_all(
+        list(zip(sources, held))
+        + [(gain, gain_out), (hidden, hidden_out), (state.at[0], state_out), (weight.at[0], weight_out)],
+        sems,
+    )
+    for copy in copies[: len(held)]:
+        copy.wait()
+    layers, depth = hv.shape[:2]
+    for layer in range(layers):
+        taps = [ref[layer].astype(f32) for ref in (tv, tw, tr)]
+        out[layer, 0:chunks] = pack(taps[0][depth : depth + 1])
+        out[layer, chunks : 2 * chunks] = jnp.concatenate(
+            [pack(taps[1][depth : depth + 1]), pack(taps[2][depth : depth + 1])], axis=0
+        )
+        out[layer, 2 * chunks : 3 * chunks] = interleave(
+            scratch, column(direct[layer : layer + 1, :], heads)
+        )
+        out[layer, 3 * chunks : 4 * chunks] = pack(norm[layer : layer + 1, :])
+        at = 4 * chunks
+        out[layer, at : at + heads] = column(bias[layer : layer + 1, :], heads)
+        at += heads
+        out[layer, at : at + heads] = -jnp.exp(column(rate[layer : layer + 1, :], heads))
+        at += heads
+        for s in range(seqs):
+            position = lengths_ref[s] - 1
+            sums = []
+            for ref, tap in zip((hv, hw, hr), taps):
+                total = None
+                for k in range(depth):
+                    term = ref[layer, k].astype(f32)[s : s + 1] * tap[k : k + 1]
+                    term = jnp.where(depth - position <= k, term, 0.0)
+                    total = term if total is None else total + term
+                sums.append(pack(total))
+            out[layer, at : at + chunks] = sums[0]
+            at += chunks
+            out[layer, at : at + chunks] = jnp.concatenate(sums[1:], axis=0)
+            at += chunks
+            logs = pos[layer]
+            here = jnp.sum(jnp.where(lane_iota(logs.shape) == position, logs, 0.0), axis=1, keepdims=True)
+            out[layer, at : at + heads] = jnp.where(
+                position > 0, jnp.broadcast_to(here, (heads, LANES)), -1e30
+            )
+            at += heads
+    for copy in copies[len(held) : -1]:
+        copy.wait()
+    split_state(state_out, split_out)
+    copies[-1].wait()
+
+
+def two_terms(x):
+    high = x.astype(bf16)
+    return high, (x - high.astype(f32)).astype(bf16)
+
+
+def split_state(held, out):
+    seqs, heads, depth, _ = held.shape
+    for s in range(seqs):
+        for h in range(heads):
+            high, rest = two_terms(held[s, h])
+            at = (s * heads + h) * depth
+            out[at : at + depth, 0:LANES] = high
+            out[at : at + depth, LANES : 2 * LANES] = rest
+
+
+def fetch_state_kernel(layer, *refs):
+    state, weight, held, weight_out, split_out, sems = refs[1:]
+    copies = start_all(halves(state.at[layer], held) + halves(weight.at[layer], weight_out), sems)
+    copies[0].wait()
+    copies[1].wait()
+    split_state(held, split_out)
+    copies[2].wait()
+    copies[3].wait()
+
+
+def fetch_kernel(plan, *refs):
+    count = len(plan)
+    sources, targets, sems = refs[1 : 1 + count], refs[1 + count : 1 + 2 * count], refs[-1]
+    pairs = []
+    for block, source, target in zip(plan, sources, targets):
+        pairs += halves(source if block is None else source.at[block], target)
+    for copy in start_all(pairs, sems):
+        copy.wait()
+
+
+def update_kernel(dims, layer, *refs):
+    seqs, chunks, shared, heads, rows, fan = dims
+    lead_ref, acts, decays, held = refs[:4]
+    out, made, sems = refs[-3:]
+    per_group = heads // shared
+    half = LANES // 2
+    lead = lead_ref[...]
+    count = lead.shape[0]
+    high, rest = two_terms(lead)
+    last = lead - high.astype(f32) - rest.astype(f32)
+    terms = [high.astype(f32)] * 3 + [rest.astype(f32)] * 2 + [last]
+    blank = jnp.zeros((LANES - 6 * count, LANES), f32)
+    left = jnp.transpose(jnp.concatenate(terms + [blank], axis=0)).astype(bf16)
+    at_row = lax.broadcasted_iota(jnp.int32, (count, LANES), 0)
+    copies = []
+    for s in range(seqs):
+        for g in range(shared):
+            write = acts[s, g : g + 1, :]
+            high, rest = two_terms(write)
+            last = write - high.astype(f32) - rest.astype(f32)
+            high, rest = high.astype(f32), rest.astype(f32)
+            right = []
+            for i in range(per_group // 2):
+                here = at_row == s * chunks + g * per_group // 2 + i
+                terms = [jnp.where(here, jnp.broadcast_to(t, (count, LANES)), 0.0) for t in (high, rest, last)]
+                order = [terms[0], terms[1], terms[2], terms[0], terms[1], terms[0], blank]
+                right.append(jnp.concatenate(order, axis=0).astype(bf16))
+            added = jnp.dot(left, jnp.concatenate(right, axis=1), preferred_element_type=f32)
+            for i in range(per_group // 2):
+                for j in range(2):
+                    h = g * per_group + 2 * i + j
+                    made[s, h] = (
+                        decays[s, h : h + 1, :] * held[s, h]
+                        + added[j * half : (j + 1) * half, i * LANES : (i + 1) * LANES]
+                    )
+            copy = pltpu.make_async_copy(
+                made.at[s, pl.ds(g * per_group, per_group)],
+                out.at[layer, s, pl.ds(g * per_group, per_group)],
+                sems.at[s * shared + g],
+            )
+            copy.start()
+            copies.append(copy)
+    for copy in copies:
+        copy.wait()
+
+
+def silu(x):
+    return x / (1.0 + jnp.exp(-x))
+
+
+def mix_kernel(dims, layer, *refs):
+    seqs, chunks, shared, heads, rows, fan = dims
+    parts, table, split = refs[:fan], refs[fan], refs[fan + 1]
+    gated_ref, rows_ref, lead_ref, acts, decays, pairs = refs[fan + 2 :]
+    groups = shared
+    per_group = heads // groups
+    span = per_group // 2
+    total = tree_sum([part[...] for part in parts])
+    at_row = lax.broadcasted_iota(jnp.int32, (chunks, LANES), 0)
+    for s in range(seqs):
+        block = total[s * rows : (s + 1) * rows]
+        at = 4 * chunks + 2 * heads + s * (2 * chunks + heads)
+        last = block[2 * chunks + 2 * shared : 2 * chunks + 2 * shared + 1]
+        scale = lax.rsqrt(last[:, LANES // 2 : LANES // 2 + 1] / D + epsilon)
+        share_row = (block[2 * chunks : 2 * chunks + 2 * shared] * scale).astype(bf16).astype(f32)
+        act = silu(
+            share_row * table[layer, chunks : 2 * chunks]
+            + table[layer, at + chunks : at + chunks + 2 * shared]
+        )
+        acts[s] = act
+        sums = jnp.zeros((chunks, LANES), f32)
+        write_rows, read_rows = [], []
+        for g in range(groups):
+            read = act[groups + g : groups + g + 1]
+            here = (at_row >= g * span) & (at_row < (g + 1) * span)
+            high, rest = two_terms(jnp.where(here, jnp.broadcast_to(read, (chunks, LANES)), 0.0))
+            left = jnp.concatenate([high.astype(f32), rest.astype(f32)], axis=0).astype(bf16)
+            size = span * LANES
+            first = (s * groups + g) * size
+            product = lax.dot_general(
+                jnp.concatenate([left, left], axis=1),
+                split[first : first + size, :],
+                (((1,), (1,)), ((), ())),
+                preferred_element_type=f32,
+            )
+            product = product[0:chunks] + product[chunks : 2 * chunks]
+            for i in range(span):
+                sums = jnp.where(at_row == g * span + i, product[:, i * LANES : (i + 1) * LANES], sums)
+            write_rows += [act[g : g + 1]] * span
+            read_rows += [read] * span
+        overlap = jnp.sum(
+            jnp.concatenate(write_rows, axis=0) * jnp.concatenate(read_rows, axis=0), axis=1, keepdims=True
+        )
+        gate = silu(block[0:chunks] * scale)
+        value_row = (block[chunks : 2 * chunks] * scale).astype(bf16).astype(f32)
+        rows_ref[s, 0:chunks] = value_row
+        rows_ref[s, chunks : chunks + 2 * shared] = share_row
+        value_act = silu(value_row * table[layer, 0:chunks] + table[layer, at : at + chunks])
+        raw = column(last * scale, heads) + table[layer, 4 * chunks : 4 * chunks + heads]
+        step = jnp.maximum(raw, 0.0) + jnp.log1p(jnp.exp(-jnp.abs(raw)))
+        decay = jnp.exp(
+            table[layer, 4 * chunks + heads : 4 * chunks + 2 * heads] * step
+            + table[layer, at + 2 * chunks : at + 2 * chunks + heads]
+        )
+        decays[s] = decay
+        lead = interleave(pairs.at[2 * s], step) * value_act
+        lead_ref[s * chunks : (s + 1) * chunks, :] = lead
+        readout = interleave(pairs.at[2 * s + 1], decay) * sums + lead * overlap
+        mixed = (readout + table[layer, 2 * chunks : 3 * chunks] * value_act) * gate
+        power = jnp.broadcast_to(jnp.sum(mixed * mixed, axis=1, keepdims=True), (chunks, LANES))
+        other = jnp.where(
+            lax.rem(at_row, 2) == 0, pltpu.roll(power, chunks - 1, 0), pltpu.roll(power, 1, 0)
+        )
+        mixed = mixed * lax.rsqrt((power + other) / (2 * LANES) + epsilon)
+        gated_ref[s * chunks : (s + 1) * chunks, :] = (
+            mixed * table[layer, 3 * chunks : 4 * chunks]
+        ).astype(bf16)
+
+
+def output_kernel(dims, *refs):
+    seqs, chunks, shared, heads, rows, fan = dims
+    parts, weight = refs[:fan], refs[fan]
+    out, scratch = refs[fan + 2 :]
+    me = lax.axis_index("dp")
+    block = seqs * chunks
+    for mask in range(fan):
+        start = pl.multiple_of(lax.bitwise_xor(me, jnp.int32(mask)) * block, block)
+        scratch[pl.ds(start, block), :] = parts[mask][...].astype(f32)
+    whole = jnp.concatenate(
+        [scratch[pl.ds(c, fan * seqs, stride=chunks), :] for c in range(chunks)], axis=1
+    ).astype(bf16)
+    out[...] = jnp.dot(whole, weight[...], preferred_element_type=f32)
+
+
+def close_kernel(x_ref, *refs):
+    out = refs[-1]
+    out[...] = (x_ref[...].astype(f32) + tree_sum([ref[...] for ref in refs[:-1]])).astype(bf16)
+
+
+def buffer_kernel(dims, layers, *refs):
+    seqs, chunks, shared, heads, rows, fan = dims
+    new_rows = refs[1 : 1 + layers]
+    past = refs[1 + layers : 4 + layers]
+    outs = refs[4 + layers : 7 + layers]
+    held = refs[7 + layers : 10 + layers]
+    built = refs[10 + layers : 13 + layers]
+    sems = refs[-1]
+    for copy in start_all(list(zip(past, held)), sems):
+        copy.wait()
+    spans = ((0, chunks), (chunks, chunks + shared), (chunks + shared, chunks + 2 * shared))
+    for old, new, (low, high) in zip(held, built, spans):
+        depth = old.shape[1]
+        for layer in range(layers):
+            for k in range(depth - 1):
+                new[layer, k] = old[layer, k + 1]
+            new[layer, depth - 1] = jnp.concatenate(
+                [unpack(new_rows[layer][s, low:high]) for s in range(seqs)], axis=0
+            ).astype(bf16)
+    for copy in start_all(list(zip(built, outs)), sems):
+        copy.wait()
+
+
+def full(memory=VMEM):
+    return pl.BlockSpec(memory_space=memory)
+
+
+HBM = pltpu.HBM
+
+
+def place(arrays, memory):
+    return [pltpu.with_memory_space_constraint(array, memory) for array in arrays]
+
+
+def cost(flops, moved):
+    return pl.CostEstimate(flops=flops, bytes_accessed=moved, transcendentals=0)
+
+
+def direct(axis):
+    size = lax.axis_size(axis)
+    return size <= 8 and size & (size - 1) == 0
+
+
+def swap(array, axis, mask):
+    return lax.ppermute(array, axis, [(i, i ^ mask) for i in range(lax.axis_size(axis))])
+
+
+def swaps(array, axis):
+    return [array] + [swap(array, axis, mask) for mask in range(1, lax.axis_size(axis))]
+
+
+def on_device_kernels(
+    hidden,
+    lengths,
+    input_norm_gain,
+    gate_matrix,
+    input_matrix,
+    write_matrix,
+    read_matrix,
+    step_matrix,
+    step_size_bias,
+    log_decay_rate,
+    direct_path_gain,
+    input_filter_taps,
+    write_filter_taps,
+    read_filter_taps,
+    position_log_decay,
+    grouped_norm_gain,
+    output_matrix,
+    recurrent_head_state,
+    history_input_rows,
+    history_write_rows,
+    history_read_rows,
+):
+    layers, seqs, heads = recurrent_head_state.shape[:3]
+    chunks = input_filter_taps.shape[2] // LANES
+    shared = write_filter_taps.shape[2] // LANES
+    rows = -(-(2 * chunks + 2 * shared + 1) // 8) * 8
+    fan = lax.axis_size("dp")
+    dims = (seqs, chunks, shared, heads, rows, fan)
+    count = hidden.shape[0]
+    weights = (
+        gate_matrix,
+        input_matrix,
+        write_matrix,
+        read_matrix,
+        jnp.swapaxes(step_matrix, 1, 2),
+    )
+    past = [
+        jnp.swapaxes(h, 1, 2) for h in (history_input_rows, history_write_rows, history_read_rows)
+    ]
+    state = recurrent_head_state
+    params = pltpu.CompilerParams(vmem_limit_bytes=12 * 1024 * 1024)
+    table_rows = 4 * chunks + 2 * heads + seqs * (2 * chunks + heads)
+    message = pltpu.VMEM((seqs * rows, LANES), f32)
+    pool = pltpu.VMEM((rows * count, LANES), f32)
+
+    def fetch(after, blocks, name):
+        sources = [array for array, _ in blocks]
+        plan = [block for _, block in blocks]
+        return pl.pallas_call(
+            functools.partial(fetch_kernel, plan),
+            out_shape=[
+                pltpu.VMEM(a.shape if block is None else a.shape[1:], a.dtype) for a, block in blocks
+            ],
+            in_specs=[full()] + [full(HBM)] * len(blocks),
+            out_specs=[full()] * len(blocks),
+            scratch_shapes=[pltpu.SemaphoreType.DMA((2 * len(blocks),))],
+            compiler_params=params,
+            cost_estimate=cost(4_000_000, 1_000_000),
+            name=name,
+        )(*place([after], VMEM), *place(sources, HBM))
+
+    def fetch_state(layer, after):
+        return pl.pallas_call(
+            functools.partial(fetch_state_kernel, layer),
+            out_shape=[
+                pltpu.VMEM(state.shape[1:], f32),
+                pltpu.VMEM(output_matrix.shape[1:], bf16),
+                pltpu.VMEM((seqs * heads * state.shape[3], 2 * LANES), bf16),
+            ],
+            in_specs=[full()] + [full(HBM)] * 2,
+            out_specs=[full()] * 3,
+            scratch_shapes=[pltpu.SemaphoreType.DMA((4,))],
+            compiler_params=params,
+            cost_estimate=cost(4_000_000, 1_000_000),
+            name="fetch",
+        )(*place([after], VMEM), *place([state, output_matrix], HBM))
+
+    def mix(layer, parts, tables, split):
+        return pl.pallas_call(
+            functools.partial(mix_kernel, dims, layer),
+            out_shape=[
+                pltpu.VMEM((seqs * chunks, LANES), bf16),
+                pltpu.VMEM((seqs, chunks + 2 * shared, LANES), f32),
+                pltpu.VMEM((seqs * chunks, LANES), f32),
+                pltpu.VMEM((seqs, 2 * shared, LANES), f32),
+                pltpu.VMEM((seqs, heads, LANES), f32),
+            ],
+            in_specs=[full()] * (fan + 2),
+            out_specs=[full()] * 5,
+            scratch_shapes=[pltpu.VMEM((2 * seqs, heads, LANES), f32)],
+            compiler_params=params,
+            name="mix",
+        )(*place(list(parts) + [tables, split], VMEM))
+
+    def update(layer, factors, held, states):
+        given = place([*factors, held], VMEM)
+        if states is not None:
+            given += place([states], HBM)
+        return pl.pallas_call(
+            functools.partial(update_kernel, dims, layer),
+            out_shape=jax.ShapeDtypeStruct(state.shape, f32),
+            in_specs=[full()] * 4 + [full(HBM)] * (len(given) - 4),
+            out_specs=full(HBM),
+            scratch_shapes=[
+                pltpu.VMEM(state.shape[1:], f32),
+                pltpu.SemaphoreType.DMA((seqs * shared,)),
+            ],
+            input_output_aliases={4: 0} if states is not None else {},
+            compiler_params=params,
+            cost_estimate=cost(4_000_000, 1_000_000),
+            name="update",
+        )(*given)
+
+    def output(parts, weight, states):
+        return pl.pallas_call(
+            functools.partial(output_kernel, dims),
+            out_shape=pltpu.VMEM((count, output_matrix.shape[2]), f32),
+            in_specs=[full()] * (fan + 1) + [full(HBM)],
+            out_specs=full(),
+            scratch_shapes=[pltpu.VMEM((fan * seqs * chunks, LANES), f32)],
+            compiler_params=params,
+            name="output",
+        )(*place(list(parts) + [weight], VMEM), *place([states], HBM))
+
+    given = [hidden, input_norm_gain, *weights]
+    made = pl.pallas_call(
+        functools.partial(first_project_kernel, dims, 0),
+        out_shape=[message] * fan,
+        in_specs=[full(HBM) for _ in given],
+        out_specs=[full()] * fan,
+        scratch_shapes=[pltpu.VMEM(hidden.shape, bf16), pltpu.VMEM(input_norm_gain.shape, f32)]
+        + [pltpu.VMEM(w.shape[1:], bf16) for w in weights]
+        + [pool, pltpu.SemaphoreType.DMA((12,))],
+        compiler_params=params,
+        name="project",
+    )(*place(given, HBM))
+    small = past + [
+        input_filter_taps,
+        write_filter_taps,
+        read_filter_taps,
+        step_size_bias,
+        log_decay_rate,
+        direct_path_gain,
+        jnp.swapaxes(position_log_decay, 1, 2),
+        grouped_norm_gain,
+    ]
+    tables, held, weight, gain, stream, split = pl.pallas_call(
+        functools.partial(table_kernel, dims),
+        out_shape=[
+            pltpu.VMEM((layers, table_rows, LANES), f32),
+            pltpu.VMEM(state.shape[1:], f32),
+            pltpu.VMEM(output_matrix.shape[1:], bf16),
+            pltpu.VMEM(input_norm_gain.shape, f32),
+            pltpu.VMEM(hidden.shape, bf16),
+            pltpu.VMEM((seqs * heads * state.shape[3], 2 * LANES), bf16),
+        ],
+        in_specs=[full(pltpu.SMEM), full()] + [full(HBM)] * (len(small) + 4),
+        out_specs=[full()] * 6,
+        scratch_shapes=[pltpu.VMEM(a.shape, a.dtype) for a in small]
+        + [pltpu.VMEM((heads, LANES), f32), pltpu.SemaphoreType.DMA((len(small) + 4,))],
+        compiler_params=params,
+        cost_estimate=cost(4_000_000, 1_000_000),
+        name="tables",
+    )(
+        lengths,
+        *place([made[0]], VMEM),
+        *place(small + [state, output_matrix, input_norm_gain, hidden], HBM),
+    )
+    states = None
+    new_rows = []
+    for layer in range(layers):
+        parts = [made[0]] + [swap(made[mask], "dp", mask) for mask in range(1, fan)]
+        if layer > 0:
+            held, weight, split = fetch_state(layer, made[0])
+        gated, row_values, *factors = mix(layer, parts, tables, split)
+        new_rows.append(row_values)
+        parts = swaps(gated, "dp")
+        states = update(layer, factors, held, states)
+        own = output(parts, weight, states)
+        partial = swaps(own, "tp")
+        if layer + 1 < layers:
+            ahead = fetch(own, [(w, layer + 1) for w in weights], "fetch")
+            stream, *made = pl.pallas_call(
+                functools.partial(next_project_kernel, dims, layer + 1),
+                out_shape=[pltpu.VMEM(hidden.shape, bf16)] + [message] * fan,
+                in_specs=[full()] * (2 + len(partial) + len(weights)),
+                out_specs=[full()] * (1 + fan),
+                scratch_shapes=[pool],
+                compiler_params=params,
+                name="project",
+            )(*place([stream, *partial, gain, *ahead], VMEM))
+    buffers = pl.pallas_call(
+        functools.partial(buffer_kernel, dims, layers),
+        out_shape=[jax.ShapeDtypeStruct(h.shape, bf16) for h in past],
+        in_specs=[full()] * (1 + layers) + [full(HBM)] * 3,
+        out_specs=[full(HBM)] * 3,
+        scratch_shapes=[pltpu.VMEM(h.shape, bf16) for h in past] * 2 + [pltpu.SemaphoreType.DMA((3,))],
+        compiler_params=params,
+        cost_estimate=cost(4_000_000, 1_000_000),
+        name="buffers",
+    )(*place([own] + new_rows, VMEM), *place(past, HBM))
+    buffers = [jnp.swapaxes(b, 1, 2) for b in buffers]
+    stream = pl.pallas_call(
+        close_kernel,
+        out_shape=jax.ShapeDtypeStruct(hidden.shape, bf16),
+        in_specs=[full()] * (1 + len(partial)),
+        out_specs=full(),
+        compiler_params=params,
+        name="close",
+    )(*place([stream, *partial], VMEM))
+    return (stream, states, *buffers)
+
+
+def kernels_fit(state, taps, write_taps, hidden, output_matrix, step_matrix):
+    layers, seqs, heads, head_dim, state_dim = state.shape
+    shared = write_taps.shape[2] // LANES
+    chunks = taps.shape[2] // LANES
+    return (
+        direct("dp")
+        and direct("tp")
+        and state_dim == LANES
+        and head_dim * 2 == LANES
+        and shared > 0
+        and heads == 4 * shared
+        and chunks == 2 * shared
+        and chunks % 8 == 0
+        and heads % 16 == 0
+        and seqs * chunks <= LANES
+        and seqs * chunks % 16 == 0
+        and hidden.shape[0] == seqs * lax.axis_size("dp")
+        and hidden.shape[0] % 8 == 0
+        and hidden.shape[1] % LANES == 0
+        and output_matrix.shape[2] % LANES == 0
+        and step_matrix.shape[2] <= LANES
+        and heads <= LANES // 2
+    )
 
 
 def convolve(buffer, new_row, weights, tap_valid):
@@ -24,21 +677,6 @@
     return jnp.broadcast_to(grouped, (seq_local, groups_local, per_group, state_dim)).reshape(
         seq_local, groups_local * per_group, state_dim
     )
-
-
-def direct(axis):
-    size = lax.axis_size(axis)
-    return size <= 8 and size & (size - 1) == 0
-
-
-def swap(array, axis, mask):
-    return lax.ppermute(array, axis, [(i, i ^ mask) for i in range(lax.axis_size(axis))])
-
-
-def tree_sum(parts):
-    while len(parts) > 1:
-        parts = [parts[i] + parts[i + 1] for i in range(0, len(parts), 2)]
-    return parts[0]
 
 
 def exchange_rows(rows, axis, count):
@@ -69,7 +707,7 @@
     return tree_sum([rows] + [swap(rows, axis, mask) for mask in range(1, lax.axis_size(axis))])
 
 
-def on_device(
+def on_device_plain(
     hidden,
     lengths,
     input_norm_gain,
@@ -178,6 +816,13 @@
     return (stream, jnp.stack(states), jnp.stack(values), jnp.stack(writes), jnp.stack(reads))
 
 
+def on_device(*args):
+    hidden, taps, write_taps = args[0], args[11], args[12]
+    if kernels_fit(args[17], taps, write_taps, hidden, args[16], args[7]):
+        return on_device_kernels(*args)
+    return on_device_plain(*args)
+
+
 def solution(mesh):
     placed = (
         P("grp", "dp"),

time: 62.2 us -> 40.7 us (0.65)
  matrix products: 17.7 us -> 0 us
  Pallas kernels: 0 us -> 15.1 us
  other arithmetic: 9.12 us -> 0 us
  waiting for transfers between devices: 12.3 us -> 6.92 us
  local copies, waits for them, and re-layouts: 2.86 us -> 0.01 us
    dot_general x16 -> x0, matrix products: 17.7 us -> none  [the longest x2 6.15 us: on_device(): jnp.einsum('shpn,shn->shp', updated, read_heads, precision=lax.Precision....]
    pallas_call x0 -> x13, Pallas kernels: none -> 15.1 us  [the longest x2 2.54 us: update(): pl.pallas_call(functools.partial(update_kernel, dims, layer), out_shape=j...]
    ppermute x18, waiting for transfers between devices: 12.3 us -> 6.92 us  [swap(): lax.ppermute(array, axis, [(i, i ^ mask) for i in range(lax.axis_size(axi...]
    another operation x12 -> x0, other arithmetic: 3.67 us -> none  [the longest x1 1.52 us: on_device(): jnp.stack(states)]
    add x3 -> x0, other arithmetic: 2.09 us -> none  [the longest x1 2.02 us: on_device(): current_decay[:, :, None, None] * recurrent_head_state[layer_index]]
    reduce_sum x6 -> x0, other arithmetic: 1.56 us -> none  [the longest x2 1.06 us: on_device(): squares = jnp.sum(stream_float * stream_float, axis=1)]
    slice x15 -> x0, local copies, waits for them, and re-layouts: 0.88 us -> none  [the longest x1 0.77 us: on_device(): normed = (stream_float * input_norm_gain[layer_index]).astype(jnp.bfloat16)]
    reshape x10 -> x0, local copies, waits for them, and re-layouts: 0.7 us -> none  [the longest x4 0.34 us: on_device(): grouped = mixed_heads.reshape(seq_local, groups_local, per_group * head_dim)]
  transfers between devices with their start and end apart: 18 -> 18, of which waited for: 11 -> 7; matrix products, arithmetic and copies ran while one was open for 10% -> 0% of each run, Pallas kernels for 0% -> 24%
where the time goes in v2:
time: 40.7 us; the launch traced here: 40.5 us
  starting transfers between devices  17.7 us (43%)
  Pallas kernels  15.1 us (37%)
  waiting for transfers between devices  6.92 us (17%)
  between operations  0.78 us (2%)
    ppermute x18, starting transfers between devices, swap(): lax.ppermute(array, axis, [(i, i ^ mask) for i in range(lax.axis_size(axi...  17.7 us
    ppermute x18, waiting for transfers between devices, swap(): lax.ppermute(array, axis, [(i, i ^ mask) for i in range(lax.axis_size(axi...  6.92 us
    pallas_call x2, Pallas kernels, update(): pl.pallas_call(functools.partial(update_kernel, dims, layer), out_shape=j...  2.54 us
    pallas_call x1, Pallas kernels, on_device_kernels(): pl.pallas_call(functools.partial(first_project_kernel, dims, 0), out_shap...  2.51 us
    pallas_call x1, Pallas kernels, on_device_kernels(): pl.pallas_call(functools.partial(table_kernel, dims), out_shape=[pltpu.VM...  2.38 us
    pallas_call x1, Pallas kernels, fetch(): pl.pallas_call(functools.partial(fetch_kernel, plan), out_shape=[pltpu.VM...  1.91 us
    pallas_call x1, Pallas kernels, fetch_state(): pl.pallas_call(functools.partial(fetch_state_kernel, layer), out_shape=[p...  1.55 us
    pallas_call x1, Pallas kernels, on_device_kernels(): pl.pallas_call(functools.partial(buffer_kernel, dims, layers), out_shape=...  1.39 us
  transfers between devices with their start and end apart: 18, of which 7 were waited for; matrix products, arithmetic and copies ran while one was open for 0% of the time, Pallas kernels for 24%

profile of v2, /device:TPU:0, one launch (start us, length us, event | category | flops | bytes accessed | tf_op | source)
XLA Modules:
  0.0 40.5 jit_solution(15110457904368768865)
XLA Ops:
  0.6 0.0 copy-start
  0.6 2.5 %project.2 = (f32[64,128]{1,0:T(8,128)S(1)}, f32[64,128]{1,0:T(8,128)S(1)}, f32[64,128]{1,0:T(8,128)S(1)}, f32[64,128]{1,0:T(8,128)S(1)}) custom-call(bf16[8,512]{1,0:T(8,128)(2,1)} %refs_16_.1, f32[2,512]{1,0:T(2,128)} %refs_15_.1, bf16[2,512,1024]{2,1,0:T(8,128)(2,1)} %refs_1_.4, bf16[2,512,1024]{2,1,0:T(8,128)(2,1)} %refs_2_.4, ...), custom_call_target="tpu_custom_call" | custom-call | tf_op jit(solution)/shard_map/project/pallas_call | solution.py:552
  3.2 0.6 %collective-permute-start = (f32[64,128]{1,0:T(8,128)S(1)}, f32[64,128]{1,0:T(8,128)S(1)}, u32[]{:S(2)}, u32[]{:S(2)}) collective-permute-start(f32[64,128]{1,0:T(8,128)S(1)} %get-tuple-element.43), channel_id=1, source_target_pairs={{0,1},{1,0},{2,3},{3,2},{4,5},{5,4},{6,7},{7,6},{8,9},{9,8},{10,11... | collective-permute-start | bytes 98312 | tf_op jit(solution)/shard_map/ppermute | solution.py:419
  3.7 2.6 %collective-permute-start.1 = (f32[64,128]{1,0:T(8,128)S(1)}, f32[64,128]{1,0:T(8,128)S(1)}, u32[]{:S(2)}, u32[]{:S(2)}) collective-permute-start(f32[64,128]{1,0:T(8,128)S(1)} %get-tuple-element.44), channel_id=1, source_target_pairs={{0,2},{1,3},{2,0},{3,1},{4,6},{5,7},{6,4},{7,5},{8,10},{9,11},{10,... | collective-permute-start | bytes 98312 | tf_op jit(solution)/shard_map/ppermute | solution.py:419
  6.3 0.0 collective-permute-start.2
  6.3 0.0 copy-done
  6.3 2.4 %tables.1 = (f32[2,128,128]{2,1,0:T(8,128)S(1)}, f32[2,16,64,128]{3,2,1,0:T(8,128)S(1)}, bf16[1024,512]{1,0:T(8,128)(2,1)S(1)}, f32[2,512]{1,0:T(2,128)S(1)}, bf...) custom-call(s32[2]{0:T(128)S(1)} %copy-done, f32[64,128]{1,0:T(8,128)S(1)} %get-tuple-element.41.refs_1_.refs_0_, ...), custom_call_target="tpu_custom_call" | custom-call | flops 4000000 | bytes 1000000 | tf_op jit(solution)/shard_map/tables/pallas_call | solution.py:573
  8.7 0.0 collective-permute-done.refs_1_
  8.7 0.0 collective-permute-done.1.refs_2_
  8.8 0.9 %collective-permute-done.2.refs_3_ = f32[64,128]{1,0:T(8,128)S(1)} collective-permute-done((f32[64,128]{1,0:T(8,128)S(1)}, f32[64,128]{1,0:T(8,128)S(1)}, u32[]{:S(2)}, u32[]{:S(2)}) %collective-permute-start.2) | collective-permute-done | bytes 32800 | tf_op jit(solution)/shard_map/ppermute | solution.py:419
  9.7 0.5 %mix.2 = (bf16[16,128]{1,0:T(8,128)(2,1)S(1)}, f32[2,16,128]{2,1,0:T(8,128)S(1)}, f32[16,128]{1,0:T(8,128)S(1)}, f32[2,8,128]{2,1,0:T(8,128)S(1)}, f32[2,16,128]{2,1,0:T(8,128)S(1)}) custom-call(f32[64,128]{1,0:T(8,128)S(1)} %get-tuple-element.41.refs_1_.refs_0_, f32[64,128]{1,0:T(8,128)S(1)} %collective-permute-done.refs_1_, ...), custom_call_target="tpu_custom_call" | custom-call | tf_op jit(solution)/shard_map/mix/pallas_call | solution.py:505
  10.2 0.9 %collective-permute-start.5 = (bf16[16,128]{1,0:T(8,128)(2,1)S(1)}, bf16[16,128]{1,0:T(8,128)(2,1)S(1)}, u32[]{:S(2)}, u32[]{:S(2)}) collective-permute-start(bf16[16,128]{1,0:T(8,128)(2,1)S(1)} %get-tuple-element.48.refs_0_), channel_id=1, source_target_pairs={{0,3},{1,2},{2,1},{3,0},{4,7},{5,6},{6,5},{7,4},{8,11},{9,10},{10,... | collective-permute-start | bytes 12296 | tf_op jit(solution)/shard_map/ppermute | solution.py:419
  11.0 1.0 %collective-permute-start.4 = (bf16[16,128]{1,0:T(8,128)(2,1)S(1)}, bf16[16,128]{1,0:T(8,128)(2,1)S(1)}, u32[]{:S(2)}, u32[]{:S(2)}) collective-permute-start(bf16[16,128]{1,0:T(8,128)(2,1)S(1)} %get-tuple-element.48.refs_0_), channel_id=1, source_target_pairs={{0,2},{1,3},{2,0},{3,1},{4,6},{5,7},{6,4},{7,5},{8,10},{9,11},{10,... | collective-permute-start | bytes 12296 | tf_op jit(solution)/shard_map/ppermute | solution.py:419
  12.0 0.1 collective-permute-start.3
  12.1 1.3 %update.2.refs_5_.refs_4_ = f32[2,2,16,64,128]{4,3,2,1,0:T(8,128)} custom-call(f32[16,128]{1,0:T(8,128)S(1)} %get-tuple-element.50.refs_0_, f32[2,8,128]{2,1,0:T(8,128)S(1)} %get-tuple-element.51.refs_1_, f32[2,16,128]{2,1,0:T(8,128)S(1)} %get-tuple-element.52.refs_2_, f32[2,16,64,128]{3,2,1,0:T(8,128)S(1)} %get-tuple-element.53.refs_3_), custom_call_target="tpu_custom_call" | custom-call | flops 4000000 | bytes 1000000 | tf_op jit(solution)/shard_map/update/pallas_call | solution.py:525
  13.4 0.0 collective-permute-done.5.refs_3_
  13.4 1.3 %collective-permute-done.4.refs_2_ = bf16[16,128]{1,0:T(8,128)(2,1)S(1)} collective-permute-done((bf16[16,128]{1,0:T(8,128)(2,1)S(1)}, bf16[16,128]{1,0:T(8,128)(2,1)S(1)}, u32[]{:S(2)}, u32[]{:S(2)}) %collective-permute-start.4) | collective-permute-done | bytes 4128 | tf_op jit(solution)/shard_map/ppermute | solution.py:419
  14.6 0.0 collective-permute-done.3.refs_1_
  14.7 0.2 output.2.refs_0_.refs_1_
  14.9 3.6 %collective-permute-start.8 = (f32[8,512]{1,0:T(8,128)S(1)}, f32[8,512]{1,0:T(8,128)S(1)}, u32[]{:S(2)}, u32[]{:S(2)}) collective-permute-start(f32[8,512]{1,0:T(8,128)S(1)} %output.2.refs_0_.refs_1_), channel_id=1, source_target_pairs={{0,12},{4,8},{8,4},{12,0},{1,13},{5,9},{9,5},{13,1},{2,14},{6,10},... | collective-permute-start | bytes 49160 | tf_op jit(solution)/shard_map/ppermute | solution.py:419
  18.5 0.0 collective-permute-start.7
  18.5 0.8 %collective-permute-start.6 = (f32[8,512]{1,0:T(8,128)S(1)}, f32[8,512]{1,0:T(8,128)S(1)}, u32[]{:S(2)}, u32[]{:S(2)}) collective-permute-start(f32[8,512]{1,0:T(8,128)S(1)} %output.2.refs_0_.refs_1_), channel_id=1, source_target_pairs={{0,4},{4,0},{8,12},{12,8},{1,5},{5,1},{9,13},{13,9},{2,6},{6,2},{1... | collective-permute-start | bytes 49160 | tf_op jit(solution)/shard_map/ppermute | solution.py:419
  19.3 1.9 %fetch.2 = (bf16[512,1024]{1,0:T(8,128)(2,1)S(1)}, bf16[512,1024]{1,0:T(8,128)(2,1)S(1)}, bf16[512,512]{1,0:T(8,128)(2,1)S(1)}, bf16[512,512]{1,0:T(8,128)(2,1)S(1)}, bf16[64,512]{1,0:T(8,128)(2,1)S(1)}) custom-call(f32[8,512]{1,0:T(8,128)S(1)} %output.2.refs_0_.refs_1_, bf16[2,512,1024]{2,1,0:T(8,128)(2,1)} %refs_1_.4, bf16[2,512,1024]{2,1,0:T(8,128)(2,1)} %refs_2_.4, ...), custom_call_target="tpu_custom_call" | custom-call | flops 4000000 | bytes 1000000 | tf_op jit(solution)/shard_map/fetch/pallas_call | solution.py:475
  21.2 0.0 collective-permute-done.8.refs_4_
  21.2 1.9 %collective-permute-done.7.refs_3_ = f32[8,512]{1,0:T(8,128)S(1)} collective-permute-done((f32[8,512]{1,0:T(8,128)S(1)}, f32[8,512]{1,0:T(8,128)S(1)}, u32[]{:S(2)}, u32[]{:S(2)}) %collective-permute-start.7) | collective-permute-done | bytes 16416 | tf_op jit(solution)/shard_map/ppermute | solution.py:419
  23.1 0.0 collective-permute-done.6.refs_2_
  23.1 0.6 %project.3 = (bf16[8,512]{1,0:T(8,128)(2,1)S(1)}, f32[64,128]{1,0:T(8,128)S(1)}, f32[64,128]{1,0:T(8,128)S(1)}, f32[64,128]{1,0:T(8,128)S(1)}, f32[64,128]{1,0:T(8,128)S(1)}) custom-call(bf16[8,512]{1,0:T(8,128)(2,1)S(1)} %get-tuple-element.42.refs_0_, f32[8,512]{1,0:T(8,128)S(1)} %output.2.refs_0_.refs_1_, f32[8,512]{1,0:T(8,128)S(1)} %collective-permute-done.6.refs_2_, ...), custom_call_target="tpu_custom_call" | custom-call | tf_op jit(solution)/shard_map/project/pallas_call | solution.py:609
  23.8 0.1 collective-permute-start.9
  23.9 1.0 %collective-permute-start.10 = (f32[64,128]{1,0:T(8,128)S(1)}, f32[64,128]{1,0:T(8,128)S(1)}, u32[]{:S(2)}, u32[]{:S(2)}) collective-permute-start(f32[64,128]{1,0:T(8,128)S(1)} %get-tuple-element.63), channel_id=1, source_target_pairs={{0,2},{1,3},{2,0},{3,1},{4,6},{5,7},{6,4},{7,5},{8,10},{9,11},{10,... | collective-permute-start | bytes 98312 | tf_op jit(solution)/shard_map/ppermute | solution.py:419
  24.9 0.8 %collective-permute-start.11 = (f32[64,128]{1,0:T(8,128)S(1)}, f32[64,128]{1,0:T(8,128)S(1)}, u32[]{:S(2)}, u32[]{:S(2)}) collective-permute-start(f32[64,128]{1,0:T(8,128)S(1)} %get-tuple-element.64), channel_id=1, source_target_pairs={{0,3},{1,2},{2,1},{3,0},{4,7},{5,6},{6,5},{7,4},{8,11},{9,10},{10,... | collective-permute-start | bytes 98312 | tf_op jit(solution)/shard_map/ppermute | solution.py:419
  25.7 1.5 %fetch.3 = (f32[2,16,64,128]{3,2,1,0:T(8,128)S(1)}, bf16[1024,512]{1,0:T(8,128)(2,1)S(1)}, bf16[2048,256]{1,0:T(8,128)(2,1)S(1)}) custom-call(f32[64,128]{1,0:T(8,128)S(1)} %get-tuple-element.61.refs_0_, f32[2,2,16,64,128]{4,3,2,1,0:T(8,128)} %refs_1_.5, bf16[2,1024,512]{2,1,0:T(8,128)(2,1)} %refs_2_.5), custom_call_target="tpu_custom_call" | custom-call | flops 4000000 | bytes 1000000 | tf_op jit(solution)/shard_map/fetch/pallas_call | solution.py:489
  27.3 0.0 collective-permute-done.9.refs_1_
  27.3 0.6 %collective-permute-done.10.refs_2_ = f32[64,128]{1,0:T(8,128)S(1)} collective-permute-done((f32[64,128]{1,0:T(8,128)S(1)}, f32[64,128]{1,0:T(8,128)S(1)}, u32[]{:S(2)}, u32[]{:S(2)}) %collective-permute-start.10) | collective-permute-done | bytes 32800 | tf_op jit(solution)/shard_map/ppermute | solution.py:419
  27.9 0.4 %collective-permute-done.11.refs_3_ = f32[64,128]{1,0:T(8,128)S(1)} collective-permute-done((f32[64,128]{1,0:T(8,128)S(1)}, f32[64,128]{1,0:T(8,128)S(1)}, u32[]{:S(2)}, u32[]{:S(2)}) %collective-permute-start.11) | collective-permute-done | bytes 32800 | tf_op jit(solution)/shard_map/ppermute | solution.py:419
  28.3 0.5 %mix.3 = (bf16[16,128]{1,0:T(8,128)(2,1)S(1)}, f32[2,16,128]{2,1,0:T(8,128)S(1)}, f32[16,128]{1,0:T(8,128)S(1)}, f32[2,8,128]{2,1,0:T(8,128)S(1)}, f32[2,16,128]{2,1,0:T(8,128)S(1)}) custom-call(f32[64,128]{1,0:T(8,128)S(1)} %get-tuple-element.61.refs_0_, f32[64,128]{1,0:T(8,128)S(1)} %collective-permute-done.9.refs_1_, ...), custom_call_target="tpu_custom_call" | custom-call | tf_op jit(solution)/shard_map/mix/pallas_call | solution.py:505
  28.8 0.8 %collective-permute-start.14 = (bf16[16,128]{1,0:T(8,128)(2,1)S(1)}, bf16[16,128]{1,0:T(8,128)(2,1)S(1)}, u32[]{:S(2)}, u32[]{:S(2)}) collective-permute-start(bf16[16,128]{1,0:T(8,128)(2,1)S(1)} %get-tuple-element.66.refs_0_), channel_id=1, source_target_pairs={{0,3},{1,2},{2,1},{3,0},{4,7},{5,6},{6,5},{7,4},{8,11},{9,10},{10,... | collective-permute-start | bytes 12296 | tf_op jit(solution)/shard_map/ppermute | solution.py:419
  29.6 1.0 %collective-permute-start.13 = (bf16[16,128]{1,0:T(8,128)(2,1)S(1)}, bf16[16,128]{1,0:T(8,128)(2,1)S(1)}, u32[]{:S(2)}, u32[]{:S(2)}) collective-permute-start(bf16[16,128]{1,0:T(8,128)(2,1)S(1)} %get-tuple-element.66.refs_0_), channel_id=1, source_target_pairs={{0,2},{1,3},{2,0},{3,1},{4,6},{5,7},{6,4},{7,5},{8,10},{9,11},{10,... | collective-permute-start | bytes 12296 | tf_op jit(solution)/shard_map/ppermute | solution.py:419
  30.6 0.1 collective-permute-start.12
  30.7 1.3 %update.3.refs_5_ = f32[2,2,16,64,128]{4,3,2,1,0:T(8,128)} custom-call(f32[16,128]{1,0:T(8,128)S(1)} %get-tuple-element.68.refs_0_, f32[2,8,128]{2,1,0:T(8,128)S(1)} %get-tuple-element.69.refs_1_, f32[2,16,128]{2,1,0:T(8,128)S(1)} %get-tuple-element.70.refs_2_, f32[2,16,64,128]{3,2,1,0:T(8,128)S(1)} %get-tuple-element.71.refs_3_, ...), custom_call_target="tpu_custom_call", output_to_operand_aliasing={{}: (4, {})} | custom-call | flops 4000000 | bytes 1000000 | tf_op jit(solution)/shard_map/update/pallas_call | solution.py:525
  32.0 0.0 collective-permute-done.14.refs_3_
  32.0 1.3 %collective-permute-done.13.refs_2_ = bf16[16,128]{1,0:T(8,128)(2,1)S(1)} collective-permute-done((bf16[16,128]{1,0:T(8,128)(2,1)S(1)}, bf16[16,128]{1,0:T(8,128)(2,1)S(1)}, u32[]{:S(2)}, u32[]{:S(2)}) %collective-permute-start.13) | collective-permute-done | bytes 4128 | tf_op jit(solution)/shard_map/ppermute | solution.py:419
  33.3 0.0 collective-permute-done.12.refs_1_
  33.3 0.2 output.3.refs_0_
  33.5 1.7 %collective-permute-start.17 = (f32[8,512]{1,0:T(8,128)S(1)}, f32[8,512]{1,0:T(8,128)S(1)}, u32[]{:S(2)}, u32[]{:S(2)}) collective-permute-start(f32[8,512]{1,0:T(8,128)S(1)} %output.3.refs_0_), channel_id=1, source_target_pairs={{0,12},{4,8},{8,4},{12,0},{1,13},{5,9},{9,5},{13,1},{2,14},{6,10},... | collective-permute-start | bytes 49160 | tf_op jit(solution)/shard_map/ppermute | solution.py:419
  35.2 0.4 collective-permute-start.16
  35.6 2.3 %collective-permute-start.15 = (f32[8,512]{1,0:T(8,128)S(1)}, f32[8,512]{1,0:T(8,128)S(1)}, u32[]{:S(2)}, u32[]{:S(2)}) collective-permute-start(f32[8,512]{1,0:T(8,128)S(1)} %output.3.refs_0_), channel_id=1, source_target_pairs={{0,4},{4,0},{8,12},{12,8},{1,5},{5,1},{9,13},{13,9},{2,6},{6,2},{1... | collective-permute-start | bytes 49160 | tf_op jit(solution)/shard_map/ppermute | solution.py:419
  37.9 1.4 %buffers.1 = (bf16[2,3,2,1024]{3,2,1,0:T(2,128)(2,1)}, bf16[2,3,2,512]{3,2,1,0:T(2,128)(2,1)}, bf16[2,3,2,512]{3,2,1,0:T(2,128)(2,1)}) custom-call(f32[8,512]{1,0:T(8,128)S(1)} %output.3.refs_0_, f32[2,16,128]{2,1,0:T(8,128)S(1)} %get-tuple-element.72.refs_1_, f32[2,16,128]{2,1,0:T(8,128)S(1)} %get-tuple-element.73.refs_2_, ...), custom_call_target="tpu_custom_call" | custom-call | flops 4000000 | bytes 1000000 | tf_op jit(solution)/shard_map/buffers/pallas_call | solution.py:618
  39.3 0.0 collective-permute-done.17.refs_3_
  39.3 0.5 %collective-permute-done.16.refs_2_ = f32[8,512]{1,0:T(8,128)S(1)} collective-permute-done((f32[8,512]{1,0:T(8,128)S(1)}, f32[8,512]{1,0:T(8,128)S(1)}, u32[]{:S(2)}, u32[]{:S(2)}) %collective-permute-start.16) | collective-permute-done | bytes 16416 | tf_op jit(solution)/shard_map/ppermute | solution.py:419
  39.8 0.0 collective-permute-done.15.refs_1_
  39.8 0.6 %close.1 = bf16[8,512]{1,0:T(8,128)(2,1)} custom-call(bf16[8,512]{1,0:T(8,128)(2,1)S(1)} %get-tuple-element.60.x_ref, f32[8,512]{1,0:T(8,128)S(1)} %output.3.refs_0_, f32[8,512]{1,0:T(8,128)S(1)} %collective-permute-done.15.refs_1_, f32[8,512]{1,0:T(8,128)S(1)} %collective-permute-done.16.refs_2_, f32[8,512]{1,0:T(8,128)S(1)} %collective-permute-done.17.refs_3_), custom_call_target="tpu_custom_call" | custom-call | tf_op jit(solution)/shard_map/close/pallas_call | solution.py:629
Async XLA Ops:
  0.6 5.7 %copy-start = (s32[2]{0:T(128)S(1)}, s32[2]{0:T(128)}, u32[]{:S(2)}) copy-start(s32[2]{0:T(128)} %refs_0_.3) | copy-start | bytes 28
  3.2 5.6 %collective-permute-start = (f32[64,128]{1,0:T(8,128)S(1)}, f32[64,128]{1,0:T(8,128)S(1)}, u32[]{:S(2)}, u32[]{:S(2)}) collective-permute-start(f32[64,128]{1,0:T(8,128)S(1)} %get-tuple-element.43), channel_id=1, source_target_pairs={{0,1},{1,0},{2,3},{3,2},{4,5},{5,4},{6,7},{7,6},{8,9},{9,8},{10,11... | collective-permute-start | bytes 98312 | tf_op jit(solution)/shard_map/ppermute | solution.py:419
  3.7 5.0 %collective-permute-start.1 = (f32[64,128]{1,0:T(8,128)S(1)}, f32[64,128]{1,0:T(8,128)S(1)}, u32[]{:S(2)}, u32[]{:S(2)}) collective-permute-start(f32[64,128]{1,0:T(8,128)S(1)} %get-tuple-element.44), channel_id=1, source_target_pairs={{0,2},{1,3},{2,0},{3,1},{4,6},{5,7},{6,4},{7,5},{8,10},{9,11},{10,... | collective-permute-start | bytes 98312 | tf_op jit(solution)/shard_map/ppermute | solution.py:419
  6.3 3.4 %collective-permute-start.2 = (f32[64,128]{1,0:T(8,128)S(1)}, f32[64,128]{1,0:T(8,128)S(1)}, u32[]{:S(2)}, u32[]{:S(2)}) collective-permute-start(f32[64,128]{1,0:T(8,128)S(1)} %get-tuple-element.45), channel_id=1, source_target_pairs={{0,3},{1,2},{2,1},{3,0},{4,7},{5,6},{6,5},{7,4},{8,11},{9,10},{10,... | collective-permute-start | bytes 98312 | tf_op jit(solution)/shard_map/ppermute | solution.py:419
  10.2 3.2 %collective-permute-start.5 = (bf16[16,128]{1,0:T(8,128)(2,1)S(1)}, bf16[16,128]{1,0:T(8,128)(2,1)S(1)}, u32[]{:S(2)}, u32[]{:S(2)}) collective-permute-start(bf16[16,128]{1,0:T(8,128)(2,1)S(1)} %get-tuple-element.48.refs_0_), channel_id=1, source_target_pairs={{0,3},{1,2},{2,1},{3,0},{4,7},{5,6},{6,5},{7,4},{8,11},{9,10},{10,... | collective-permute-start | bytes 12296 | tf_op jit(solution)/shard_map/ppermute | solution.py:419
  11.0 3.6 %collective-permute-start.4 = (bf16[16,128]{1,0:T(8,128)(2,1)S(1)}, bf16[16,128]{1,0:T(8,128)(2,1)S(1)}, u32[]{:S(2)}, u32[]{:S(2)}) collective-permute-start(bf16[16,128]{1,0:T(8,128)(2,1)S(1)} %get-tuple-element.48.refs_0_), channel_id=1, source_target_pairs={{0,2},{1,3},{2,0},{3,1},{4,6},{5,7},{6,4},{7,5},{8,10},{9,11},{10,... | collective-permute-start | bytes 12296 | tf_op jit(solution)/shard_map/ppermute | solution.py:419
  12.0 2.6 %collective-permute-start.3 = (bf16[16,128]{1,0:T(8,128)(2,1)S(1)}, bf16[16,128]{1,0:T(8,128)(2,1)S(1)}, u32[]{:S(2)}, u32[]{:S(2)}) collective-permute-start(bf16[16,128]{1,0:T(8,128)(2,1)S(1)} %get-tuple-element.48.refs_0_), channel_id=1, source_target_pairs={{0,1},{1,0},{2,3},{3,2},{4,5},{5,4},{6,7},{7,6},{8,9},{9,8},{10,11... | collective-permute-start | bytes 12296 | tf_op jit(solution)/shard_map/ppermute | solution.py:419
  14.9 6.3 %collective-permute-start.8 = (f32[8,512]{1,0:T(8,128)S(1)}, f32[8,512]{1,0:T(8,128)S(1)}, u32[]{:S(2)}, u32[]{:S(2)}) collective-permute-start(f32[8,512]{1,0:T(8,128)S(1)} %output.2.refs_0_.refs_1_), channel_id=1, source_target_pairs={{0,12},{4,8},{8,4},{12,0},{1,13},{5,9},{9,5},{13,1},{2,14},{6,10},... | collective-permute-start | bytes 49160 | tf_op jit(solution)/shard_map/ppermute | solution.py:419
  18.5 4.6 %collective-permute-start.7 = (f32[8,512]{1,0:T(8,128)S(1)}, f32[8,512]{1,0:T(8,128)S(1)}, u32[]{:S(2)}, u32[]{:S(2)}) collective-permute-start(f32[8,512]{1,0:T(8,128)S(1)} %output.2.refs_0_.refs_1_), channel_id=1, source_target_pairs={{0,8},{4,12},{8,0},{12,4},{1,9},{5,13},{9,1},{13,5},{2,10},{6,14},... | collective-permute-start | bytes 49160 | tf_op jit(solution)/shard_map/ppermute | solution.py:419
  18.5 4.6 %collective-permute-start.6 = (f32[8,512]{1,0:T(8,128)S(1)}, f32[8,512]{1,0:T(8,128)S(1)}, u32[]{:S(2)}, u32[]{:S(2)}) collective-permute-start(f32[8,512]{1,0:T(8,128)S(1)} %output.2.refs_0_.refs_1_), channel_id=1, source_target_pairs={{0,4},{4,0},{8,12},{12,8},{1,5},{5,1},{9,13},{13,9},{2,6},{6,2},{1... | collective-permute-start | bytes 49160 | tf_op jit(solution)/shard_map/ppermute | solution.py:419
  23.8 3.5 %collective-permute-start.9 = (f32[64,128]{1,0:T(8,128)S(1)}, f32[64,128]{1,0:T(8,128)S(1)}, u32[]{:S(2)}, u32[]{:S(2)}) collective-permute-start(f32[64,128]{1,0:T(8,128)S(1)} %get-tuple-element.62), channel_id=1, source_target_pairs={{0,1},{1,0},{2,3},{3,2},{4,5},{5,4},{6,7},{7,6},{8,9},{9,8},{10,11... | collective-permute-start | bytes 98312 | tf_op jit(solution)/shard_map/ppermute | solution.py:419
  23.9 4.0 %collective-permute-start.10 = (f32[64,128]{1,0:T(8,128)S(1)}, f32[64,128]{1,0:T(8,128)S(1)}, u32[]{:S(2)}, u32[]{:S(2)}) collective-permute-start(f32[64,128]{1,0:T(8,128)S(1)} %get-tuple-element.63), channel_id=1, source_target_pairs={{0,2},{1,3},{2,0},{3,1},{4,6},{5,7},{6,4},{7,5},{8,10},{9,11},{10,... | collective-permute-start | bytes 98312 | tf_op jit(solution)/shard_map/ppermute | solution.py:419
  24.9 3.4 %collective-permute-start.11 = (f32[64,128]{1,0:T(8,128)S(1)}, f32[64,128]{1,0:T(8,128)S(1)}, u32[]{:S(2)}, u32[]{:S(2)}) collective-permute-start(f32[64,128]{1,0:T(8,128)S(1)} %get-tuple-element.64), channel_id=1, source_target_pairs={{0,3},{1,2},{2,1},{3,0},{4,7},{5,6},{6,5},{7,4},{8,11},{9,10},{10,... | collective-permute-start | bytes 98312 | tf_op jit(solution)/shard_map/ppermute | solution.py:419
  28.8 3.2 %collective-permute-start.14 = (bf16[16,128]{1,0:T(8,128)(2,1)S(1)}, bf16[16,128]{1,0:T(8,128)(2,1)S(1)}, u32[]{:S(2)}, u32[]{:S(2)}) collective-permute-start(bf16[16,128]{1,0:T(8,128)(2,1)S(1)} %get-tuple-element.66.refs_0_), channel_id=1, source_target_pairs={{0,3},{1,2},{2,1},{3,0},{4,7},{5,6},{6,5},{7,4},{8,11},{9,10},{10,... | collective-permute-start | bytes 12296 | tf_op jit(solution)/shard_map/ppermute | solution.py:419
  29.6 3.6 %collective-permute-start.13 = (bf16[16,128]{1,0:T(8,128)(2,1)S(1)}, bf16[16,128]{1,0:T(8,128)(2,1)S(1)}, u32[]{:S(2)}, u32[]{:S(2)}) collective-permute-start(bf16[16,128]{1,0:T(8,128)(2,1)S(1)} %get-tuple-element.66.refs_0_), channel_id=1, source_target_pairs={{0,2},{1,3},{2,0},{3,1},{4,6},{5,7},{6,4},{7,5},{8,10},{9,11},{10,... | collective-permute-start | bytes 12296 | tf_op jit(solution)/shard_map/ppermute | solution.py:419
  30.6 2.6 %collective-permute-start.12 = (bf16[16,128]{1,0:T(8,128)(2,1)S(1)}, bf16[16,128]{1,0:T(8,128)(2,1)S(1)}, u32[]{:S(2)}, u32[]{:S(2)}) collective-permute-start(bf16[16,128]{1,0:T(8,128)(2,1)S(1)} %get-tuple-element.66.refs_0_), channel_id=1, source_target_pairs={{0,1},{1,0},{2,3},{3,2},{4,5},{5,4},{6,7},{7,6},{8,9},{9,8},{10,11... | collective-permute-start | bytes 12296 | tf_op jit(solution)/shard_map/ppermute | solution.py:419
  33.5 5.8 %collective-permute-start.17 = (f32[8,512]{1,0:T(8,128)S(1)}, f32[8,512]{1,0:T(8,128)S(1)}, u32[]{:S(2)}, u32[]{:S(2)}) collective-permute-start(f32[8,512]{1,0:T(8,128)S(1)} %output.3.refs_0_), channel_id=1, source_target_pairs={{0,12},{4,8},{8,4},{12,0},{1,13},{5,9},{9,5},{13,1},{2,14},{6,10},... | collective-permute-start | bytes 49160 | tf_op jit(solution)/shard_map/ppermute | solution.py:419
  35.2 4.6 %collective-permute-start.16 = (f32[8,512]{1,0:T(8,128)S(1)}, f32[8,512]{1,0:T(8,128)S(1)}, u32[]{:S(2)}, u32[]{:S(2)}) collective-permute-start(f32[8,512]{1,0:T(8,128)S(1)} %output.3.refs_0_), channel_id=1, source_target_pairs={{0,8},{4,12},{8,0},{12,4},{1,9},{5,13},{9,1},{13,5},{2,10},{6,14},... | collective-permute-start | bytes 49160 | tf_op jit(solution)/shard_map/ppermute | solution.py:419
  35.6 4.3 %collective-permute-start.15 = (f32[8,512]{1,0:T(8,128)S(1)}, f32[8,512]{1,0:T(8,128)S(1)}, u32[]{:S(2)}, u32[]{:S(2)}) collective-permute-start(f32[8,512]{1,0:T(8,128)S(1)} %output.3.refs_0_), channel_id=1, source_target_pairs={{0,4},{4,0},{8,12},{12,8},{1,5},{5,1},{9,13},{13,9},{2,6},{6,2},{1... | collective-permute-start | bytes 49160 | tf_op jit(solution)/shard_map/ppermute | solution.py:419

commit v3 on v2

--- a/solution.py
+++ b/solution.py
@@ -7,12 +7,12 @@
 from jax.experimental.pallas import tpu as pltpu
 from jax.sharding import PartitionSpec as P
 
+
 D = 2048
 
 
 epsilon = 1e-06
 LANES = 128
-TABLE = 64
 f32 = jnp.float32
 bf16 = jnp.bfloat16
 VMEM = pltpu.VMEM
@@ -69,7 +69,7 @@
 
 
 def project_rows(dims, x, gain, held, waits, outs, scratch):
-    seqs, chunks, shared, heads, rows, fan = dims
+    seqs, _, _, heads, rows, fan = dims
     squares = jnp.sum(x * x, axis=1, keepdims=True)
     normed = (x * gain).astype(bf16)
     count = x.shape[0]
@@ -142,7 +142,7 @@
 
 
 def table_kernel(dims, *refs):
-    seqs, chunks, shared, heads, rows, fan = dims
+    seqs, chunks, _, heads, _, _ = dims
     lengths_ref = refs[0]
     sources = refs[2:13]
     state, weight, gain, hidden = refs[13:17]
@@ -234,7 +234,7 @@
 
 
 def update_kernel(dims, layer, *refs):
-    seqs, chunks, shared, heads, rows, fan = dims
+    seqs, chunks, shared, heads, _, _ = dims
     lead_ref, acts, decays, held = refs[:4]
     out, made, sems = refs[-3:]
     per_group = heads // shared
@@ -353,7 +353,7 @@
 
 
 def output_kernel(dims, *refs):
-    seqs, chunks, shared, heads, rows, fan = dims
+    seqs, chunks, _, _, _, fan = dims
     parts, weight = refs[:fan], refs[fan]
     out, scratch = refs[fan + 2 :]
     me = lax.axis_index("dp")
@@ -373,7 +373,7 @@
 
 
 def buffer_kernel(dims, layers, *refs):
-    seqs, chunks, shared, heads, rows, fan = dims
+    seqs, chunks, shared, _, _, _ = dims
     new_rows = refs[1 : 1 + layers]
     past = refs[1 + layers : 4 + layers]
     outs = refs[4 + layers : 7 + layers]
@@ -469,7 +469,7 @@
     message = pltpu.VMEM((seqs * rows, LANES), f32)
     pool = pltpu.VMEM((rows * count, LANES), f32)
 
-    def fetch(after, blocks, name):
+    def fetch(after, blocks):
         sources = [array for array, _ in blocks]
         plan = [block for _, block in blocks]
         return pl.pallas_call(
@@ -482,7 +482,6 @@
             scratch_shapes=[pltpu.SemaphoreType.DMA((2 * len(blocks),))],
             compiler_params=params,
             cost_estimate=cost(4_000_000, 1_000_000),
-            name=name,
         )(*place([after], VMEM), *place(sources, HBM))
 
     def fetch_state(layer, after):
@@ -605,7 +604,7 @@
         own = output(parts, weight, states)
         partial = swaps(own, "tp")
         if layer + 1 < layers:
-            ahead = fetch(own, [(w, layer + 1) for w in weights], "fetch")
+            ahead = fetch(own, [(w, layer + 1) for w in weights])
             stream, *made = pl.pallas_call(
                 functools.partial(next_project_kernel, dims, layer + 1),
                 out_shape=[pltpu.VMEM(hidden.shape, bf16)] + [message] * fan,
@@ -638,7 +637,7 @@
 
 
 def kernels_fit(state, taps, write_taps, hidden, output_matrix, step_matrix):
-    layers, seqs, heads, head_dim, state_dim = state.shape
+    _, seqs, heads, head_dim, state_dim = state.shape
     shared = write_taps.shape[2] // LANES
     chunks = taps.shape[2] // LANES
     return (

time: 40.7 us -> 40.7 us (level)
  no operation moved by 1% of the time
where the time goes in v3:
time: 40.7 us; the launch traced here: 40.5 us
  starting transfers between devices  17.7 us (43%)
  Pallas kernels  15.1 us (37%)
  waiting for transfers between devices  6.92 us (17%)
  between operations  0.78 us (2%)
    ppermute x18, starting transfers between devices, swap(): lax.ppermute(array, axis, [(i, i ^ mask) for i in range(lax.axis_size(axi...  17.7 us
    ppermute x18, waiting for transfers between devices, swap(): lax.ppermute(array, axis, [(i, i ^ mask) for i in range(lax.axis_size(axi...  6.92 us
    pallas_call x2, Pallas kernels, update(): pl.pallas_call(functools.partial(update_kernel, dims, layer), out_shape=j...  2.54 us
    pallas_call x1, Pallas kernels, on_device_kernels(): pl.pallas_call(functools.partial(first_project_kernel, dims, 0), out_shap...  2.51 us
    pallas_call x1, Pallas kernels, on_device_kernels(): pl.pallas_call(functools.partial(table_kernel, dims), out_shape=[pltpu.VM...  2.38 us
    pallas_call x1, Pallas kernels, fetch(): pl.pallas_call(functools.partial(fetch_kernel, plan), out_shape=[pltpu.VM...  1.91 us
    pallas_call x1, Pallas kernels, fetch_state(): pl.pallas_call(functools.partial(fetch_state_kernel, layer), out_shape=[p...  1.55 us
    pallas_call x1, Pallas kernels, on_device_kernels(): pl.pallas_call(functools.partial(buffer_kernel, dims, layers), out_shape=...  1.39 us
  transfers between devices with their start and end apart: 18, of which 7 were waited for; matrix products, arithmetic and copies ran while one was open for 0% of the time, Pallas kernels for 24%

profile of v3, /device:TPU:0, one launch (start us, length us, event | category | flops | bytes accessed | tf_op | source)
XLA Modules:
  0.0 40.5 jit_solution(15110457904368768865)
XLA Ops:
  0.6 0.0 copy-start
  0.6 2.5 %project.2 = (f32[64,128]{1,0:T(8,128)S(1)}, f32[64,128]{1,0:T(8,128)S(1)}, f32[64,128]{1,0:T(8,128)S(1)}, f32[64,128]{1,0:T(8,128)S(1)}) custom-call(bf16[8,512]{1,0:T(8,128)(2,1)} %refs_16_.1, f32[2,512]{1,0:T(2,128)} %refs_15_.1, bf16[2,512,1024]{2,1,0:T(8,128)(2,1)} %refs_1_.4, bf16[2,512,1024]{2,1,0:T(8,128)(2,1)} %refs_2_.4, ...), custom_call_target="tpu_custom_call" | custom-call | tf_op jit(solution)/shard_map/project/pallas_call | solution.py:551
  3.2 0.6 %collective-permute-start = (f32[64,128]{1,0:T(8,128)S(1)}, f32[64,128]{1,0:T(8,128)S(1)}, u32[]{:S(2)}, u32[]{:S(2)}) collective-permute-start(f32[64,128]{1,0:T(8,128)S(1)} %get-tuple-element.43), channel_id=1, source_target_pairs={{0,1},{1,0},{2,3},{3,2},{4,5},{5,4},{6,7},{7,6},{8,9},{9,8},{10,11... | collective-permute-start | bytes 98312 | tf_op jit(solution)/shard_map/ppermute | solution.py:419
  3.7 2.6 %collective-permute-start.1 = (f32[64,128]{1,0:T(8,128)S(1)}, f32[64,128]{1,0:T(8,128)S(1)}, u32[]{:S(2)}, u32[]{:S(2)}) collective-permute-start(f32[64,128]{1,0:T(8,128)S(1)} %get-tuple-element.44), channel_id=1, source_target_pairs={{0,2},{1,3},{2,0},{3,1},{4,6},{5,7},{6,4},{7,5},{8,10},{9,11},{10,... | collective-permute-start | bytes 98312 | tf_op jit(solution)/shard_map/ppermute | solution.py:419
  6.3 0.0 collective-permute-start.2
  6.3 0.0 copy-done
  6.3 2.4 %tables.1 = (f32[2,128,128]{2,1,0:T(8,128)S(1)}, f32[2,16,64,128]{3,2,1,0:T(8,128)S(1)}, bf16[1024,512]{1,0:T(8,128)(2,1)S(1)}, f32[2,512]{1,0:T(2,128)S(1)}, bf...) custom-call(s32[2]{0:T(128)S(1)} %copy-done, f32[64,128]{1,0:T(8,128)S(1)} %get-tuple-element.41.refs_1_.refs_0_, ...), custom_call_target="tpu_custom_call" | custom-call | flops 4000000 | bytes 1000000 | tf_op jit(solution)/shard_map/tables/pallas_call | solution.py:572
  8.7 0.0 collective-permute-done.refs_1_
  8.7 0.0 collective-permute-done.1.refs_2_
  8.8 0.9 %collective-permute-done.2.refs_3_ = f32[64,128]{1,0:T(8,128)S(1)} collective-permute-done((f32[64,128]{1,0:T(8,128)S(1)}, f32[64,128]{1,0:T(8,128)S(1)}, u32[]{:S(2)}, u32[]{:S(2)}) %collective-permute-start.2) | collective-permute-done | bytes 32800 | tf_op jit(solution)/shard_map/ppermute | solution.py:419
  9.7 0.5 %mix.2 = (bf16[16,128]{1,0:T(8,128)(2,1)S(1)}, f32[2,16,128]{2,1,0:T(8,128)S(1)}, f32[16,128]{1,0:T(8,128)S(1)}, f32[2,8,128]{2,1,0:T(8,128)S(1)}, f32[2,16,128]{2,1,0:T(8,128)S(1)}) custom-call(f32[64,128]{1,0:T(8,128)S(1)} %get-tuple-element.41.refs_1_.refs_0_, f32[64,128]{1,0:T(8,128)S(1)} %collective-permute-done.refs_1_, ...), custom_call_target="tpu_custom_call" | custom-call | tf_op jit(solution)/shard_map/mix/pallas_call | solution.py:504
  10.2 0.9 %collective-permute-start.5 = (bf16[16,128]{1,0:T(8,128)(2,1)S(1)}, bf16[16,128]{1,0:T(8,128)(2,1)S(1)}, u32[]{:S(2)}, u32[]{:S(2)}) collective-permute-start(bf16[16,128]{1,0:T(8,128)(2,1)S(1)} %get-tuple-element.48.refs_0_), channel_id=1, source_target_pairs={{0,3},{1,2},{2,1},{3,0},{4,7},{5,6},{6,5},{7,4},{8,11},{9,10},{10,... | collective-permute-start | bytes 12296 | tf_op jit(solution)/shard_map/ppermute | solution.py:419
  11.0 1.0 %collective-permute-start.4 = (bf16[16,128]{1,0:T(8,128)(2,1)S(1)}, bf16[16,128]{1,0:T(8,128)(2,1)S(1)}, u32[]{:S(2)}, u32[]{:S(2)}) collective-permute-start(bf16[16,128]{1,0:T(8,128)(2,1)S(1)} %get-tuple-element.48.refs_0_), channel_id=1, source_target_pairs={{0,2},{1,3},{2,0},{3,1},{4,6},{5,7},{6,4},{7,5},{8,10},{9,11},{10,... | collective-permute-start | bytes 12296 | tf_op jit(solution)/shard_map/ppermute | solution.py:419
  12.0 0.1 collective-permute-start.3
  12.1 1.3 %update.2.refs_5_.refs_4_ = f32[2,2,16,64,128]{4,3,2,1,0:T(8,128)} custom-call(f32[16,128]{1,0:T(8,128)S(1)} %get-tuple-element.50.refs_0_, f32[2,8,128]{2,1,0:T(8,128)S(1)} %get-tuple-element.51.refs_1_, f32[2,16,128]{2,1,0:T(8,128)S(1)} %get-tuple-element.52.refs_2_, f32[2,16,64,128]{3,2,1,0:T(8,128)S(1)} %get-tuple-element.53.refs_3_), custom_call_target="tpu_custom_call" | custom-call | flops 4000000 | bytes 1000000 | tf_op jit(solution)/shard_map/update/pallas_call | solution.py:524
  13.4 0.0 collective-permute-done.5.refs_3_
  13.4 1.3 %collective-permute-done.4.refs_2_ = bf16[16,128]{1,0:T(8,128)(2,1)S(1)} collective-permute-done((bf16[16,128]{1,0:T(8,128)(2,1)S(1)}, bf16[16,128]{1,0:T(8,128)(2,1)S(1)}, u32[]{:S(2)}, u32[]{:S(2)}) %collective-permute-start.4) | collective-permute-done | bytes 4128 | tf_op jit(solution)/shard_map/ppermute | solution.py:419
  14.6 0.0 collective-permute-done.3.refs_1_
  14.7 0.2 output.2.refs_0_.refs_1_
  14.9 3.6 %collective-permute-start.8 = (f32[8,512]{1,0:T(8,128)S(1)}, f32[8,512]{1,0:T(8,128)S(1)}, u32[]{:S(2)}, u32[]{:S(2)}) collective-permute-start(f32[8,512]{1,0:T(8,128)S(1)} %output.2.refs_0_.refs_1_), channel_id=1, source_target_pairs={{0,12},{4,8},{8,4},{12,0},{1,13},{5,9},{9,5},{13,1},{2,14},{6,10},... | collective-permute-start | bytes 49160 | tf_op jit(solution)/shard_map/ppermute | solution.py:419
  18.5 0.0 collective-permute-start.7
  18.5 0.8 %collective-permute-start.6 = (f32[8,512]{1,0:T(8,128)S(1)}, f32[8,512]{1,0:T(8,128)S(1)}, u32[]{:S(2)}, u32[]{:S(2)}) collective-permute-start(f32[8,512]{1,0:T(8,128)S(1)} %output.2.refs_0_.refs_1_), channel_id=1, source_target_pairs={{0,4},{4,0},{8,12},{12,8},{1,5},{5,1},{9,13},{13,9},{2,6},{6,2},{1... | collective-permute-start | bytes 49160 | tf_op jit(solution)/shard_map/ppermute | solution.py:419
  19.3 1.9 %shard_map.236 = (bf16[512,1024]{1,0:T(8,128)(2,1)S(1)}, bf16[512,1024]{1,0:T(8,128)(2,1)S(1)}, bf16[512,512]{1,0:T(8,128)(2,1)S(1)}, bf16[512,512]{1,0:T(8,128)(2,1)S(1)}, bf16[64,512]{1,0:T(8,128)(2,1)S(1)}) custom-call(f32[8,512]{1,0:T(8,128)S(1)} %output.2.refs_0_.refs_1_, bf16[2,512,1024]{2,1,0:T(8,128)(2,1)} %refs_1_.4, bf16[2,512,1024]{2,1,0:T(8,128)(2,1)} %refs_2_.4, ...), custom_call_target="tpu_custom_call" | custom-call | flops 4000000 | bytes 1000000 | tf_op jit(solution)/shard_map/pallas_call | solution.py:475
  21.2 0.0 collective-permute-done.8.refs_4_
  21.2 1.9 %collective-permute-done.7.refs_3_ = f32[8,512]{1,0:T(8,128)S(1)} collective-permute-done((f32[8,512]{1,0:T(8,128)S(1)}, f32[8,512]{1,0:T(8,128)S(1)}, u32[]{:S(2)}, u32[]{:S(2)}) %collective-permute-start.7) | collective-permute-done | bytes 16416 | tf_op jit(solution)/shard_map/ppermute | solution.py:419
  23.1 0.0 collective-permute-done.6.refs_2_
  23.1 0.6 %project.3 = (bf16[8,512]{1,0:T(8,128)(2,1)S(1)}, f32[64,128]{1,0:T(8,128)S(1)}, f32[64,128]{1,0:T(8,128)S(1)}, f32[64,128]{1,0:T(8,128)S(1)}, f32[64,128]{1,0:T(8,128)S(1)}) custom-call(bf16[8,512]{1,0:T(8,128)(2,1)S(1)} %get-tuple-element.42.refs_0_, f32[8,512]{1,0:T(8,128)S(1)} %output.2.refs_0_.refs_1_, f32[8,512]{1,0:T(8,128)S(1)} %collective-permute-done.6.refs_2_, ...), custom_call_target="tpu_custom_call" | custom-call | tf_op jit(solution)/shard_map/project/pallas_call | solution.py:608
  23.8 0.1 collective-permute-start.9
  23.9 1.0 %collective-permute-start.10 = (f32[64,128]{1,0:T(8,128)S(1)}, f32[64,128]{1,0:T(8,128)S(1)}, u32[]{:S(2)}, u32[]{:S(2)}) collective-permute-start(f32[64,128]{1,0:T(8,128)S(1)} %get-tuple-element.63), channel_id=1, source_target_pairs={{0,2},{1,3},{2,0},{3,1},{4,6},{5,7},{6,4},{7,5},{8,10},{9,11},{10,... | collective-permute-start | bytes 98312 | tf_op jit(solution)/shard_map/ppermute | solution.py:419
  24.9 0.8 %collective-permute-start.11 = (f32[64,128]{1,0:T(8,128)S(1)}, f32[64,128]{1,0:T(8,128)S(1)}, u32[]{:S(2)}, u32[]{:S(2)}) collective-permute-start(f32[64,128]{1,0:T(8,128)S(1)} %get-tuple-element.64), channel_id=1, source_target_pairs={{0,3},{1,2},{2,1},{3,0},{4,7},{5,6},{6,5},{7,4},{8,11},{9,10},{10,... | collective-permute-start | bytes 98312 | tf_op jit(solution)/shard_map/ppermute | solution.py:419
  25.7 1.5 %fetch.1 = (f32[2,16,64,128]{3,2,1,0:T(8,128)S(1)}, bf16[1024,512]{1,0:T(8,128)(2,1)S(1)}, bf16[2048,256]{1,0:T(8,128)(2,1)S(1)}) custom-call(f32[64,128]{1,0:T(8,128)S(1)} %get-tuple-element.61.refs_0_, f32[2,2,16,64,128]{4,3,2,1,0:T(8,128)} %refs_1_.5, bf16[2,1024,512]{2,1,0:T(8,128)(2,1)} %refs_2_.5), custom_call_target="tpu_custom_call" | custom-call | flops 4000000 | bytes 1000000 | tf_op jit(solution)/shard_map/fetch/pallas_call | solution.py:488
  27.3 0.0 collective-permute-done.9.refs_1_
  27.3 0.6 %collective-permute-done.10.refs_2_ = f32[64,128]{1,0:T(8,128)S(1)} collective-permute-done((f32[64,128]{1,0:T(8,128)S(1)}, f32[64,128]{1,0:T(8,128)S(1)}, u32[]{:S(2)}, u32[]{:S(2)}) %collective-permute-start.10) | collective-permute-done | bytes 32800 | tf_op jit(solution)/shard_map/ppermute | solution.py:419
  27.9 0.4 %collective-permute-done.11.refs_3_ = f32[64,128]{1,0:T(8,128)S(1)} collective-permute-done((f32[64,128]{1,0:T(8,128)S(1)}, f32[64,128]{1,0:T(8,128)S(1)}, u32[]{:S(2)}, u32[]{:S(2)}) %collective-permute-start.11) | collective-permute-done | bytes 32800 | tf_op jit(solution)/shard_map/ppermute | solution.py:419
  28.3 0.5 %mix.3 = (bf16[16,128]{1,0:T(8,128)(2,1)S(1)}, f32[2,16,128]{2,1,0:T(8,128)S(1)}, f32[16,128]{1,0:T(8,128)S(1)}, f32[2,8,128]{2,1,0:T(8,128)S(1)}, f32[2,16,128]{2,1,0:T(8,128)S(1)}) custom-call(f32[64,128]{1,0:T(8,128)S(1)} %get-tuple-element.61.refs_0_, f32[64,128]{1,0:T(8,128)S(1)} %collective-permute-done.9.refs_1_, ...), custom_call_target="tpu_custom_call" | custom-call | tf_op jit(solution)/shard_map/mix/pallas_call | solution.py:504
  28.8 0.8 %collective-permute-start.14 = (bf16[16,128]{1,0:T(8,128)(2,1)S(1)}, bf16[16,128]{1,0:T(8,128)(2,1)S(1)}, u32[]{:S(2)}, u32[]{:S(2)}) collective-permute-start(bf16[16,128]{1,0:T(8,128)(2,1)S(1)} %get-tuple-element.66.refs_0_), channel_id=1, source_target_pairs={{0,3},{1,2},{2,1},{3,0},{4,7},{5,6},{6,5},{7,4},{8,11},{9,10},{10,... | collective-permute-start | bytes 12296 | tf_op jit(solution)/shard_map/ppermute | solution.py:419
  29.6 1.0 %collective-permute-start.13 = (bf16[16,128]{1,0:T(8,128)(2,1)S(1)}, bf16[16,128]{1,0:T(8,128)(2,1)S(1)}, u32[]{:S(2)}, u32[]{:S(2)}) collective-permute-start(bf16[16,128]{1,0:T(8,128)(2,1)S(1)} %get-tuple-element.66.refs_0_), channel_id=1, source_target_pairs={{0,2},{1,3},{2,0},{3,1},{4,6},{5,7},{6,4},{7,5},{8,10},{9,11},{10,... | collective-permute-start | bytes 12296 | tf_op jit(solution)/shard_map/ppermute | solution.py:419
  30.6 0.1 collective-permute-start.12
  30.7 1.3 %update.3.refs_5_ = f32[2,2,16,64,128]{4,3,2,1,0:T(8,128)} custom-call(f32[16,128]{1,0:T(8,128)S(1)} %get-tuple-element.68.refs_0_, f32[2,8,128]{2,1,0:T(8,128)S(1)} %get-tuple-element.69.refs_1_, f32[2,16,128]{2,1,0:T(8,128)S(1)} %get-tuple-element.70.refs_2_, f32[2,16,64,128]{3,2,1,0:T(8,128)S(1)} %get-tuple-element.71.refs_3_, ...), custom_call_target="tpu_custom_call", output_to_operand_aliasing={{}: (4, {})} | custom-call | flops 4000000 | bytes 1000000 | tf_op jit(solution)/shard_map/update/pallas_call | solution.py:524
  32.0 0.0 collective-permute-done.14.refs_3_
  32.0 1.3 %collective-permute-done.13.refs_2_ = bf16[16,128]{1,0:T(8,128)(2,1)S(1)} collective-permute-done((bf16[16,128]{1,0:T(8,128)(2,1)S(1)}, bf16[16,128]{1,0:T(8,128)(2,1)S(1)}, u32[]{:S(2)}, u32[]{:S(2)}) %collective-permute-start.13) | collective-permute-done | bytes 4128 | tf_op jit(solution)/shard_map/ppermute | solution.py:419
  33.3 0.0 collective-permute-done.12.refs_1_
  33.3 0.2 output.3.refs_0_
  33.5 1.7 %collective-permute-start.17 = (f32[8,512]{1,0:T(8,128)S(1)}, f32[8,512]{1,0:T(8,128)S(1)}, u32[]{:S(2)}, u32[]{:S(2)}) collective-permute-start(f32[8,512]{1,0:T(8,128)S(1)} %output.3.refs_0_), channel_id=1, source_target_pairs={{0,12},{4,8},{8,4},{12,0},{1,13},{5,9},{9,5},{13,1},{2,14},{6,10},... | collective-permute-start | bytes 49160 | tf_op jit(solution)/shard_map/ppermute | solution.py:419
  35.2 0.4 collective-permute-start.16
  35.6 2.3 %collective-permute-start.15 = (f32[8,512]{1,0:T(8,128)S(1)}, f32[8,512]{1,0:T(8,128)S(1)}, u32[]{:S(2)}, u32[]{:S(2)}) collective-permute-start(f32[8,512]{1,0:T(8,128)S(1)} %output.3.refs_0_), channel_id=1, source_target_pairs={{0,4},{4,0},{8,12},{12,8},{1,5},{5,1},{9,13},{13,9},{2,6},{6,2},{1... | collective-permute-start | bytes 49160 | tf_op jit(solution)/shard_map/ppermute | solution.py:419
  37.9 1.4 %buffers.1 = (bf16[2,3,2,1024]{3,2,1,0:T(2,128)(2,1)}, bf16[2,3,2,512]{3,2,1,0:T(2,128)(2,1)}, bf16[2,3,2,512]{3,2,1,0:T(2,128)(2,1)}) custom-call(f32[8,512]{1,0:T(8,128)S(1)} %output.3.refs_0_, f32[2,16,128]{2,1,0:T(8,128)S(1)} %get-tuple-element.72.refs_1_, f32[2,16,128]{2,1,0:T(8,128)S(1)} %get-tuple-element.73.refs_2_, ...), custom_call_target="tpu_custom_call" | custom-call | flops 4000000 | bytes 1000000 | tf_op jit(solution)/shard_map/buffers/pallas_call | solution.py:617
  39.3 0.0 collective-permute-done.17.refs_3_
  39.3 0.5 %collective-permute-done.16.refs_2_ = f32[8,512]{1,0:T(8,128)S(1)} collective-permute-done((f32[8,512]{1,0:T(8,128)S(1)}, f32[8,512]{1,0:T(8,128)S(1)}, u32[]{:S(2)}, u32[]{:S(2)}) %collective-permute-start.16) | collective-permute-done | bytes 16416 | tf_op jit(solution)/shard_map/ppermute | solution.py:419
  39.8 0.0 collective-permute-done.15.refs_1_
  39.8 0.6 %close.1 = bf16[8,512]{1,0:T(8,128)(2,1)} custom-call(bf16[8,512]{1,0:T(8,128)(2,1)S(1)} %get-tuple-element.60.x_ref, f32[8,512]{1,0:T(8,128)S(1)} %output.3.refs_0_, f32[8,512]{1,0:T(8,128)S(1)} %collective-permute-done.15.refs_1_, f32[8,512]{1,0:T(8,128)S(1)} %collective-permute-done.16.refs_2_, f32[8,512]{1,0:T(8,128)S(1)} %collective-permute-done.17.refs_3_), custom_call_target="tpu_custom_call" | custom-call | tf_op jit(solution)/shard_map/close/pallas_call | solution.py:628
Async XLA Ops:
  0.6 5.7 %copy-start = (s32[2]{0:T(128)S(1)}, s32[2]{0:T(128)}, u32[]{:S(2)}) copy-start(s32[2]{0:T(128)} %refs_0_.3) | copy-start | bytes 28
  3.2 5.6 %collective-permute-start = (f32[64,128]{1,0:T(8,128)S(1)}, f32[64,128]{1,0:T(8,128)S(1)}, u32[]{:S(2)}, u32[]{:S(2)}) collective-permute-start(f32[64,128]{1,0:T(8,128)S(1)} %get-tuple-element.43), channel_id=1, source_target_pairs={{0,1},{1,0},{2,3},{3,2},{4,5},{5,4},{6,7},{7,6},{8,9},{9,8},{10,11... | collective-permute-start | bytes 98312 | tf_op jit(solution)/shard_map/ppermute | solution.py:419
  3.7 5.0 %collective-permute-start.1 = (f32[64,128]{1,0:T(8,128)S(1)}, f32[64,128]{1,0:T(8,128)S(1)}, u32[]{:S(2)}, u32[]{:S(2)}) collective-permute-start(f32[64,128]{1,0:T(8,128)S(1)} %get-tuple-element.44), channel_id=1, source_target_pairs={{0,2},{1,3},{2,0},{3,1},{4,6},{5,7},{6,4},{7,5},{8,10},{9,11},{10,... | collective-permute-start | bytes 98312 | tf_op jit(solution)/shard_map/ppermute | solution.py:419
  6.3 3.4 %collective-permute-start.2 = (f32[64,128]{1,0:T(8,128)S(1)}, f32[64,128]{1,0:T(8,128)S(1)}, u32[]{:S(2)}, u32[]{:S(2)}) collective-permute-start(f32[64,128]{1,0:T(8,128)S(1)} %get-tuple-element.45), channel_id=1, source_target_pairs={{0,3},{1,2},{2,1},{3,0},{4,7},{5,6},{6,5},{7,4},{8,11},{9,10},{10,... | collective-permute-start | bytes 98312 | tf_op jit(solution)/shard_map/ppermute | solution.py:419
  10.2 3.2 %collective-permute-start.5 = (bf16[16,128]{1,0:T(8,128)(2,1)S(1)}, bf16[16,128]{1,0:T(8,128)(2,1)S(1)}, u32[]{:S(2)}, u32[]{:S(2)}) collective-permute-start(bf16[16,128]{1,0:T(8,128)(2,1)S(1)} %get-tuple-element.48.refs_0_), channel_id=1, source_target_pairs={{0,3},{1,2},{2,1},{3,0},{4,7},{5,6},{6,5},{7,4},{8,11},{9,10},{10,... | collective-permute-start | bytes 12296 | tf_op jit(solution)/shard_map/ppermute | solution.py:419
  11.0 3.6 %collective-permute-start.4 = (bf16[16,128]{1,0:T(8,128)(2,1)S(1)}, bf16[16,128]{1,0:T(8,128)(2,1)S(1)}, u32[]{:S(2)}, u32[]{:S(2)}) collective-permute-start(bf16[16,128]{1,0:T(8,128)(2,1)S(1)} %get-tuple-element.48.refs_0_), channel_id=1, source_target_pairs={{0,2},{1,3},{2,0},{3,1},{4,6},{5,7},{6,4},{7,5},{8,10},{9,11},{10,... | collective-permute-start | bytes 12296 | tf_op jit(solution)/shard_map/ppermute | solution.py:419
  12.0 2.6 %collective-permute-start.3 = (bf16[16,128]{1,0:T(8,128)(2,1)S(1)}, bf16[16,128]{1,0:T(8,128)(2,1)S(1)}, u32[]{:S(2)}, u32[]{:S(2)}) collective-permute-start(bf16[16,128]{1,0:T(8,128)(2,1)S(1)} %get-tuple-element.48.refs_0_), channel_id=1, source_target_pairs={{0,1},{1,0},{2,3},{3,2},{4,5},{5,4},{6,7},{7,6},{8,9},{9,8},{10,11... | collective-permute-start | bytes 12296 | tf_op jit(solution)/shard_map/ppermute | solution.py:419
  14.9 6.3 %collective-permute-start.8 = (f32[8,512]{1,0:T(8,128)S(1)}, f32[8,512]{1,0:T(8,128)S(1)}, u32[]{:S(2)}, u32[]{:S(2)}) collective-permute-start(f32[8,512]{1,0:T(8,128)S(1)} %output.2.refs_0_.refs_1_), channel_id=1, source_target_pairs={{0,12},{4,8},{8,4},{12,0},{1,13},{5,9},{9,5},{13,1},{2,14},{6,10},... | collective-permute-start | bytes 49160 | tf_op jit(solution)/shard_map/ppermute | solution.py:419
  18.5 4.6 %collective-permute-start.7 = (f32[8,512]{1,0:T(8,128)S(1)}, f32[8,512]{1,0:T(8,128)S(1)}, u32[]{:S(2)}, u32[]{:S(2)}) collective-permute-start(f32[8,512]{1,0:T(8,128)S(1)} %output.2.refs_0_.refs_1_), channel_id=1, source_target_pairs={{0,8},{4,12},{8,0},{12,4},{1,9},{5,13},{9,1},{13,5},{2,10},{6,14},... | collective-permute-start | bytes 49160 | tf_op jit(solution)/shard_map/ppermute | solution.py:419
  18.5 4.6 %collective-permute-start.6 = (f32[8,512]{1,0:T(8,128)S(1)}, f32[8,512]{1,0:T(8,128)S(1)}, u32[]{:S(2)}, u32[]{:S(2)}) collective-permute-start(f32[8,512]{1,0:T(8,128)S(1)} %output.2.refs_0_.refs_1_), channel_id=1, source_target_pairs={{0,4},{4,0},{8,12},{12,8},{1,5},{5,1},{9,13},{13,9},{2,6},{6,2},{1... | collective-permute-start | bytes 49160 | tf_op jit(solution)/shard_map/ppermute | solution.py:419
  23.8 3.5 %collective-permute-start.9 = (f32[64,128]{1,0:T(8,128)S(1)}, f32[64,128]{1,0:T(8,128)S(1)}, u32[]{:S(2)}, u32[]{:S(2)}) collective-permute-start(f32[64,128]{1,0:T(8,128)S(1)} %get-tuple-element.62), channel_id=1, source_target_pairs={{0,1},{1,0},{2,3},{3,2},{4,5},{5,4},{6,7},{7,6},{8,9},{9,8},{10,11... | collective-permute-start | bytes 98312 | tf_op jit(solution)/shard_map/ppermute | solution.py:419
  23.9 4.0 %collective-permute-start.10 = (f32[64,128]{1,0:T(8,128)S(1)}, f32[64,128]{1,0:T(8,128)S(1)}, u32[]{:S(2)}, u32[]{:S(2)}) collective-permute-start(f32[64,128]{1,0:T(8,128)S(1)} %get-tuple-element.63), channel_id=1, source_target_pairs={{0,2},{1,3},{2,0},{3,1},{4,6},{5,7},{6,4},{7,5},{8,10},{9,11},{10,... | collective-permute-start | bytes 98312 | tf_op jit(solution)/shard_map/ppermute | solution.py:419
  24.9 3.4 %collective-permute-start.11 = (f32[64,128]{1,0:T(8,128)S(1)}, f32[64,128]{1,0:T(8,128)S(1)}, u32[]{:S(2)}, u32[]{:S(2)}) collective-permute-start(f32[64,128]{1,0:T(8,128)S(1)} %get-tuple-element.64), channel_id=1, source_target_pairs={{0,3},{1,2},{2,1},{3,0},{4,7},{5,6},{6,5},{7,4},{8,11},{9,10},{10,... | collective-permute-start | bytes 98312 | tf_op jit(solution)/shard_map/ppermute | solution.py:419
  28.8 3.2 %collective-permute-start.14 = (bf16[16,128]{1,0:T(8,128)(2,1)S(1)}, bf16[16,128]{1,0:T(8,128)(2,1)S(1)}, u32[]{:S(2)}, u32[]{:S(2)}) collective-permute-start(bf16[16,128]{1,0:T(8,128)(2,1)S(1)} %get-tuple-element.66.refs_0_), channel_id=1, source_target_pairs={{0,3},{1,2},{2,1},{3,0},{4,7},{5,6},{6,5},{7,4},{8,11},{9,10},{10,... | collective-permute-start | bytes 12296 | tf_op jit(solution)/shard_map/ppermute | solution.py:419
  29.6 3.6 %collective-permute-start.13 = (bf16[16,128]{1,0:T(8,128)(2,1)S(1)}, bf16[16,128]{1,0:T(8,128)(2,1)S(1)}, u32[]{:S(2)}, u32[]{:S(2)}) collective-permute-start(bf16[16,128]{1,0:T(8,128)(2,1)S(1)} %get-tuple-element.66.refs_0_), channel_id=1, source_target_pairs={{0,2},{1,3},{2,0},{3,1},{4,6},{5,7},{6,4},{7,5},{8,10},{9,11},{10,... | collective-permute-start | bytes 12296 | tf_op jit(solution)/shard_map/ppermute | solution.py:419
  30.6 2.6 %collective-permute-start.12 = (bf16[16,128]{1,0:T(8,128)(2,1)S(1)}, bf16[16,128]{1,0:T(8,128)(2,1)S(1)}, u32[]{:S(2)}, u32[]{:S(2)}) collective-permute-start(bf16[16,128]{1,0:T(8,128)(2,1)S(1)} %get-tuple-element.66.refs_0_), channel_id=1, source_target_pairs={{0,1},{1,0},{2,3},{3,2},{4,5},{5,4},{6,7},{7,6},{8,9},{9,8},{10,11... | collective-permute-start | bytes 12296 | tf_op jit(solution)/shard_map/ppermute | solution.py:419
  33.5 5.8 %collective-permute-start.17 = (f32[8,512]{1,0:T(8,128)S(1)}, f32[8,512]{1,0:T(8,128)S(1)}, u32[]{:S(2)}, u32[]{:S(2)}) collective-permute-start(f32[8,512]{1,0:T(8,128)S(1)} %output.3.refs_0_), channel_id=1, source_target_pairs={{0,12},{4,8},{8,4},{12,0},{1,13},{5,9},{9,5},{13,1},{2,14},{6,10},... | collective-permute-start | bytes 49160 | tf_op jit(solution)/shard_map/ppermute | solution.py:419
  35.2 4.6 %collective-permute-start.16 = (f32[8,512]{1,0:T(8,128)S(1)}, f32[8,512]{1,0:T(8,128)S(1)}, u32[]{:S(2)}, u32[]{:S(2)}) collective-permute-start(f32[8,512]{1,0:T(8,128)S(1)} %output.3.refs_0_), channel_id=1, source_target_pairs={{0,8},{4,12},{8,0},{12,4},{1,9},{5,13},{9,1},{13,5},{2,10},{6,14},... | collective-permute-start | bytes 49160 | tf_op jit(solution)/shard_map/ppermute | solution.py:419
  35.6 4.3 %collective-permute-start.15 = (f32[8,512]{1,0:T(8,128)S(1)}, f32[8,512]{1,0:T(8,128)S(1)}, u32[]{:S(2)}, u32[]{:S(2)}) collective-permute-start(f32[8,512]{1,0:T(8,128)S(1)} %output.3.refs_0_), channel_id=1, source_target_pairs={{0,4},{4,0},{8,12},{12,8},{1,5},{5,1},{9,13},{13,9},{2,6},{6,2},{1... | collective-permute-start | bytes 49160 | tf_op jit(solution)/shard_map/ppermute | solution.py:419

commit v4 on v3

--- a/solution.py
+++ b/solution.py
@@ -13,6 +13,8 @@
 
 epsilon = 1e-06
 LANES = 128
+LINE = ((1, 3, 0, 2), (3, 2, 1, 0), (2, 0, 3, 1))
+LINE_LAST = ((3, 2, 1, 0), (2, 3, 0, 1), (1, 0, 3, 2))
 f32 = jnp.float32
 bf16 = jnp.bfloat16
 VMEM = pltpu.VMEM
@@ -419,6 +421,14 @@
     return lax.ppermute(array, axis, [(i, i ^ mask) for i in range(lax.axis_size(axis))])
 
 
+def line_swaps(array, axis, rounds):
+    got = []
+    for targets in rounds:
+        got.append(lax.ppermute(array, axis, list(enumerate(targets))))
+    paired = [all(t[t[i]] == i for i in range(len(t))) for t in rounds].index(True)
+    return [array, got[paired]] + got[:paired] + got[paired + 1 :]
+
+
 def swaps(array, axis):
     return [array] + [swap(array, axis, mask) for mask in range(1, lax.axis_size(axis))]
 
@@ -449,7 +459,7 @@
     layers, seqs, heads = recurrent_head_state.shape[:3]
     chunks = input_filter_taps.shape[2] // LANES
     shared = write_filter_taps.shape[2] // LANES
-    rows = -(-(2 * chunks + 2 * shared + 1) // 8) * 8
+    rows = -(-(2 * chunks + 2 * shared + 1) // 4) * 4
     fan = lax.axis_size("dp")
     dims = (seqs, chunks, shared, heads, rows, fan)
     count = hidden.shape[0]
@@ -602,7 +612,11 @@
         parts = swaps(gated, "dp")
         states = update(layer, factors, held, states)
         own = output(parts, weight, states)
-        partial = swaps(own, "tp")
+        if lax.axis_size("tp") == 4:
+            rounds = LINE_LAST if layer + 1 == layers else LINE
+            partial = line_swaps(own, "tp", rounds)
+        else:
+            partial = swaps(own, "tp")
         if layer + 1 < layers:
             ahead = fetch(own, [(w, layer + 1) for w in weights])
             stream, *made = pl.pallas_call(

time: 40.7 us -> 43.3 us (1.064)
  waiting for transfers between devices: 6.92 us -> 8.3 us
  starting transfers between devices: 17.7 us -> 18.9 us
    ppermute x0 -> x6, starting transfers between devices: none -> 10 us  [line_swaps(): got.append(lax.ppermute(array, axis, list(enumerate(targets))))]
    ppermute x18 -> x12, starting transfers between devices: 17.7 us -> 8.88 us  [swap(): lax.ppermute(array, axis, [(i, i ^ mask) for i in range(lax.axis_size(axi...]
    ppermute x0 -> x6, waiting for transfers between devices: none -> 3.91 us  [line_swaps(): got.append(lax.ppermute(array, axis, list(enumerate(targets))))]
    ppermute x18 -> x12, waiting for transfers between devices: 6.92 us -> 4.39 us  [swap(): lax.ppermute(array, axis, [(i, i ^ mask) for i in range(lax.axis_size(axi...]
  transfers between devices with their start and end apart: 18 -> 18, of which waited for: 7 -> 7; matrix products, arithmetic and copies ran while one was open for 0% -> 0% of each run, Pallas kernels for 24% -> 23%
where the time goes in v4:
time: 43.3 us; the launch traced here: 43.1 us
  starting transfers between devices  18.9 us (44%)
  Pallas kernels  15 us (35%)
  waiting for transfers between devices  8.3 us (19%)
  between operations  0.8 us (2%)
    ppermute x6, starting transfers between devices, line_swaps(): got.append(lax.ppermute(array, axis, list(enumerate(targets))))  10 us
    ppermute x12, starting transfers between devices, swap(): lax.ppermute(array, axis, [(i, i ^ mask) for i in range(lax.axis_size(axi...  8.88 us
    ppermute x12, waiting for transfers between devices, swap(): lax.ppermute(array, axis, [(i, i ^ mask) for i in range(lax.axis_size(axi...  4.39 us
    ppermute x6, waiting for transfers between devices, line_swaps(): got.append(lax.ppermute(array, axis, list(enumerate(targets))))  3.91 us
    pallas_call x2, Pallas kernels, update(): pl.pallas_call(functools.partial(update_kernel, dims, layer), out_shape=j...  2.53 us
    pallas_call x1, Pallas kernels, on_device_kernels(): pl.pallas_call(functools.partial(first_project_kernel, dims, 0), out_shap...  2.51 us
    pallas_call x1, Pallas kernels, on_device_kernels(): pl.pallas_call(functools.partial(table_kernel, dims), out_shape=[pltpu.VM...  2.38 us
    pallas_call x1, Pallas kernels, fetch(): pl.pallas_call(functools.partial(fetch_kernel, plan), out_shape=[pltpu.VM...  1.91 us
  transfers between devices with their start and end apart: 18, of which 7 were waited for; matrix products, arithmetic and copies ran while one was open for 0% of the time, Pallas kernels for 23%

profile of v4, /device:TPU:0, one launch (start us, length us, event | category | flops | bytes accessed | tf_op | source)
XLA Modules:
  0.0 43.1 jit_solution(9668471981742776030)
XLA Ops:
  0.6 0.0 copy-start
  0.6 2.5 %project.2 = (f32[56,128]{1,0:T(8,128)S(1)}, f32[56,128]{1,0:T(8,128)S(1)}, f32[56,128]{1,0:T(8,128)S(1)}, f32[56,128]{1,0:T(8,128)S(1)}) custom-call(bf16[8,512]{1,0:T(8,128)(2,1)} %refs_16_.1, f32[2,512]{1,0:T(2,128)} %refs_15_.1, bf16[2,512,1024]{2,1,0:T(8,128)(2,1)} %refs_1_.4, bf16[2,512,1024]{2,1,0:T(8,128)(2,1)} %refs_2_.4, ...), custom_call_target="tpu_custom_call" | custom-call | tf_op jit(solution)/shard_map/project/pallas_call | solution.py:561
  3.2 0.6 %collective-permute-start = (f32[56,128]{1,0:T(8,128)S(1)}, f32[56,128]{1,0:T(8,128)S(1)}, u32[]{:S(2)}, u32[]{:S(2)}) collective-permute-start(f32[56,128]{1,0:T(8,128)S(1)} %get-tuple-element.43), channel_id=1, source_target_pairs={{0,1},{1,0},{2,3},{3,2},{4,5},{5,4},{6,7},{7,6},{8,9},{9,8},{10,11... | collective-permute-start | bytes 86024 | tf_op jit(solution)/shard_map/ppermute | solution.py:421
  3.7 2.6 %collective-permute-start.1 = (f32[56,128]{1,0:T(8,128)S(1)}, f32[56,128]{1,0:T(8,128)S(1)}, u32[]{:S(2)}, u32[]{:S(2)}) collective-permute-start(f32[56,128]{1,0:T(8,128)S(1)} %get-tuple-element.44), channel_id=1, source_target_pairs={{0,2},{1,3},{2,0},{3,1},{4,6},{5,7},{6,4},{7,5},{8,10},{9,11},{10,... | collective-permute-start | bytes 86024 | tf_op jit(solution)/shard_map/ppermute | solution.py:421
  6.3 0.0 collective-permute-start.2
  6.3 0.0 copy-done
  6.3 2.4 %tables.1 = (f32[2,128,128]{2,1,0:T(8,128)S(1)}, f32[2,16,64,128]{3,2,1,0:T(8,128)S(1)}, bf16[1024,512]{1,0:T(8,128)(2,1)S(1)}, f32[2,512]{1,0:T(2,128)S(1)}, bf...) custom-call(s32[2]{0:T(128)S(1)} %copy-done, f32[56,128]{1,0:T(8,128)S(1)} %get-tuple-element.41.refs_1_.refs_0_, ...), custom_call_target="tpu_custom_call" | custom-call | flops 4000000 | bytes 1000000 | tf_op jit(solution)/shard_map/tables/pallas_call | solution.py:582
  8.7 0.0 collective-permute-done.refs_1_
  8.7 0.0 collective-permute-done.1.refs_2_
  8.8 0.8 %collective-permute-done.2.refs_3_ = f32[56,128]{1,0:T(8,128)S(1)} collective-permute-done((f32[56,128]{1,0:T(8,128)S(1)}, f32[56,128]{1,0:T(8,128)S(1)}, u32[]{:S(2)}, u32[]{:S(2)}) %collective-permute-start.2) | collective-permute-done | bytes 28704 | tf_op jit(solution)/shard_map/ppermute | solution.py:421
  9.6 0.5 %mix.2 = (bf16[16,128]{1,0:T(8,128)(2,1)S(1)}, f32[2,16,128]{2,1,0:T(8,128)S(1)}, f32[16,128]{1,0:T(8,128)S(1)}, f32[2,8,128]{2,1,0:T(8,128)S(1)}, f32[2,16,128]{2,1,0:T(8,128)S(1)}) custom-call(f32[56,128]{1,0:T(8,128)S(1)} %get-tuple-element.41.refs_1_.refs_0_, f32[56,128]{1,0:T(8,128)S(1)} %collective-permute-done.refs_1_, ...), custom_call_target="tpu_custom_call" | custom-call | tf_op jit(solution)/shard_map/mix/pallas_call | solution.py:514
  10.1 0.9 %collective-permute-start.5 = (bf16[16,128]{1,0:T(8,128)(2,1)S(1)}, bf16[16,128]{1,0:T(8,128)(2,1)S(1)}, u32[]{:S(2)}, u32[]{:S(2)}) collective-permute-start(bf16[16,128]{1,0:T(8,128)(2,1)S(1)} %get-tuple-element.48.refs_0_), channel_id=1, source_target_pairs={{0,3},{1,2},{2,1},{3,0},{4,7},{5,6},{6,5},{7,4},{8,11},{9,10},{10,... | collective-permute-start | bytes 12296 | tf_op jit(solution)/shard_map/ppermute | solution.py:421
  11.0 0.9 %collective-permute-start.4 = (bf16[16,128]{1,0:T(8,128)(2,1)S(1)}, bf16[16,128]{1,0:T(8,128)(2,1)S(1)}, u32[]{:S(2)}, u32[]{:S(2)}) collective-permute-start(bf16[16,128]{1,0:T(8,128)(2,1)S(1)} %get-tuple-element.48.refs_0_), channel_id=1, source_target_pairs={{0,2},{1,3},{2,0},{3,1},{4,6},{5,7},{6,4},{7,5},{8,10},{9,11},{10,... | collective-permute-start | bytes 12296 | tf_op jit(solution)/shard_map/ppermute | solution.py:421
  11.9 0.1 collective-permute-start.3
  12.0 1.3 %update.2.refs_5_.refs_4_ = f32[2,2,16,64,128]{4,3,2,1,0:T(8,128)} custom-call(f32[16,128]{1,0:T(8,128)S(1)} %get-tuple-element.50.refs_0_, f32[2,8,128]{2,1,0:T(8,128)S(1)} %get-tuple-element.51.refs_1_, f32[2,16,128]{2,1,0:T(8,128)S(1)} %get-tuple-element.52.refs_2_, f32[2,16,64,128]{3,2,1,0:T(8,128)S(1)} %get-tuple-element.53.refs_3_), custom_call_target="tpu_custom_call" | custom-call | flops 4000000 | bytes 1000000 | tf_op jit(solution)/shard_map/update/pallas_call | solution.py:534
  13.3 0.0 collective-permute-done.5.refs_3_
  13.3 1.3 %collective-permute-done.4.refs_2_ = bf16[16,128]{1,0:T(8,128)(2,1)S(1)} collective-permute-done((bf16[16,128]{1,0:T(8,128)(2,1)S(1)}, bf16[16,128]{1,0:T(8,128)(2,1)S(1)}, u32[]{:S(2)}, u32[]{:S(2)}) %collective-permute-start.4) | collective-permute-done | bytes 4128 | tf_op jit(solution)/shard_map/ppermute | solution.py:421
  14.6 0.0 collective-permute-done.3.refs_1_
  14.6 0.2 output.2.refs_0_.refs_1_
  14.9 2.6 %collective-permute-start.8 = (f32[8,512]{1,0:T(8,128)S(1)}, f32[8,512]{1,0:T(8,128)S(1)}, u32[]{:S(2)}, u32[]{:S(2)}) collective-permute-start(f32[8,512]{1,0:T(8,128)S(1)} %output.2.refs_0_.refs_1_), channel_id=1, source_target_pairs={{0,8},{4,0},{8,12},{12,4},{1,9},{5,1},{9,13},{13,5},{2,10},{6,2},{... | collective-permute-start | bytes 49160 | tf_op jit(solution)/shard_map/ppermute | solution.py:427
  17.5 0.0 collective-permute-start.7
  17.5 3.0 %collective-permute-start.6 = (f32[8,512]{1,0:T(8,128)S(1)}, f32[8,512]{1,0:T(8,128)S(1)}, u32[]{:S(2)}, u32[]{:S(2)}) collective-permute-start(f32[8,512]{1,0:T(8,128)S(1)} %output.2.refs_0_.refs_1_), channel_id=1, source_target_pairs={{0,12},{4,8},{8,4},{12,0},{1,13},{5,9},{9,5},{13,1},{2,14},{6,10},... | collective-permute-start | bytes 49160 | tf_op jit(solution)/shard_map/ppermute | solution.py:427
  20.5 1.9 %shard_map.236 = (bf16[512,1024]{1,0:T(8,128)(2,1)S(1)}, bf16[512,1024]{1,0:T(8,128)(2,1)S(1)}, bf16[512,512]{1,0:T(8,128)(2,1)S(1)}, bf16[512,512]{1,0:T(8,128)(2,1)S(1)}, bf16[64,512]{1,0:T(8,128)(2,1)S(1)}) custom-call(f32[8,512]{1,0:T(8,128)S(1)} %output.2.refs_0_.refs_1_, bf16[2,512,1024]{2,1,0:T(8,128)(2,1)} %refs_1_.4, bf16[2,512,1024]{2,1,0:T(8,128)(2,1)} %refs_2_.4, ...), custom_call_target="tpu_custom_call" | custom-call | flops 4000000 | bytes 1000000 | tf_op jit(solution)/shard_map/pallas_call | solution.py:485
  22.4 0.0 collective-permute-done.8.refs_4_
  22.5 0.0 collective-permute-done.7.refs_3_
  22.5 0.6 %collective-permute-done.6.refs_2_ = f32[8,512]{1,0:T(8,128)S(1)} collective-permute-done((f32[8,512]{1,0:T(8,128)S(1)}, f32[8,512]{1,0:T(8,128)S(1)}, u32[]{:S(2)}, u32[]{:S(2)}) %collective-permute-start.6) | collective-permute-done | bytes 16416 | tf_op jit(solution)/shard_map/ppermute | solution.py:427
  23.0 0.6 %project.3 = (bf16[8,512]{1,0:T(8,128)(2,1)S(1)}, f32[56,128]{1,0:T(8,128)S(1)}, f32[56,128]{1,0:T(8,128)S(1)}, f32[56,128]{1,0:T(8,128)S(1)}, f32[56,128]{1,0:T(8,128)S(1)}) custom-call(bf16[8,512]{1,0:T(8,128)(2,1)S(1)} %get-tuple-element.42.refs_0_, f32[8,512]{1,0:T(8,128)S(1)} %output.2.refs_0_.refs_1_, f32[8,512]{1,0:T(8,128)S(1)} %collective-permute-done.6.refs_2_, ...), custom_call_target="tpu_custom_call" | custom-call | tf_op jit(solution)/shard_map/project/pallas_call | solution.py:622
  23.7 0.1 collective-permute-start.9
  23.8 1.0 %collective-permute-start.10 = (f32[56,128]{1,0:T(8,128)S(1)}, f32[56,128]{1,0:T(8,128)S(1)}, u32[]{:S(2)}, u32[]{:S(2)}) collective-permute-start(f32[56,128]{1,0:T(8,128)S(1)} %get-tuple-element.63), channel_id=1, source_target_pairs={{0,2},{1,3},{2,0},{3,1},{4,6},{5,7},{6,4},{7,5},{8,10},{9,11},{10,... | collective-permute-start | bytes 86024 | tf_op jit(solution)/shard_map/ppermute | solution.py:421
  24.7 0.9 %collective-permute-start.11 = (f32[56,128]{1,0:T(8,128)S(1)}, f32[56,128]{1,0:T(8,128)S(1)}, u32[]{:S(2)}, u32[]{:S(2)}) collective-permute-start(f32[56,128]{1,0:T(8,128)S(1)} %get-tuple-element.64), channel_id=1, source_target_pairs={{0,3},{1,2},{2,1},{3,0},{4,7},{5,6},{6,5},{7,4},{8,11},{9,10},{10,... | collective-permute-start | bytes 86024 | tf_op jit(solution)/shard_map/ppermute | solution.py:421
  25.6 1.5 %fetch.1 = (f32[2,16,64,128]{3,2,1,0:T(8,128)S(1)}, bf16[1024,512]{1,0:T(8,128)(2,1)S(1)}, bf16[2048,256]{1,0:T(8,128)(2,1)S(1)}) custom-call(f32[56,128]{1,0:T(8,128)S(1)} %get-tuple-element.61.refs_0_, f32[2,2,16,64,128]{4,3,2,1,0:T(8,128)} %refs_1_.5, bf16[2,1024,512]{2,1,0:T(8,128)(2,1)} %refs_2_.5), custom_call_target="tpu_custom_call" | custom-call | flops 4000000 | bytes 1000000 | tf_op jit(solution)/shard_map/fetch/pallas_call | solution.py:498
  27.2 0.0 collective-permute-done.9.refs_1_
  27.2 0.5 %collective-permute-done.10.refs_2_ = f32[56,128]{1,0:T(8,128)S(1)} collective-permute-done((f32[56,128]{1,0:T(8,128)S(1)}, f32[56,128]{1,0:T(8,128)S(1)}, u32[]{:S(2)}, u32[]{:S(2)}) %collective-permute-start.10) | collective-permute-done | bytes 28704 | tf_op jit(solution)/shard_map/ppermute | solution.py:421
  27.7 0.3 collective-permute-done.11.refs_3_
  28.0 0.5 %mix.3 = (bf16[16,128]{1,0:T(8,128)(2,1)S(1)}, f32[2,16,128]{2,1,0:T(8,128)S(1)}, f32[16,128]{1,0:T(8,128)S(1)}, f32[2,8,128]{2,1,0:T(8,128)S(1)}, f32[2,16,128]{2,1,0:T(8,128)S(1)}) custom-call(f32[56,128]{1,0:T(8,128)S(1)} %get-tuple-element.61.refs_0_, f32[56,128]{1,0:T(8,128)S(1)} %collective-permute-done.9.refs_1_, ...), custom_call_target="tpu_custom_call" | custom-call | tf_op jit(solution)/shard_map/mix/pallas_call | solution.py:514
  28.6 0.9 %collective-permute-start.14 = (bf16[16,128]{1,0:T(8,128)(2,1)S(1)}, bf16[16,128]{1,0:T(8,128)(2,1)S(1)}, u32[]{:S(2)}, u32[]{:S(2)}) collective-permute-start(bf16[16,128]{1,0:T(8,128)(2,1)S(1)} %get-tuple-element.66.refs_0_), channel_id=1, source_target_pairs={{0,3},{1,2},{2,1},{3,0},{4,7},{5,6},{6,5},{7,4},{8,11},{9,10},{10,... | collective-permute-start | bytes 12296 | tf_op jit(solution)/shard_map/ppermute | solution.py:421
  29.5 0.9 %collective-permute-start.13 = (bf16[16,128]{1,0:T(8,128)(2,1)S(1)}, bf16[16,128]{1,0:T(8,128)(2,1)S(1)}, u32[]{:S(2)}, u32[]{:S(2)}) collective-permute-start(bf16[16,128]{1,0:T(8,128)(2,1)S(1)} %get-tuple-element.66.refs_0_), channel_id=1, source_target_pairs={{0,2},{1,3},{2,0},{3,1},{4,6},{5,7},{6,4},{7,5},{8,10},{9,11},{10,... | collective-permute-start | bytes 12296 | tf_op jit(solution)/shard_map/ppermute | solution.py:421
  30.4 0.1 collective-permute-start.12
  30.4 1.3 %update.3.refs_5_ = f32[2,2,16,64,128]{4,3,2,1,0:T(8,128)} custom-call(f32[16,128]{1,0:T(8,128)S(1)} %get-tuple-element.68.refs_0_, f32[2,8,128]{2,1,0:T(8,128)S(1)} %get-tuple-element.69.refs_1_, f32[2,16,128]{2,1,0:T(8,128)S(1)} %get-tuple-element.70.refs_2_, f32[2,16,64,128]{3,2,1,0:T(8,128)S(1)} %get-tuple-element.71.refs_3_, ...), custom_call_target="tpu_custom_call", output_to_operand_aliasing={{}: (4, {})} | custom-call | flops 4000000 | bytes 1000000 | tf_op jit(solution)/shard_map/update/pallas_call | solution.py:534
  31.7 0.0 collective-permute-done.14.refs_3_
  31.7 1.3 %collective-permute-done.13.refs_2_ = bf16[16,128]{1,0:T(8,128)(2,1)S(1)} collective-permute-done((bf16[16,128]{1,0:T(8,128)(2,1)S(1)}, bf16[16,128]{1,0:T(8,128)(2,1)S(1)}, u32[]{:S(2)}, u32[]{:S(2)}) %collective-permute-start.13) | collective-permute-done | bytes 4128 | tf_op jit(solution)/shard_map/ppermute | solution.py:421
  33.1 0.0 collective-permute-done.12.refs_1_
  33.1 0.2 output.3.refs_0_
  33.3 0.1 collective-permute-start.17
  33.4 3.5 %collective-permute-start.16 = (f32[8,512]{1,0:T(8,128)S(1)}, f32[8,512]{1,0:T(8,128)S(1)}, u32[]{:S(2)}, u32[]{:S(2)}) collective-permute-start(f32[8,512]{1,0:T(8,128)S(1)} %output.3.refs_0_), channel_id=1, source_target_pairs={{0,8},{4,12},{8,0},{12,4},{1,9},{5,13},{9,1},{13,5},{2,10},{6,14},... | collective-permute-start | bytes 49160 | tf_op jit(solution)/shard_map/ppermute | solution.py:427
  36.9 0.8 %collective-permute-start.15 = (f32[8,512]{1,0:T(8,128)S(1)}, f32[8,512]{1,0:T(8,128)S(1)}, u32[]{:S(2)}, u32[]{:S(2)}) collective-permute-start(f32[8,512]{1,0:T(8,128)S(1)} %output.3.refs_0_), channel_id=1, source_target_pairs={{0,12},{4,8},{8,4},{12,0},{1,13},{5,9},{9,5},{13,1},{2,14},{6,10},... | collective-permute-start | bytes 49160 | tf_op jit(solution)/shard_map/ppermute | solution.py:427
  37.7 1.4 %buffers.1 = (bf16[2,3,2,1024]{3,2,1,0:T(2,128)(2,1)}, bf16[2,3,2,512]{3,2,1,0:T(2,128)(2,1)}, bf16[2,3,2,512]{3,2,1,0:T(2,128)(2,1)}) custom-call(f32[8,512]{1,0:T(8,128)S(1)} %output.3.refs_0_, f32[2,16,128]{2,1,0:T(8,128)S(1)} %get-tuple-element.72.refs_1_, f32[2,16,128]{2,1,0:T(8,128)S(1)} %get-tuple-element.73.refs_2_, ...), custom_call_target="tpu_custom_call" | custom-call | flops 4000000 | bytes 1000000 | tf_op jit(solution)/shard_map/buffers/pallas_call | solution.py:631
  39.1 0.0 collective-permute-done.17.refs_3_
  39.1 0.0 collective-permute-done.16.refs_2_
  39.1 3.3 %collective-permute-done.15.refs_1_ = f32[8,512]{1,0:T(8,128)S(1)} collective-permute-done((f32[8,512]{1,0:T(8,128)S(1)}, f32[8,512]{1,0:T(8,128)S(1)}, u32[]{:S(2)}, u32[]{:S(2)}) %collective-permute-start.15) | collective-permute-done | bytes 16416 | tf_op jit(solution)/shard_map/ppermute | solution.py:427
  42.5 0.6 %close.1 = bf16[8,512]{1,0:T(8,128)(2,1)} custom-call(bf16[8,512]{1,0:T(8,128)(2,1)S(1)} %get-tuple-element.60.x_ref, f32[8,512]{1,0:T(8,128)S(1)} %output.3.refs_0_, f32[8,512]{1,0:T(8,128)S(1)} %collective-permute-done.15.refs_1_, f32[8,512]{1,0:T(8,128)S(1)} %collective-permute-done.16.refs_2_, f32[8,512]{1,0:T(8,128)S(1)} %collective-permute-done.17.refs_3_), custom_call_target="tpu_custom_call" | custom-call | tf_op jit(solution)/shard_map/close/pallas_call | solution.py:642
Async XLA Ops:
  0.6 5.7 %copy-start = (s32[2]{0:T(128)S(1)}, s32[2]{0:T(128)}, u32[]{:S(2)}) copy-start(s32[2]{0:T(128)} %refs_0_.3) | copy-start | bytes 28
  3.2 5.6 %collective-permute-start = (f32[56,128]{1,0:T(8,128)S(1)}, f32[56,128]{1,0:T(8,128)S(1)}, u32[]{:S(2)}, u32[]{:S(2)}) collective-permute-start(f32[56,128]{1,0:T(8,128)S(1)} %get-tuple-element.43), channel_id=1, source_target_pairs={{0,1},{1,0},{2,3},{3,2},{4,5},{5,4},{6,7},{7,6},{8,9},{9,8},{10,11... | collective-permute-start | bytes 86024 | tf_op jit(solution)/shard_map/ppermute | solution.py:421
  3.7 5.0 %collective-permute-start.1 = (f32[56,128]{1,0:T(8,128)S(1)}, f32[56,128]{1,0:T(8,128)S(1)}, u32[]{:S(2)}, u32[]{:S(2)}) collective-permute-start(f32[56,128]{1,0:T(8,128)S(1)} %get-tuple-element.44), channel_id=1, source_target_pairs={{0,2},{1,3},{2,0},{3,1},{4,6},{5,7},{6,4},{7,5},{8,10},{9,11},{10,... | collective-permute-start | bytes 86024 | tf_op jit(solution)/shard_map/ppermute | solution.py:421
  6.3 3.3 %collective-permute-start.2 = (f32[56,128]{1,0:T(8,128)S(1)}, f32[56,128]{1,0:T(8,128)S(1)}, u32[]{:S(2)}, u32[]{:S(2)}) collective-permute-start(f32[56,128]{1,0:T(8,128)S(1)} %get-tuple-element.45), channel_id=1, source_target_pairs={{0,3},{1,2},{2,1},{3,0},{4,7},{5,6},{6,5},{7,4},{8,11},{9,10},{10,... | collective-permute-start | bytes 86024 | tf_op jit(solution)/shard_map/ppermute | solution.py:421
  10.1 3.2 %collective-permute-start.5 = (bf16[16,128]{1,0:T(8,128)(2,1)S(1)}, bf16[16,128]{1,0:T(8,128)(2,1)S(1)}, u32[]{:S(2)}, u32[]{:S(2)}) collective-permute-start(bf16[16,128]{1,0:T(8,128)(2,1)S(1)} %get-tuple-element.48.refs_0_), channel_id=1, source_target_pairs={{0,3},{1,2},{2,1},{3,0},{4,7},{5,6},{6,5},{7,4},{8,11},{9,10},{10,... | collective-permute-start | bytes 12296 | tf_op jit(solution)/shard_map/ppermute | solution.py:421
  11.0 3.6 %collective-permute-start.4 = (bf16[16,128]{1,0:T(8,128)(2,1)S(1)}, bf16[16,128]{1,0:T(8,128)(2,1)S(1)}, u32[]{:S(2)}, u32[]{:S(2)}) collective-permute-start(bf16[16,128]{1,0:T(8,128)(2,1)S(1)} %get-tuple-element.48.refs_0_), channel_id=1, source_target_pairs={{0,2},{1,3},{2,0},{3,1},{4,6},{5,7},{6,4},{7,5},{8,10},{9,11},{10,... | collective-permute-start | bytes 12296 | tf_op jit(solution)/shard_map/ppermute | solution.py:421
  11.9 2.7 %collective-permute-start.3 = (bf16[16,128]{1,0:T(8,128)(2,1)S(1)}, bf16[16,128]{1,0:T(8,128)(2,1)S(1)}, u32[]{:S(2)}, u32[]{:S(2)}) collective-permute-start(bf16[16,128]{1,0:T(8,128)(2,1)S(1)} %get-tuple-element.48.refs_0_), channel_id=1, source_target_pairs={{0,1},{1,0},{2,3},{3,2},{4,5},{5,4},{6,7},{7,6},{8,9},{9,8},{10,11... | collective-permute-start | bytes 12296 | tf_op jit(solution)/shard_map/ppermute | solution.py:421
  14.9 7.6 %collective-permute-start.8 = (f32[8,512]{1,0:T(8,128)S(1)}, f32[8,512]{1,0:T(8,128)S(1)}, u32[]{:S(2)}, u32[]{:S(2)}) collective-permute-start(f32[8,512]{1,0:T(8,128)S(1)} %output.2.refs_0_.refs_1_), channel_id=1, source_target_pairs={{0,8},{4,0},{8,12},{12,4},{1,9},{5,1},{9,13},{13,5},{2,10},{6,2},{... | collective-permute-start | bytes 49160 | tf_op jit(solution)/shard_map/ppermute | solution.py:427
  17.5 5.0 %collective-permute-start.7 = (f32[8,512]{1,0:T(8,128)S(1)}, f32[8,512]{1,0:T(8,128)S(1)}, u32[]{:S(2)}, u32[]{:S(2)}) collective-permute-start(f32[8,512]{1,0:T(8,128)S(1)} %output.2.refs_0_.refs_1_), channel_id=1, source_target_pairs={{0,4},{4,12},{8,0},{12,8},{1,5},{5,13},{9,1},{13,9},{2,6},{6,14},{... | collective-permute-start | bytes 49160 | tf_op jit(solution)/shard_map/ppermute | solution.py:427
  17.5 5.5 %collective-permute-start.6 = (f32[8,512]{1,0:T(8,128)S(1)}, f32[8,512]{1,0:T(8,128)S(1)}, u32[]{:S(2)}, u32[]{:S(2)}) collective-permute-start(f32[8,512]{1,0:T(8,128)S(1)} %output.2.refs_0_.refs_1_), channel_id=1, source_target_pairs={{0,12},{4,8},{8,4},{12,0},{1,13},{5,9},{9,5},{13,1},{2,14},{6,10},... | collective-permute-start | bytes 49160 | tf_op jit(solution)/shard_map/ppermute | solution.py:427
  23.7 3.5 %collective-permute-start.9 = (f32[56,128]{1,0:T(8,128)S(1)}, f32[56,128]{1,0:T(8,128)S(1)}, u32[]{:S(2)}, u32[]{:S(2)}) collective-permute-start(f32[56,128]{1,0:T(8,128)S(1)} %get-tuple-element.62), channel_id=1, source_target_pairs={{0,1},{1,0},{2,3},{3,2},{4,5},{5,4},{6,7},{7,6},{8,9},{9,8},{10,11... | collective-permute-start | bytes 86024 | tf_op jit(solution)/shard_map/ppermute | solution.py:421
  23.8 3.9 %collective-permute-start.10 = (f32[56,128]{1,0:T(8,128)S(1)}, f32[56,128]{1,0:T(8,128)S(1)}, u32[]{:S(2)}, u32[]{:S(2)}) collective-permute-start(f32[56,128]{1,0:T(8,128)S(1)} %get-tuple-element.63), channel_id=1, source_target_pairs={{0,2},{1,3},{2,0},{3,1},{4,6},{5,7},{6,4},{7,5},{8,10},{9,11},{10,... | collective-permute-start | bytes 86024 | tf_op jit(solution)/shard_map/ppermute | solution.py:421
  24.7 3.3 %collective-permute-start.11 = (f32[56,128]{1,0:T(8,128)S(1)}, f32[56,128]{1,0:T(8,128)S(1)}, u32[]{:S(2)}, u32[]{:S(2)}) collective-permute-start(f32[56,128]{1,0:T(8,128)S(1)} %get-tuple-element.64), channel_id=1, source_target_pairs={{0,3},{1,2},{2,1},{3,0},{4,7},{5,6},{6,5},{7,4},{8,11},{9,10},{10,... | collective-permute-start | bytes 86024 | tf_op jit(solution)/shard_map/ppermute | solution.py:421
  28.6 3.2 %collective-permute-start.14 = (bf16[16,128]{1,0:T(8,128)(2,1)S(1)}, bf16[16,128]{1,0:T(8,128)(2,1)S(1)}, u32[]{:S(2)}, u32[]{:S(2)}) collective-permute-start(bf16[16,128]{1,0:T(8,128)(2,1)S(1)} %get-tuple-element.66.refs_0_), channel_id=1, source_target_pairs={{0,3},{1,2},{2,1},{3,0},{4,7},{5,6},{6,5},{7,4},{8,11},{9,10},{10,... | collective-permute-start | bytes 12296 | tf_op jit(solution)/shard_map/ppermute | solution.py:421
  29.5 3.6 %collective-permute-start.13 = (bf16[16,128]{1,0:T(8,128)(2,1)S(1)}, bf16[16,128]{1,0:T(8,128)(2,1)S(1)}, u32[]{:S(2)}, u32[]{:S(2)}) collective-permute-start(bf16[16,128]{1,0:T(8,128)(2,1)S(1)} %get-tuple-element.66.refs_0_), channel_id=1, source_target_pairs={{0,2},{1,3},{2,0},{3,1},{4,6},{5,7},{6,4},{7,5},{8,10},{9,11},{10,... | collective-permute-start | bytes 12296 | tf_op jit(solution)/shard_map/ppermute | solution.py:421
  30.4 2.7 %collective-permute-start.12 = (bf16[16,128]{1,0:T(8,128)(2,1)S(1)}, bf16[16,128]{1,0:T(8,128)(2,1)S(1)}, u32[]{:S(2)}, u32[]{:S(2)}) collective-permute-start(bf16[16,128]{1,0:T(8,128)(2,1)S(1)} %get-tuple-element.66.refs_0_), channel_id=1, source_target_pairs={{0,1},{1,0},{2,3},{3,2},{4,5},{5,4},{6,7},{7,6},{8,9},{9,8},{10,11... | collective-permute-start | bytes 12296 | tf_op jit(solution)/shard_map/ppermute | solution.py:421
  33.3 5.8 %collective-permute-start.17 = (f32[8,512]{1,0:T(8,128)S(1)}, f32[8,512]{1,0:T(8,128)S(1)}, u32[]{:S(2)}, u32[]{:S(2)}) collective-permute-start(f32[8,512]{1,0:T(8,128)S(1)} %output.3.refs_0_), channel_id=1, source_target_pairs={{0,4},{4,0},{8,12},{12,8},{1,5},{5,1},{9,13},{13,9},{2,6},{6,2},{1... | collective-permute-start | bytes 49160 | tf_op jit(solution)/shard_map/ppermute | solution.py:427
  33.4 5.7 %collective-permute-start.16 = (f32[8,512]{1,0:T(8,128)S(1)}, f32[8,512]{1,0:T(8,128)S(1)}, u32[]{:S(2)}, u32[]{:S(2)}) collective-permute-start(f32[8,512]{1,0:T(8,128)S(1)} %output.3.refs_0_), channel_id=1, source_target_pairs={{0,8},{4,12},{8,0},{12,4},{1,9},{5,13},{9,1},{13,5},{2,10},{6,14},... | collective-permute-start | bytes 49160 | tf_op jit(solution)/shard_map/ppermute | solution.py:427
  36.9 5.5 %collective-permute-start.15 = (f32[8,512]{1,0:T(8,128)S(1)}, f32[8,512]{1,0:T(8,128)S(1)}, u32[]{:S(2)}, u32[]{:S(2)}) collective-permute-start(f32[8,512]{1,0:T(8,128)S(1)} %output.3.refs_0_), channel_id=1, source_target_pairs={{0,12},{4,8},{8,4},{12,0},{1,13},{5,9},{9,5},{13,1},{2,14},{6,10},... | collective-permute-start | bytes 49160 | tf_op jit(solution)/shard_map/ppermute | solution.py:427
